TPU v7x, 128 devices: a whole 4x4x4 slice. The times are simulated.
128 devices in a mesh: fs: 16 (over z, y), tp: 8 (over x, core).
Axes of the slice: x: 4, y: 4, z: 4, core: 2. Of those that a mesh axis runs over, the one named last changes fastest.
Arguments:
- resid: bfloat16 [16384, 2048], P(('fs', 'tp')), may hold values from -6 to 6
- mix_gain: float32 [2048], replicated, may hold values from 0.1 to 1.9
- w_query: bfloat16 [2048, 1024], P('fs', 'tp'), may hold values from -0.125 to 0.125
- w_key: bfloat16 [2048, 1024], P('fs', 'tp'), may hold values from -0.125 to 0.125
- w_value: bfloat16 [2048, 2048], P('fs', 'tp'), may hold values from -0.125 to 0.125
- w_gate: bfloat16 [2048, 2048], P('fs', 'tp'), may hold values from -0.125 to 0.125
- w_output: bfloat16 [2048, 2048], P('tp', 'fs'), may hold values from -0.125 to 0.125
- decay_rate: float32 [8], P('tp'), may hold values from 0.0008 to 0.034, as said below
- mlp_gain: float32 [2048], replicated, may hold values from 0.1 to 1.9
- w_up: bfloat16 [2048, 8192], P('fs', 'tp'), may hold values from -0.125 to 0.125
- w_down: bfloat16 [8192, 2048], P('tp', 'fs'), may hold values from -0.0625 to 0.0625
Outputs:
- layer_out: bfloat16 [16384, 2048], P(('fs', 'tp'))
Inputs may be any that keep to these rules, and one draw needn't show every extreme that they name: `decay_rate`: decay rates per position, one for each head.
All inputs are finite; a program needn't handle non-finite values.
Results may differ from a plain program's by a relative error of at most 0.038.
Values may be sent and summed in bfloat16 or wider, within the bound.
A program may use at most 64 MiB of HBM per device.

v0:
```python
import jax
import jax.numpy as jnp
from jax import lax
from jax.sharding import PartitionSpec as P

DK = 128
DV = 256
BLOCK = 128
LENGTH = 512


epsilon = 1e-06


def side_by_side(arrays, axis, dim, along):
    widths = [a.shape[along] for a in arrays]
    both = jnp.concatenate(arrays, axis=along)
    whole = lax.all_gather(both, axis, axis=dim, tiled=True)
    return tuple(jnp.split(whole, [sum(widths[:k]) for k in range(1, len(widths))], axis=along))


def joined_along(tiles, dim):
    tiles = jnp.moveaxis(tiles, 0, dim)
    lengths = tiles.shape
    return tiles.reshape(*lengths[:dim], lengths[dim] * lengths[dim + 1], *lengths[dim + 2 :])


def from_everyone(value, axis):
    devices = lax.axis_size(axis)
    return lax.all_to_all(
        jnp.broadcast_to(value[None], (devices, *value.shape)), axis, 0, 0, tiled=True
    )


def gather_directly(value, axis, dim):
    return joined_along(from_everyone(value, axis), dim)


def cut_along(value, dim, devices):
    lengths = value.shape
    tiles = value.reshape(*lengths[:dim], devices, lengths[dim] // devices, *lengths[dim + 1 :])
    return jnp.moveaxis(tiles, dim, 0)


def sent_and_summed(value, axis, dim):
    devices = lax.axis_size(axis)
    tiles = lax.all_to_all(cut_along(value, dim, devices), axis, 0, 0, tiled=True)
    return jnp.sum(tiles.astype(jnp.float32), axis=0)


def rms_scale(source, gains):
    widened = source.astype(jnp.float32)
    scaled = widened * lax.rsqrt(jnp.mean(widened * widened, axis=-1, keepdims=True) + epsilon)
    return (scaled * gains).astype(jnp.bfloat16)


def retention(queries, key_rows, values, rates):
    seq_count, length, head_count, key_width = queries.shape
    value_width = values.shape[-1]
    block_count = length // BLOCK
    queries = queries.reshape(seq_count, block_count, BLOCK, head_count, key_width)
    key_rows = key_rows.reshape(
        seq_count, block_count, BLOCK, head_count, key_width
    ) * key_width ** (-0.5)
    values = values.reshape(seq_count, block_count, BLOCK, head_count, value_width)
    places = jnp.arange(BLOCK, dtype=jnp.float32)
    offset = places[:, None] - places[None, :]
    causal = offset >= 0
    inner_decay = jnp.where(
        causal[None], jnp.exp(-rates[:, None, None] * jnp.where(causal, offset, 0.0)[None]), 0.0
    )
    scores = jnp.einsum("bnihd,bnjhd->bnhij", queries, key_rows) * inner_decay[None, None]
    within = jnp.einsum("bnhij,bnjhe->bnihe", scores, values)
    key_decayed = (
        key_rows
        * jnp.exp(-rates[None, :] * (BLOCK - 1.0 - places)[:, None])[None, None, :, :, None]
    )
    updates = jnp.einsum("bnjhd,bnjhe->nbhde", key_decayed, values)
    carry_decay = jnp.exp(-rates * BLOCK)[None, :, None, None]

    def advance(memory, update):
        return (carry_decay * memory + update, memory)

    _, before = lax.scan(
        advance, jnp.zeros((seq_count, head_count, key_width, value_width), jnp.float32), updates
    )
    query_decayed = (
        queries * jnp.exp(-rates[None, :] * (places + 1.0)[:, None])[None, None, :, :, None]
    )
    carried = jnp.einsum("bnihd,nbhde->bnihe", query_decayed, before)
    mixed = (within + carried).reshape(seq_count, length, head_count, value_width)
    centre = jnp.mean(mixed, axis=-1, keepdims=True)
    spread = jnp.mean(jnp.square(mixed - centre), axis=-1, keepdims=True)
    return (mixed - centre) * lax.rsqrt(spread + epsilon)


def heads_view(source, width):
    return source.astype(jnp.float32).reshape(-1, LENGTH, source.shape[1] // width, width)


def on_device(
    resid, mix_gain, w_query, w_key, w_value, w_gate, w_output, decay_rate, mlp_gain, w_up, w_down
):
    up_whole = lax.all_gather(w_up, "fs", axis=0, tiled=True)
    down_whole = lax.all_gather(w_down, "fs", axis=1, tiled=True)
    normed = lax.all_gather(rms_scale(resid, mix_gain), "tp", axis=0, tiled=True)
    tokens = normed.shape[0]
    pieces = side_by_side((w_query, w_key, w_value, w_gate), "fs", 0, 1)
    projected = tuple(
        (jnp.dot(normed, shard_rows, preferred_element_type=jnp.float32) for shard_rows in pieces)
    )
    queries, key_rows, values, gate_rows = (
        member_sum.astype(jnp.bfloat16) for member_sum in projected
    )
    output_whole = gather_directly(w_output, "fs", 1)
    grouped = retention(
        heads_view(queries, DK), heads_view(key_rows, DK), heads_view(values, DV), decay_rate
    )
    gated = (jax.nn.silu(gate_rows.astype(jnp.float32)) * grouped.reshape(tokens, -1)).astype(
        jnp.bfloat16
    )
    mix_sum = sent_and_summed(
        jnp.dot(gated, output_whole, preferred_element_type=jnp.float32).astype(jnp.bfloat16),
        "tp",
        0,
    )
    after_mix = (resid.astype(jnp.float32) + mix_sum).astype(jnp.bfloat16)
    normed_mlp = lax.all_gather(rms_scale(after_mix, mlp_gain), "tp", axis=0, tiled=True)
    lifted = jnp.dot(normed_mlp, up_whole, preferred_element_type=jnp.float32)
    hidden = jnp.square(jax.nn.relu(lifted)).astype(jnp.bfloat16)
    mlp_sum = lax.psum_scatter(
        jnp.dot(hidden, down_whole, preferred_element_type=jnp.float32).astype(jnp.bfloat16),
        "tp",
        scatter_dimension=0,
        tiled=True,
    ).astype(jnp.float32)
    return (after_mix.astype(jnp.float32) + mlp_sum).astype(jnp.bfloat16)


def solution(mesh):
    placed = (
        P(("fs", "tp"), None),
        P(),
        P("fs", "tp"),
        P("fs", "tp"),
        P("fs", "tp"),
        P("fs", "tp"),
        P("tp", "fs"),
        P("tp"),
        P(),
        P("fs", "tp"),
        P("tp", "fs"),
    )
    return jax.shard_map(
        on_device, mesh=mesh, in_specs=placed, out_specs=P(("fs", "tp"), None), check_vma=False
    )
```

profile of v0, /device:TPU:1, one launch (start us, length us, event | category | flops | bytes accessed | tf_op | source)
XLA Modules:
  0.0 305.5 jit_solution(976130120628553870)
XLA Ops:
  6.5 1.6 pad_maximum_fusion
  8.2 1.2 fusion.7
  9.4 2.0 fusion.9
  11.5 0.7 all-gather.12.cloned.1.call-update
  12.2 0.9 copy.31
  13.2 1.1 broadcast_in_dim.18
  14.3 8.6 %all-to-all-start = ((bf16[16,256,128]{1,2,0:T(8,128)(2,1)}), bf16[16,256,128]{1,2,0:T(8,128)(2,1)}, u32[]{:S(2)}, u32[]{:S(2)}) async-start(bf16[16,256,128]{1,2,0:T(8,128)(2,1)} %broadcast_in_dim.18), calls=%async_computation | async-start | bytes 2097152 | tf_op jit(solution)/shard_map/all_to_all | solution.py:30
  23.0 0.5 all-gather.14.cloned.1.call-update
  24.3 44.8 %all-gather.8.cloned.1.call-done = bf16[2048,768]{1,0:T(8,128)(2,1)} async-done(((bf16[128,768]{1,0:T(8,128)(2,1)}), bf16[2048,768]{1,0:T(8,128)(2,1)}) %all-gather.8.cloned.1.call-update) | async-done | bytes 3145744 | tf_op jit(solution)/shard_map/all_gather | solution.py:18
  69.1 33.4 %all-gather.6.cloned.1.call-done = bf16[1024,2048]{1,0:T(8,128)(2,1)} async-done(((bf16[128,2048]{1,0:T(8,128)(2,1)}), bf16[1024,2048]{1,0:T(8,128)(2,1)}) %all-gather.6.cloned.1.call-update) | async-done | bytes 4194320 | tf_op jit(solution)/shard_map/all_gather | solution.py:106
  102.5 3.5 %convolution_convert_fusion.4 = bf16[1024,128]{1,0:T(8,128)(2,1)S(1)} fusion(bf16[1024,2048]{1,0:T(8,128)(2,1)} %all-gather.6.cloned.1.call-done, bf16[2048,768]{1,0:T(8,128)(2,1)} %all-gather.8.cloned.1.call-done), kind=kOutput, calls=%fused_computation.22 | convolution fusion | flops 537001984 | bytes 4980736 | tf_op jit(solution)/shard_map/dot_general | solution.py:110
  106.1 0.1 copy.27
  106.2 3.7 %convolution_convert_fusion.2 = bf16[1024,256]{1,0:T(8,128)(2,1)S(1)} fusion(bf16[1024,2048]{1,0:T(8,128)(2,1)} %all-gather.6.cloned.1.call-done, bf16[2048,768]{1,0:T(8,128)(2,1)} %all-gather.8.cloned.1.call-done), kind=kOutput, calls=%fused_computation.18 | convolution fusion | flops 1074003968 | bytes 5767168 | tf_op jit(solution)/shard_map/dot_general | solution.py:110
  110.0 0.3 convolution_bitcast_fusion
  110.3 0.5 while.13
  110.8 3.5 %convolution_convert_fusion.5 = bf16[1024,128]{1,0:T(8,128)(2,1)S(1)} fusion(bf16[1024,2048]{1,0:T(8,128)(2,1)} %all-gather.6.cloned.1.call-done, bf16[2048,768]{1,0:T(8,128)(2,1)} %all-gather.8.cloned.1.call-done), kind=kOutput, calls=%fused_computation.23 | convolution fusion | flops 537001984 | bytes 4980736 | tf_op jit(solution)/shard_map/dot_general | solution.py:110
  114.4 0.5 fusion.1
  114.8 0.4 bitcast_reduce_fusion
  115.3 0.4 fusion.20
  115.7 0.3 fusion.18
  116.0 9.1 %convolution_convert_fusion = bf16[1024,2048]{1,0:T(8,128)(2,1)} fusion(bf16[256,2048]{0,1:T(8,128)(2,1)} %bitcast.16, f32[1024,256]{1,0:T(8,128)S(1)} %fusion.18, bf16[1024,2048]{1,0:T(8,128)(2,1)} %all-gather.6.cloned.1.call-done, bf16[2048,768]{1,0:T(8,128)(2,1)} %all-gather.8.cloned.1.call-done), kind=kOutput, calls=%fused_computation.6 | convolution fusion | flops 2151677952 | bytes 11534336 | tf_op jit(solution)/shard_map/dot_general | solution.py:123
  125.1 52.5 %all_to_all.10 = bf16[8,128,2048]{2,1,0:T(8,128)(2,1)S(1)} all-to-all(bf16[8,128,2048]{2,1,0:T(8,128)(2,1)} %bitcast.71), channel_id=1, replica_groups=mesh['fs'=16,'tp'=8] {'tp'}, dimensions={0} | all-to-all | bytes 8388608 | tf_op jit(solution)/shard_map/all_to_all | solution.py:47
  177.6 0.7 convert_reduce_fusion
  178.4 0.3 copy-done
  178.7 0.2 fusion.11
  178.9 1.0 fusion.13
  180.0 0.2 reduce-scatter.2.cloned.1.call-start
  180.2 32.8 %all-gather.14.cloned.1.call-done = bf16[1024,2048]{1,0:T(8,128)(2,1)} async-done(((bf16[1024,128]{1,0:T(8,128)(2,1)}), bf16[1024,2048]{1,0:T(8,128)(2,1)}) %all-gather.14.cloned.1.call-update) | async-done | bytes 4194320 | tf_op jit(solution)/shard_map/all_gather | solution.py:105
  213.0 34.6 %all-gather.10.cloned.1.call-done = bf16[1024,2048]{1,0:T(8,128)(2,1)} async-done(((bf16[128,2048]{1,0:T(8,128)(2,1)}), bf16[1024,2048]{1,0:T(8,128)(2,1)}) %all-gather.10.cloned.1.call-update) | async-done | bytes 4194320 | tf_op jit(solution)/shard_map/all_gather | solution.py:128
  247.6 14.4 %convolution_convert_fusion.1 = bf16[1024,2048]{1,0:T(8,128)(2,1)} fusion(bf16[1024,2048]{1,0:T(8,128)(2,1)} %all-gather.14.cloned.1.call-done, bf16[1024,2048]{1,0:T(8,128)(2,1)} %all-gather.10.cloned.1.call-done, bf16[2048,1024]{1,0:T(8,128)(2,1)} %all-gather.12.cloned.1.call-done), kind=kOutput, calls=%fused_computation.7 | convolution fusion | flops 8595177472 | bytes 16777216 | tf_op jit(solution)/shard_map/dot_general | solution.py:132
  262.0 34.7 %reduce-scatter.2.cloned.1.call-done = bf16[128,2048]{1,0:T(8,128)(2,1)} async-done(((bf16[1024,2048]{1,0:T(8,128)(2,1)}), bf16[128,2048]{1,0:T(8,128)(2,1)}) %reduce-scatter.2.cloned.1.call-update) | async-done | bytes 524304 | tf_op jit(solution)/shard_map/reduce_scatter | solution.py:131
  296.7 2.0 fusion.14
  (30 shorter events, 0.8 us)
Async XLA Ops:
  6.5 62.6 %all-gather.8.cloned.1.call-start = ((), (), s32[]{:S(2)}) async-start(), calls=%async_computation.4 | async-start | bytes 3342336 | tf_op jit(solution)/shard_map/all_gather | solution.py:18
  8.1 94.4 %all-gather.6.cloned.1.call-start = ((), (), s32[]{:S(2)}) async-start(), calls=%async_computation.3 | async-start | bytes 4718592 | tf_op jit(solution)/shard_map/all_gather | solution.py:106
  11.5 168.7 %all-gather.12.cloned.1.call-start = ((), (), s32[]{:S(2)}) async-start(), calls=%async_computation.6 | async-start | bytes 4456448 | tf_op jit(solution)/shard_map/all_gather | solution.py:104
  14.3 101.7 %all-to-all-start = ((bf16[16,256,128]{1,2,0:T(8,128)(2,1)}), bf16[16,256,128]{1,2,0:T(8,128)(2,1)}, u32[]{:S(2)}, u32[]{:S(2)}) async-start(bf16[16,256,128]{1,2,0:T(8,128)(2,1)} %broadcast_in_dim.18), calls=%async_computation | async-start | bytes 2097152 | tf_op jit(solution)/shard_map/all_to_all | solution.py:30
  22.9 190.1 %all-gather.14.cloned.1.call-start = ((), (), s32[]{:S(2)}) async-start(), calls=%async_computation.7 | async-start | bytes 4456448 | tf_op jit(solution)/shard_map/all_gather | solution.py:105
  23.5 224.1 %all-gather.10.cloned.1.call-start = ((), (), s32[]{:S(2)}) async-start(), calls=%async_computation.5 | async-start | bytes 4718592 | tf_op jit(solution)/shard_map/all_gather | solution.py:128
  177.6 1.1 copy-start
  177.6 1.3 copy-start.1
  180.0 116.8 %reduce-scatter.2.cloned.1.call-start = ((), (), s32[]{:S(2)}) async-start(), calls=%async_computation.8 | async-start | bytes 4718592 | tf_op jit(solution)/shard_map/reduce_scatter | solution.py:131
Sparse Core Ops, SparseCore 0:
  9.5 59.6 all-gather.7
  70.9 31.6 all-gather.5
  104.7 50.9 all-gather.11
  157.6 55.3 all-gather.13
  214.6 32.9 all-gather.9
  262.1 34.5 reduce-scatter.1
where the time goes:
time: 308 us; the launch traced here: 306 us
  waiting for transfers between devices  182 us (59%)
  blocking collectives  52.5 us (17%)
  matrix products  35.5 us (12%)
  between operations  14.3 us (5%)
  other arithmetic  9.99 us (3%)
  starting transfers between devices  9.02 us (3%)
    all_to_all x1, blocking collectives, sent_and_summed(): lax.all_to_all(cut_along(value, dim, devices), axis, 0, 0, tiled=True)  52.5 us
    all_gather x1, waiting for transfers between devices, side_by_side(): whole = lax.all_gather(both, axis, axis=dim, tiled=True)  44.8 us
    reduce_scatter x1, waiting for transfers between devices, on_device(): lax.psum_scatter(jnp.dot(hidden, down_whole, preferred_element_type=jnp.f...  34.7 us
    all_gather x1, waiting for transfers between devices, on_device(): lax.all_gather(rms_scale(after_mix, mlp_gain), 'tp', axis=0, tiled=True)  34.6 us
    all_gather x1, waiting for transfers between devices, on_device(): lax.all_gather(rms_scale(resid, mix_gain), 'tp', axis=0, tiled=True)  33.4 us
    all_gather x1, waiting for transfers between devices, on_device(): down_whole = lax.all_gather(w_down, 'fs', axis=1, tiled=True)  32.8 us
    dot_general x1, matrix products, on_device(): jnp.dot(hidden, down_whole, preferred_element_type=jnp.float32)  14.4 us
    dot_general x3, matrix products, on_device(): jnp.dot(normed, shard_rows, preferred_element_type=jnp.float32)  10.8 us
  transfers between devices with their start and end apart: 7, of which 5 were waited for; matrix products, arithmetic and copies ran while one was open for 10% of the time, Pallas kernels for 0%

commit v1 on v0

v1 whole, which is shorter than its diff:
```python
import jax
import jax.numpy as jnp
from jax import lax
from jax.experimental import pallas as pl
from jax.experimental.pallas import tpu as pltpu
from jax.sharding import PartitionSpec as P

D = 2048
DK = 128
DV = 256
LENGTH = 512
RING = 4
EPS = 1e-06
MESH = pl.DeviceIdType.MESH
F32 = jnp.float32
BF16 = jnp.bfloat16

STEP = {"y+": (1, 0), "y-": (-1, 0), "z+": (0, 1), "z-": (0, -1)}


def near(d):
    return {0: 0, 1: 1, 2: 2, 3: -1}[d % RING]


def arrived(message):
    dy, dz, part, way = message
    return near(dy - STEP[way][0]), near(dz - STEP[way][1]), part, way


def onward(message):
    dy, dz, part, way = arrived(message)
    half = "0" if way[1] == "+" else "1"
    across = ("z+", "z-") if way[0] == "y" else ("y+", "y-")
    first = "A" if way[0] == "y" else "B"
    if part == "full":
        return [(dy, dz, "h" + half, way)] + [(dy, dz, first, w) for w in across]
    if part in ("h0", "h1"):
        return [(dy, dz, first + part, w) for w in across]
    if part in ("A", "B"):
        return [(dy, dz, part + "h" + half, way)]
    far = dy if part[0] == "A" else dz
    last = dz if part[0] == "A" else dy
    if far == 2 and last != 2 and part[-1] == half:
        return [(dy, dz, part, way)]
    return []


def plan():
    rounds = [[(0, 0, "full", w) for w in ("y+", "y-", "z+", "z-")]]
    while rounds[-1]:
        rounds.append([m for sent in rounds[-1] for m in onward(sent)])
    return rounds[:-1]


ROUNDS = plan()
MESSAGES = [m for sent in ROUNDS for m in sent]
NUMBER = {m: i for i, m in enumerate(MESSAGES)}

GATHER = (
    [(0, h, w) for h in (0, 1) for w in ("x+", "x-", "d")]
    + [(-1, h, "d") for h in (0, 1)]
    + [(1, h, "d") for h in (0, 1)]
    + [(-1, 0, "x+"), (1, 1, "x-")]
    + [(2, h, "d") for h in (0, 1)]
)
GATHER_NUMBER = {m: i for i, m in enumerate(GATHER)}
TURN = {2: 0, 1: 1, -1: 2, 0: 3}


def kernel(
    resid, mix_gain, wq, wk, wv, wg, wo, rate, mlp_gain, wu, wd,
    out,
    w_in, w_out, w_up, w_down, xn, rbuf, after, proj, gated, hid, decay, kept,
    dout, din, sout, rin2, rin1,
    local_sem, w_send, w_recv, g_send, g_recv, d_send, d_recv, s_send, s_recv,
):
    fs, tp = lax.axis_index("fs"), lax.axis_index("tp")
    z, y, x, c = fs // RING, fs % RING, tp // 2, tp % 2

    def turn(v, d):
        return (v + d + RING) % RING

    device = {
        "y+": (z * RING + turn(y, 1), tp),
        "y-": (z * RING + turn(y, -1), tp),
        "z+": (turn(z, 1) * RING + y, tp),
        "z-": (turn(z, -1) * RING + y, tp),
        "x+": (fs, turn(x, 1) * 2 + c),
        "x-": (fs, turn(x, -1) * 2 + c),
        "d": (fs, x * 2 + 1 - c),
    }
    started = []

    def remote(src, dst, send, recv, way):
        return pltpu.make_async_remote_copy(
            src_ref=src, dst_ref=dst, send_sem=send, recv_sem=recv,
            device_id=device[way], device_id_type=MESH,
        )

    def send(*args):
        copy = remote(*args)
        copy.start()
        started.append(copy)

    weights = (w_in, w_out, w_up, w_down)

    def piece(t, dy, dz, part):
        ref = weights[t]
        f = turn(z, dz) * RING + turn(y, dy)
        if part == "full":
            return ref.at[f]
        if part in ("A", "B"):
            return ref.at[f, :, "AB".index(part)]
        if part in ("h0", "h1"):
            return ref.at[f, int(part[1])]
        return ref.at[f, int(part[2]), "AB".index(part[0])]

    def w_send_one(t, message):
        dy, dz, part, way = message
        n = NUMBER[message]
        ref = piece(t, dy, dz, part)
        send(ref, ref, w_send.at[t, n], w_recv.at[t, n], way)

    def w_first(t):
        for message in ROUNDS[0]:
            w_send_one(t, message)

    def pump(t, r):
        for message in ROUNDS[r - 1]:
            dy, dz, part, way = arrived(message)
            n = NUMBER[message]
            ref = piece(t, dy, dz, part)
            remote(ref, ref, w_send.at[t, n], w_recv.at[t, n], way).wait_recv()
            for following in onward(message):
                w_send_one(t, following)

    def g_piece(g, dx, h, core):
        return xn.at[g, turn(x, dx) * 2 + core, h]

    def g_send_one(g, message):
        dx, h, way = message
        n = GATHER_NUMBER[message]
        ref = g_piece(g, dx, h, c)
        send(ref, ref, g_send.at[g, n], g_recv.at[g, n], way)

    def g_wait(g, message):
        dx, h, way = message
        n = GATHER_NUMBER[message]
        if way == "d":
            ref = g_piece(g, dx, h, 1 - c)
        else:
            ref = g_piece(g, near(dx - (1 if way == "x+" else -1)), h, c)
        remote(ref, ref, g_send.at[g, n], g_recv.at[g, n], way).wait_recv()

    def g_first(g, h):
        for way in ("x+", "x-", "d"):
            g_send_one(g, (0, h, way))

    def g_near(g, h):
        g_wait(g, (0, h, "x+"))
        if h == 0:
            g_send_one(g, (-1, 0, "x+"))
        g_send_one(g, (-1, h, "d"))
        g_wait(g, (0, h, "x-"))
        if h == 1:
            g_send_one(g, (1, 1, "x-"))
        g_send_one(g, (1, h, "d"))

    def g_far(g):
        g_wait(g, (-1, 0, "x+"))
        g_send_one(g, (2, 0, "d"))
        g_wait(g, (1, 1, "x-"))
        g_send_one(g, (2, 1, "d"))

    def g_partner(g, dx):
        for h in (0, 1):
            g_wait(g, (dx, h, "d"))

    def rows16(body):
        def step(i, carry):
            body(pl.ds(pl.multiple_of(i * 16, 16), 16), i * 16)
            return carry

        lax.fori_loop(0, 4, step, 0)

    def d_copy(g, k):
        return (dout.at[g, k], din.at[g, k], d_send.at[g, k], d_recv.at[g, k], "d")

    def s_copy(g, n):
        if n == 0:
            src, dst, way = sout.at[g, 0, 0], rin2.at[g, 0], "x+"
        elif n == 1:
            src, dst, way = sout.at[g, 0, 1], rin2.at[g, 1], "x-"
        elif n < 4:
            src, dst, way = sout.at[g, 1, n - 2], rin1.at[g, 0, n - 2], "x+"
        else:
            src, dst, way = sout.at[g, 2, n - 4], rin1.at[g, 1, n - 4], "x-"
        return (src, dst, s_send.at[g, n], s_recv.at[g, n], way)

    def partial(g, dx, lhs, weight):
        k = TURN[dx]
        depth = weight.shape[1] * weight.shape[2] * weight.shape[3]

        def step(j, carry):
            w = jnp.concatenate([weight[4 * j + i].reshape(depth, 128) for i in range(4)], axis=1)
            o = jnp.dot(lhs(), w, preferred_element_type=F32)
            columns = pl.ds(pl.multiple_of(j * 512, 512), 512)
            dout[g, k, 0, :, columns] = o[:64].astype(BF16)
            dout[g, k, 1, :, columns] = o[64:128].astype(BF16)
            kept[k, :, columns] = o[128:]
            return carry

        lax.fori_loop(0, 4, step, 0)
        send(*d_copy(g, k))

    def add_half(g, k, h, extra=None):
        def body(rows, first):
            at = pl.ds(pl.multiple_of(h * 64 + first, 16), 16)
            total = kept[k, at, :] + din[g, k, h, rows, :].astype(F32)
            if extra is not None:
                total = total + rin2[g, extra, rows, :].astype(F32)
            sout[g, k, h, rows, :] = total.astype(BF16)

        rows16(body)

    def d_wait(g, k):
        remote(*d_copy(g, k)).wait_recv()

    def s_wait(g, n):
        remote(*s_copy(g, n)).wait_recv()

    def combine_far(g):
        d_wait(g, 0)
        add_half(g, 0, 0)
        send(*s_copy(g, 0))
        add_half(g, 0, 1)
        send(*s_copy(g, 1))

    def combine_free(g):
        d_wait(g, 1)
        add_half(g, 1, 1)
        send(*s_copy(g, 3))
        d_wait(g, 2)
        add_half(g, 2, 0)
        send(*s_copy(g, 4))

    def combine_near(g):
        s_wait(g, 0)
        add_half(g, 1, 0, 0)
        send(*s_copy(g, 2))
        s_wait(g, 1)
        add_half(g, 2, 1, 1)
        send(*s_copy(g, 5))

    def sum_rows(g, h, rows, first):
        at = pl.ds(pl.multiple_of(h * 64 + first, 16), 16)
        total = kept[3, at, :] + din[g, 3, h, rows, :].astype(F32)
        return total + rin1[g, 0, h, rows, :].astype(F32) + rin1[g, 1, h, rows, :].astype(F32)

    def normed(values, gain):
        scale = lax.rsqrt(jnp.mean(values * values, axis=-1, keepdims=True) + EPS)
        return (values * scale * gain).astype(BF16)

    loads = []

    def load(src, dst):
        copy = pltpu.make_async_copy(src, dst, local_sem.at[len(loads)])
        copy.start()
        loads.append(copy)

    for src, low, wide in ((wq, 0, 128), (wk, 128, 128), (wv, 256, 256), (wg, 512, 256)):
        load(src, w_in.at[fs, :, :, :, low : low + wide])
    load(resid, rbuf)
    load(wo, w_out.at[fs])
    load(wu, w_up.at[fs])
    load(wd, w_down.at[fs])
    barrier = pltpu.get_barrier_semaphore()
    for way in device:
        pl.semaphore_signal(barrier, inc=1, device_id=device[way], device_id_type=MESH)
    for copy in loads[:5]:
        copy.wait()
    for h in (0, 1):
        def first_norm(rows, first):
            xn[0, tp, h, rows, :] = normed(rbuf[h, rows, :].astype(F32), mix_gain[...])

        rows16(first_norm)
    pl.semaphore_wait(barrier, 7)
    w_first(0)
    g_first(0, 0)
    g_first(0, 1)
    loads[5].wait()
    w_first(1)

    r = rate[0]

    def decay_rows(i, carry):
        rows = pl.ds(pl.multiple_of(i * 64, 64), 64)
        t = lax.broadcasted_iota(jnp.int32, (64, LENGTH), 0) + i * 64
        s = lax.broadcasted_iota(jnp.int32, (64, LENGTH), 1)
        gap = (t - s).astype(F32)
        value = jnp.exp(-r * jnp.maximum(gap, 0.0)) * DK ** (-0.5)
        decay[rows, :] = jnp.where(gap >= 0.0, value, 0.0)
        return carry

    lax.fori_loop(0, LENGTH // 64, decay_rows, 0)

    def project(first_pair, step):
        rhs = lambda j: w_in[:, :, :, :, pl.ds(pl.multiple_of(j * 256, 256), 256)].reshape(D, 256)

        def body(n, carry):
            pair = first_pair + n // 3 * step
            j = n % 3
            lhs = xn[0, pl.ds(2 * pair, 2)].reshape(256, D)
            o = jnp.dot(lhs, rhs(j), preferred_element_type=F32).astype(BF16)
            columns = pl.ds(pl.multiple_of(j * 256, 256), 256)
            proj[pl.ds(2 * pair, 2), :, columns] = o.reshape(2, 128, 256)
            return carry

        lax.fori_loop(0, 6, body, 0)

    def retain(seq):
        for i in (0, 1):
            mine = pl.ds(seq * 4 + 2 * i, 2)
            upto = pl.ds(seq * 4, 2 * i + 2)
            wide = 256 * (i + 1)
            q = proj[mine, :, 0:128].reshape(256, DK)
            k = proj[upto, :, 128:256].reshape(wide, DK)
            v = proj[upto, :, 256:512].reshape(wide, DV)
            scores = lax.dot_general(q, k, (((1,), (1,)), ((), ())), preferred_element_type=F32)
            scores = (scores * decay[i * 256 : (i + 1) * 256, 0:wide]).astype(BF16)
            mixed = jnp.dot(scores, v, preferred_element_type=F32)
            mixed = mixed - jnp.mean(mixed, axis=-1, keepdims=True)
            spread = jnp.mean(mixed * mixed, axis=-1, keepdims=True)
            gate = proj[mine, :, 512:768].reshape(256, DV).astype(F32)
            value = gate / (1.0 + jnp.exp(-gate)) * (mixed * lax.rsqrt(spread + EPS))
            gated[mine] = value.astype(BF16).reshape(2, 128, DV)

    def gated_rows(dx):
        first = turn(x, dx) * 2
        return lambda: jnp.concatenate([gated[first + 1 - c], gated[first + c]], axis=0)

    pump(0, 1)
    pump(1, 1)
    g_near(0, 0)
    pump(0, 2)
    pump(1, 2)
    g_near(0, 1)
    pump(0, 3)
    pump(1, 3)
    loads[6].wait()
    w_first(2)
    g_far(0)
    pump(0, 4)
    for dx in (0, -1, 1, 2):
        g_partner(0, dx)
    other = 1 - x // 2
    project(other * 2, 1)
    retain(other)
    pump(1, 4)
    partial(0, 2, gated_rows(2), w_out)
    pump(2, 1)
    loads[7].wait()
    w_first(3)
    combine_far(0)
    project((1 - other) * 2, 1)
    retain(1 - other)
    partial(0, 1, gated_rows(1), w_out)
    partial(0, -1, gated_rows(-1), w_out)
    combine_free(0)
    pump(2, 2)
    partial(0, 0, gated_rows(0), w_out)
    combine_near(0)
    pump(2, 3)
    pump(3, 1)
    d_wait(0, 3)
    s_wait(0, 3)
    s_wait(0, 4)
    pump(2, 4)
    s_wait(0, 2)
    s_wait(0, 5)
    for h in (0, 1):
        def second_norm(rows, first):
            value = (rbuf[h, rows, :].astype(F32) + sum_rows(0, h, rows, first)).astype(BF16)
            after[h, rows, :] = value
            xn[1, tp, h, rows, :] = normed(value.astype(F32), mlp_gain[...])

        rows16(second_norm)
        g_first(1, h)

    def lift(dx):
        k = TURN[dx]
        first = turn(x, dx) * 2

        def body(j, carry):
            columns = pl.ds(pl.multiple_of(j * 256, 256), 256)
            lhs = jnp.concatenate(
                [xn[1, first + 1 - c].reshape(128, D), xn[1, first + c].reshape(128, D)], axis=0
            )
            rhs = w_up[:, :, :, :, columns].reshape(D, 256)
            o = jnp.maximum(jnp.dot(lhs, rhs, preferred_element_type=F32), 0.0)
            hid[k, :, columns] = (o * o).astype(BF16)
            return carry

        lax.fori_loop(0, w_up.shape[4] // 256, body, 0)

    def hidden_rows(dx):
        return lambda: hid[TURN[dx]]

    pump(3, 2)
    g_partner(1, 0)
    lift(0)
    g_near(1, 0)
    pump(3, 3)
    g_near(1, 1)
    g_partner(1, -1)
    lift(-1)
    g_partner(1, 1)
    lift(1)
    pump(3, 4)
    partial(1, 0, hidden_rows(0), w_down)
    g_far(1)
    g_partner(1, 2)
    lift(2)
    partial(1, 2, hidden_rows(2), w_down)
    combine_far(1)
    partial(1, 1, hidden_rows(1), w_down)
    partial(1, -1, hidden_rows(-1), w_down)
    combine_free(1)
    combine_near(1)
    d_wait(1, 3)
    s_wait(1, 3)
    s_wait(1, 4)
    s_wait(1, 2)
    s_wait(1, 5)
    for h in (0, 1):
        def last(rows, first):
            total = after[h, rows, :].astype(F32) + sum_rows(1, h, rows, first)
            out[h, rows, :] = total.astype(BF16)

        rows16(last)
    for copy in started:
        copy.wait_send()


def on_device(
    resid, mix_gain, w_query, w_key, w_value, w_gate, w_output, decay_rate, mlp_gain, w_up, w_down
):
    def cut(w):
        return w.reshape(2, 2, w.shape[0] // 4, w.shape[1])

    wide = w_query.shape[1] + w_key.shape[1] + w_value.shape[1] + w_gate.shape[1]
    count = RING * RING

    def held(rows, columns):
        return pltpu.VMEM((count, 2, 2, rows // 4, columns), BF16)

    dma = pltpu.SemaphoreType.DMA
    vmem = pl.BlockSpec(memory_space=pltpu.VMEM)
    hbm = pl.BlockSpec(memory_space=pl.ANY)
    tokens = (2, 64, D)
    number = len(MESSAGES)
    result = pl.pallas_call(
        kernel,
        out_shape=jax.ShapeDtypeStruct(tokens, BF16),
        in_specs=[
            hbm, vmem, hbm, hbm, hbm, hbm, hbm,
            pl.BlockSpec(memory_space=pltpu.SMEM), vmem, hbm, hbm,
        ],
        out_specs=vmem,
        scratch_shapes=[
            held(128, wide),
            held(w_output.shape[0], 128),
            held(128, w_up.shape[1]),
            held(w_down.shape[0], 128),
            pltpu.VMEM((2, 8) + tokens, BF16),
            pltpu.VMEM(tokens, BF16),
            pltpu.VMEM(tokens, BF16),
            pltpu.VMEM((8, 128, wide), BF16),
            pltpu.VMEM((8, 128, DV), BF16),
            pltpu.VMEM((4, 256, w_up.shape[1]), BF16),
            pltpu.VMEM((LENGTH, LENGTH), F32),
            pltpu.VMEM((4, 128, D), F32),
            pltpu.VMEM((2, 4) + tokens, BF16),
            pltpu.VMEM((2, 4) + tokens, BF16),
            pltpu.VMEM((2, 3) + tokens, BF16),
            pltpu.VMEM((2, 2, 64, D), BF16),
            pltpu.VMEM((2, 2) + tokens, BF16),
            dma((8,)),
            dma((4, number)),
            dma((4, number)),
            dma((2, len(GATHER))),
            dma((2, len(GATHER))),
            dma((2, 4)),
            dma((2, 4)),
            dma((2, 6)),
            dma((2, 6)),
        ],
        compiler_params=pltpu.CompilerParams(
            collective_id=0, has_side_effects=True, vmem_limit_bytes=63 * 1024 * 1024
        ),
    )(
        resid.reshape(tokens), mix_gain[None], cut(w_query), cut(w_key), cut(w_value), cut(w_gate),
        cut(w_output), decay_rate, mlp_gain[None], cut(w_up), cut(w_down),
    )
    return result.reshape(resid.shape)


def solution(mesh):
    placed = (
        P(("fs", "tp"), None),
        P(),
        P("fs", "tp"),
        P("fs", "tp"),
        P("fs", "tp"),
        P("fs", "tp"),
        P("tp", "fs"),
        P("tp"),
        P(),
        P("fs", "tp"),
        P("tp", "fs"),
    )
    return jax.shard_map(
        on_device, mesh=mesh, in_specs=placed, out_specs=P(("fs", "tp"), None), check_vma=False
    )
```

time: 308 us -> 120 us (0.39)
  waiting for transfers between devices: 182 us -> 0 us
  Pallas kernels: 0 us -> 117 us
  blocking collectives: 52.5 us -> 0 us
  matrix products: 35.5 us -> 0 us
  between operations: 14.3 us -> 0.66 us
  other arithmetic: 9.99 us -> 0 us
  starting transfers between devices: 9.02 us -> 0 us
    all_gather x5 -> x0, waiting for transfers between devices: 146 us -> none  [the longest x1 44.8 us: side_by_side(): whole = lax.all_gather(both, axis, axis=dim, tiled=True)]
    pallas_call x0 -> x1, Pallas kernels: none -> 117 us  [on_device(): pl.pallas_call(kernel, out_shape=jax.ShapeDtypeStruct(tokens, BF16), in_s...]
    all_to_all x1 -> x0, blocking collectives: 52.5 us -> none  [sent_and_summed(): lax.all_to_all(cut_along(value, dim, devices), axis, 0, 0, tiled=True)]
    dot_general x8 -> x0, matrix products: 35.5 us -> none  [the longest x1 14.4 us: on_device(): jnp.dot(hidden, down_whole, preferred_element_type=jnp.float32)]
    reduce_scatter x1 -> x0, waiting for transfers between devices: 34.7 us -> none  [on_device(): lax.psum_scatter(jnp.dot(hidden, down_whole, preferred_element_type=jnp.f...]
    all_to_all x1 -> x0, starting transfers between devices: 8.64 us -> none  [from_everyone(): lax.all_to_all(jnp.broadcast_to(value[None], (devices, *value.shape)), ax...]
    convert_element_type x3 -> x0, other arithmetic: 4.98 us -> none  [the longest x2 3.01 us: rms_scale(): return (scaled * gains).astype(jnp.bfloat16)]
  transfers between devices with their start and end apart: 7 -> 0, of which waited for: 5 -> 0; matrix products, arithmetic and copies ran while one was open for 10% -> 0% of each run, Pallas kernels for 0% -> 0%
where the time goes in v1:
time: 120 us
  Pallas kernels  117 us (98%)
  local copies, waits for them, and re-layouts  1.88 us (2%)
    pallas_call x1, Pallas kernels, on_device(): pl.pallas_call(kernel, out_shape=jax.ShapeDtypeStruct(tokens, BF16), in_s...  117 us

profile of v1, /device:TPU:1, one launch (start us, length us, event | category | flops | bytes accessed | tf_op | source)
XLA Modules:
  0.0 119.8 jit_solution(16035282506474039940)
XLA Ops:
  0.7 117.3 %shard_map.109 = bf16[2,64,2048]{2,1,0:T(8,128)(2,1)} custom-call(bf16[2,64,2048]{2,1,0:T(8,128)(2,1)} %bitcast.12, f32[1,2048]{1,0:T(1,128)} %bitcast.20, bf16[2,2,32,128]{3,2,1,0:T(8,128)(2,1)} %bitcast.18, bf16[2,2,32,128]{3,2,1,0:T(8,128)(2,1)} %bitcast.19, bf16[2,2,32,256]{3,2,1,0:T(8,128)(2,1)} %bitcast.15, bf16[2,2,32,256]{3,2,1,0:T(8,128)(2,1)} %bitcast.16, ...), custom_call_target="tpu_custom_call" | custom-call | tf_op jit(solution)/shard_map/pallas_call | solution.py:462
  117.9 1.9 %copy.14 = bf16[128,2048]{1,0:T(8,128)(2,1)} copy(bf16[128,2048]{1,0:T(8,128)(2,1)} %bitcast.11) | data formatting | bytes 1048576

commit v2 on v1

v2 whole, which is shorter than its diff:
```python
import jax
import jax.numpy as jnp
from jax import lax
from jax.experimental import pallas as pl
from jax.experimental.pallas import tpu as pltpu
from jax.sharding import PartitionSpec as P

D = 2048
DK = 128
DV = 256
LENGTH = 512
RING = 4
EPS = 1e-06
MESH = pl.DeviceIdType.MESH
F32 = jnp.float32
BF16 = jnp.bfloat16

STEP = {"y+": (1, 0), "y-": (-1, 0), "z+": (0, 1), "z-": (0, -1)}


def near(d):
    return {0: 0, 1: 1, 2: 2, 3: -1}[d % RING]


def arrived(message):
    dy, dz, part, way = message
    return near(dy - STEP[way][0]), near(dz - STEP[way][1]), part, way


def onward(message):
    dy, dz, part, way = arrived(message)
    half = "0" if way[1] == "+" else "1"
    across = ("z+", "z-") if way[0] == "y" else ("y+", "y-")
    first = "A" if way[0] == "y" else "B"
    if part == "full":
        return [(dy, dz, "h" + half, way)] + [(dy, dz, first, w) for w in across]
    if part in ("h0", "h1"):
        return [(dy, dz, first + part, w) for w in across]
    if part in ("A", "B"):
        return [(dy, dz, part + "h" + half, way)]
    far = dy if part[0] == "A" else dz
    last = dz if part[0] == "A" else dy
    if far == 2 and last != 2 and part[-1] == half:
        return [(dy, dz, part, way)]
    return []


def plan():
    rounds = [[(0, 0, "full", w) for w in ("y+", "y-", "z+", "z-")]]
    while rounds[-1]:
        rounds.append([m for sent in rounds[-1] for m in onward(sent)])
    return rounds[:-1]


ROUNDS = plan()
MESSAGES = [m for sent in ROUNDS for m in sent]
NUMBER = {m: i for i, m in enumerate(MESSAGES)}

GATHER = (
    [(0, h, q, w) for h in (0, 1) for q in (0, 1) for w in ("x+", "x-")]
    + [(0, h, None, "d") for h in (0, 1)]
    + [(dx, h, q, "d") for dx in (-1, 1, 2) for h in (0, 1) for q in (0, 1)]
    + [(-1, h, 0, "x+") for h in (0, 1)]
    + [(1, h, 1, "x-") for h in (0, 1)]
)
GATHER_NUMBER = {m: i for i, m in enumerate(GATHER)}
TURN = {2: 0, 1: 1, -1: 2, 0: 3}


def kernel(
    resid, mix_gain, wq, wk, wv, wg, wo, rate, mlp_gain, wu, wd,
    out,
    w_in, w_out, w_up, w_down, xn, rbuf, after, proj, gated, hid, decay, kept,
    dout, din, sout, rin2, rin1,
    local_sem, w_send, w_recv, g_send, g_recv, d_send, d_recv, s_send, s_recv,
):
    fs, tp = lax.axis_index("fs"), lax.axis_index("tp")
    z, y, x, c = fs // RING, fs % RING, tp // 2, tp % 2

    def turn(v, d):
        return (v + d + RING) % RING

    device = {
        "y+": (z * RING + turn(y, 1), tp),
        "y-": (z * RING + turn(y, -1), tp),
        "z+": (turn(z, 1) * RING + y, tp),
        "z-": (turn(z, -1) * RING + y, tp),
        "x+": (fs, turn(x, 1) * 2 + c),
        "x-": (fs, turn(x, -1) * 2 + c),
        "d": (fs, x * 2 + 1 - c),
    }

    def remote(src, dst, send, recv, way):
        return pltpu.make_async_remote_copy(
            src_ref=src, dst_ref=dst, send_sem=send, recv_sem=recv,
            device_id=device[way], device_id_type=MESH,
        )

    def send(*args):
        remote(*args).start()

    weights = (w_in, w_out, w_up, w_down)

    def piece(t, dy, dz, part):
        ref = weights[t]
        f = turn(z, dz) * RING + turn(y, dy)
        if part == "full":
            return ref.at[f]
        if part in ("A", "B"):
            return ref.at[f, :, "AB".index(part)]
        if part in ("h0", "h1"):
            return ref.at[f, int(part[1])]
        return ref.at[f, int(part[2]), "AB".index(part[0])]

    def w_copy(t, message, place):
        dy, dz, part, way = place
        ref = piece(t, dy, dz, part)
        return (ref, ref, w_send.at[t], w_recv.at[t, NUMBER[message]], way)

    def w_first(t):
        for message in ROUNDS[0]:
            send(*w_copy(t, message, message))

    def pump(t, r):
        for message in ROUNDS[r - 1]:
            remote(*w_copy(t, message, arrived(message))).wait_recv()
            for following in onward(message):
                send(*w_copy(t, following, following))

    def g_copy(g, message, dx, core):
        h, q, way = message[1:]
        block = turn(x, dx) * 2 + core
        ref = xn.at[g, block, h] if q is None else xn.at[g, block, h, q]
        return (ref, ref, g_send.at[g], g_recv.at[g, GATHER_NUMBER[message]], way)

    def g_send_one(g, message):
        send(*g_copy(g, message, message[0], c))

    def g_wait(g, message):
        dx, h, q, way = message
        if way == "d":
            copy = g_copy(g, message, dx, 1 - c)
        else:
            copy = g_copy(g, message, near(dx - (1 if way == "x+" else -1)), c)
        remote(*copy).wait_recv()

    def g_first(g, h):
        g_send_one(g, (0, h, 0, "x+"))
        g_send_one(g, (0, h, 1, "x-"))
        g_send_one(g, (0, h, None, "d"))

    def g_second(g, h):
        g_send_one(g, (0, h, 1, "x+"))
        g_send_one(g, (0, h, 0, "x-"))

    def g_near(g, h):
        g_wait(g, (0, h, 0, "x+"))
        g_send_one(g, (-1, h, 0, "x+"))
        g_send_one(g, (-1, h, 0, "d"))
        g_wait(g, (0, h, 1, "x-"))
        g_send_one(g, (1, h, 1, "x-"))
        g_send_one(g, (1, h, 1, "d"))

    def g_rest(g, h):
        g_wait(g, (0, h, 1, "x+"))
        g_send_one(g, (-1, h, 1, "d"))
        g_wait(g, (0, h, 0, "x-"))
        g_send_one(g, (1, h, 0, "d"))

    def g_far(g, h):
        g_wait(g, (-1, h, 0, "x+"))
        g_send_one(g, (2, h, 0, "d"))
        g_wait(g, (1, h, 1, "x-"))
        g_send_one(g, (2, h, 1, "d"))

    def g_partner(g, h, dx):
        for q in (None,) if dx == 0 else (0, 1):
            g_wait(g, (dx, h, q, "d"))

    def rows16(count, body):
        def step(i, carry):
            body(pl.ds(pl.multiple_of(i * 16, 16), 16))
            return carry

        lax.fori_loop(0, count // 16, step, 0)

    def d_copy(g, k, h):
        return (dout.at[g, k, h], din.at[g, k, h], d_send.at[g], d_recv.at[g, k, h], "d")

    def s_copy(g, h, n):
        if n < 2:
            src, dst, way = sout.at[g, 0, h, n], rin2.at[g, h, n], ("x+", "x-")[n]
        elif n < 4:
            src, dst, way = sout.at[g, 1, h, n - 2], rin1.at[g, 0, h, n - 2], "x+"
        else:
            src, dst, way = sout.at[g, 2, h, n - 4], rin1.at[g, 1, h, n - 4], "x-"
        return (src, dst, s_send.at[g], s_recv.at[g, h, n], way)

    def partial(g, cases, lhs, weight):
        depth = weight.shape[1] * weight.shape[2] * weight.shape[3]

        def step(j, carry):
            w = jnp.concatenate([weight[4 * j + i].reshape(depth, 128) for i in range(4)], axis=1)
            rows = jnp.concatenate([block for case in cases for block in lhs(*case)], axis=0)
            o = jnp.dot(rows, w, preferred_element_type=F32)
            columns = pl.ds(pl.multiple_of(j * 512, 512), 512)
            for n, (dx, h) in enumerate(cases):
                mine = o[n * 128 : (n + 1) * 128]
                dout[g, TURN[dx], h, :, :, columns] = mine[:64].astype(BF16).reshape(2, 32, 512)
                kept[TURN[dx], h, :, :, columns] = mine[64:].reshape(2, 32, 512)
            return carry

        lax.fori_loop(0, 4, step, 0)
        for dx, h in cases:
            send(*d_copy(g, TURN[dx], h))

    def add_quarter(g, k, h, q, extra=False):
        def body(rows):
            total = kept[k, h, q, rows, :] + din[g, k, h, q, rows, :].astype(F32)
            if extra:
                total = total + rin2[g, h, q, rows, :].astype(F32)
            sout[g, k, h, q, rows, :] = total.astype(BF16)

        rows16(32, body)

    def d_wait(g, k, h):
        remote(*d_copy(g, k, h)).wait_recv()

    def s_wait(g, h, n):
        remote(*s_copy(g, h, n)).wait_recv()

    def combine_far(g, h):
        d_wait(g, 0, h)
        for q in (0, 1):
            add_quarter(g, 0, h, q)
            send(*s_copy(g, h, q))

    def combine_free(g, h):
        d_wait(g, 1, h)
        add_quarter(g, 1, h, 1)
        send(*s_copy(g, h, 3))
        d_wait(g, 2, h)
        add_quarter(g, 2, h, 0)
        send(*s_copy(g, h, 4))

    def combine_near(g, h):
        s_wait(g, h, 0)
        add_quarter(g, 1, h, 0, True)
        send(*s_copy(g, h, 2))
        s_wait(g, h, 1)
        add_quarter(g, 2, h, 1, True)
        send(*s_copy(g, h, 5))

    def combine_own(g, h):
        d_wait(g, 3, h)
        for n in (3, 4, 2, 5):
            s_wait(g, h, n)

    def sum_rows(g, h, q, rows):
        total = kept[3, h, q, rows, :] + din[g, 3, h, q, rows, :].astype(F32)
        return total + rin1[g, 0, h, q, rows, :].astype(F32) + rin1[g, 1, h, q, rows, :].astype(F32)

    def normed(values, gain):
        scale = lax.rsqrt(jnp.mean(values * values, axis=-1, keepdims=True) + EPS)
        return (values * scale * gain).astype(BF16)

    loads = []

    def load(src, dst):
        copy = pltpu.make_async_copy(src, dst, local_sem.at[len(loads)])
        copy.start()
        loads.append(copy)

    for src, low, wide in ((wq, 0, 128), (wk, 128, 128), (wv, 256, 256), (wg, 512, 256)):
        load(src, w_in.at[fs, :, :, :, low : low + wide])
    load(resid, rbuf)
    load(wo, w_out.at[fs])
    load(wu, w_up.at[fs])
    load(wd, w_down.at[fs])
    barrier = pltpu.get_barrier_semaphore()
    for way in device:
        pl.semaphore_signal(barrier, inc=1, device_id=device[way], device_id_type=MESH)
    for copy in loads[:5]:
        copy.wait()
    for h in (0, 1):
        for q in (0, 1):
            def first_norm(rows):
                xn[0, tp, h, q, rows, :] = normed(rbuf[h, q, rows, :].astype(F32), mix_gain[...])

            rows16(32, first_norm)
    pl.semaphore_wait(barrier, 7)
    w_first(0)
    g_first(0, 0)
    g_second(0, 0)
    g_first(0, 1)
    g_second(0, 1)
    loads[5].wait()
    w_first(1)

    r = rate[0]

    def decay_rows(i, carry):
        rows = pl.ds(pl.multiple_of(i * 64, 64), 64)
        t = lax.broadcasted_iota(jnp.int32, (64, LENGTH), 0) + i * 64
        s = lax.broadcasted_iota(jnp.int32, (64, LENGTH), 1)
        gap = (t - s).astype(F32)
        value = jnp.exp(-r * jnp.maximum(gap, 0.0)) * DK ** (-0.5)
        decay[rows, :] = jnp.where(gap >= 0.0, value, 0.0)
        return carry

    lax.fori_loop(0, LENGTH // 64, decay_rows, 0)

    def project(seq):
        def body(j, carry):
            columns = pl.ds(pl.multiple_of(j * 256, 256), 256)
            lhs = xn[0, pl.ds(4 * seq, 4)].reshape(512, D)
            rhs = w_in[:, :, :, :, columns].reshape(D, 256)
            o = jnp.dot(lhs, rhs, preferred_element_type=F32).astype(BF16)
            proj[pl.ds(4 * seq, 4), :, columns] = o.reshape(4, 128, 256)
            return carry

        lax.fori_loop(0, 3, body, 0)

    def retain(seq):
        for i in (0, 1):
            mine = pl.ds(seq * 4 + 2 * i, 2)
            upto = pl.ds(seq * 4, 2 * i + 2)
            wide = 256 * (i + 1)
            q = proj[mine, :, 0:128].reshape(256, DK)
            k = proj[upto, :, 128:256].reshape(wide, DK)
            v = proj[upto, :, 256:512].reshape(wide, DV)
            scores = lax.dot_general(q, k, (((1,), (1,)), ((), ())), preferred_element_type=F32)
            scores = (scores * decay[i * 256 : (i + 1) * 256, 0:wide]).astype(BF16)
            mixed = jnp.dot(scores, v, preferred_element_type=F32)
            mixed = mixed - jnp.mean(mixed, axis=-1, keepdims=True)
            spread = jnp.mean(mixed * mixed, axis=-1, keepdims=True)
            gate = proj[mine, :, 512:768].reshape(256, DV).astype(F32)
            value = gate / (1.0 + jnp.exp(-gate)) * (mixed * lax.rsqrt(spread + EPS))
            gated[mine] = value.astype(BF16).reshape(2, 2, 64, DV)

    def gated_rows(dx, h):
        first = turn(x, dx) * 2
        return gated[first + 1 - c, h], gated[first + c, h]

    def lift(cases):
        def body(j, carry):
            columns = pl.ds(pl.multiple_of(j * 256, 256), 256)
            lhs = jnp.concatenate(
                [
                    xn[1, turn(x, dx) * 2 + core, h].reshape(64, D)
                    for dx, h in cases
                    for core in (1 - c, c)
                ],
                axis=0,
            )
            rhs = w_up[:, :, :, :, columns].reshape(D, 256)
            o = jnp.maximum(jnp.dot(lhs, rhs, preferred_element_type=F32), 0.0)
            o = (o * o).astype(BF16)
            for n, (dx, h) in enumerate(cases):
                hid[TURN[dx], h, :, columns] = o[n * 128 : (n + 1) * 128]
            return carry

        lax.fori_loop(0, w_up.shape[4] // 256, body, 0)

    def hidden_rows(dx, h):
        return (hid[TURN[dx], h],)

    pump(0, 1)
    g_near(0, 0)
    g_rest(0, 0)
    pump(0, 2)
    g_near(0, 1)
    g_rest(0, 1)
    pump(0, 3)
    pump(1, 1)
    loads[6].wait()
    w_first(2)
    g_far(0, 0)
    pump(0, 4)
    g_far(0, 1)
    for h in (0, 1):
        for dx in (0, -1, 1, 2):
            g_partner(0, h, dx)
    other = 1 - x // 2
    project(other)
    pump(1, 2)
    retain(other)
    pump(1, 3)
    pump(2, 1)
    loads[7].wait()
    w_first(3)
    pump(1, 4)
    partial(0, ((2, 0), (2, 1)), gated_rows, w_out)
    combine_far(0, 0)
    combine_far(0, 1)
    project(1 - other)
    retain(1 - other)
    partial(0, ((1, 0), (-1, 0)), gated_rows, w_out)
    partial(0, ((1, 1), (-1, 1)), gated_rows, w_out)
    combine_free(0, 0)
    combine_near(0, 0)
    combine_free(0, 1)
    combine_near(0, 1)
    pump(2, 2)
    partial(0, ((0, 0), (0, 1)), gated_rows, w_out)
    pump(3, 1)

    def second_norm(h):
        for q in (0, 1):
            def body(rows):
                value = rbuf[h, q, rows, :].astype(F32) + sum_rows(0, h, q, rows)
                value = value.astype(BF16)
                after[h, q, rows, :] = value
                xn[1, tp, h, q, rows, :] = normed(value.astype(F32), mlp_gain[...])

            rows16(32, body)

    combine_own(0, 0)
    second_norm(0)
    g_first(1, 0)
    g_second(1, 0)
    pump(2, 3)
    combine_own(0, 1)
    second_norm(1)
    g_first(1, 1)
    g_near(1, 0)
    g_second(1, 1)
    g_rest(1, 0)
    pump(2, 4)
    pump(3, 2)

    g_partner(1, 0, 0)
    g_partner(1, 0, -1)
    g_partner(1, 0, 1)
    lift(((0, 0), (-1, 0), (1, 0)))
    g_near(1, 1)
    g_far(1, 0)
    g_partner(1, 0, 2)
    lift(((2, 0),))
    pump(3, 3)
    g_rest(1, 1)
    g_far(1, 1)
    pump(3, 4)
    partial(1, ((2, 0),), hidden_rows, w_down)
    combine_far(1, 0)
    partial(1, ((1, 0), (-1, 0)), hidden_rows, w_down)
    combine_free(1, 0)
    g_partner(1, 1, 2)
    lift(((2, 1),))
    partial(1, ((2, 1),), hidden_rows, w_down)
    combine_near(1, 0)
    combine_far(1, 1)
    g_partner(1, 1, 0)
    g_partner(1, 1, -1)
    g_partner(1, 1, 1)
    lift(((0, 1), (-1, 1), (1, 1)))
    partial(1, ((1, 1), (-1, 1)), hidden_rows, w_down)
    combine_free(1, 1)
    combine_near(1, 1)
    partial(1, ((0, 0), (0, 1)), hidden_rows, w_down)

    def finish(h):
        for q in (0, 1):
            def body(rows):
                total = after[h, q, rows, :].astype(F32) + sum_rows(1, h, q, rows)
                out[h, q, rows, :] = total.astype(BF16)

            rows16(32, body)

    combine_own(1, 0)
    finish(0)
    combine_own(1, 1)
    finish(1)
    for t in range(4):
        ref = weights[t].at[0:15]
        remote(ref, ref, w_send.at[t], w_recv.at[t, 0], "d").wait_send()
    for g in (0, 1):
        remote(xn.at[g, 0:7], xn.at[g, 0:7], g_send.at[g], g_recv.at[g, 0], "d").wait_send()
        remote(dout.at[g], din.at[g], d_send.at[g], d_recv.at[g, 0, 0], "d").wait_send()
        remote(sout.at[g], sout.at[g], s_send.at[g], s_recv.at[g, 0, 0], "d").wait_send()


def on_device(
    resid, mix_gain, w_query, w_key, w_value, w_gate, w_output, decay_rate, mlp_gain, w_up, w_down
):
    def cut(w):
        return w.reshape(2, 2, w.shape[0] // 4, w.shape[1])

    wide = w_query.shape[1] + w_key.shape[1] + w_value.shape[1] + w_gate.shape[1]
    count = RING * RING

    def held(rows, columns):
        return pltpu.VMEM((count, 2, 2, rows // 4, columns), BF16)

    dma = pltpu.SemaphoreType.DMA
    vmem = pl.BlockSpec(memory_space=pltpu.VMEM)
    hbm = pl.BlockSpec(memory_space=pl.ANY)
    tokens = (2, 2, 32, D)
    number = len(MESSAGES)
    result = pl.pallas_call(
        kernel,
        out_shape=jax.ShapeDtypeStruct(tokens, BF16),
        in_specs=[
            hbm, vmem, hbm, hbm, hbm, hbm, hbm,
            pl.BlockSpec(memory_space=pltpu.SMEM), vmem, hbm, hbm,
        ],
        out_specs=vmem,
        scratch_shapes=[
            held(128, wide),
            held(w_output.shape[0], 128),
            held(128, w_up.shape[1]),
            held(w_down.shape[0], 128),
            pltpu.VMEM((2, 8) + tokens, BF16),
            pltpu.VMEM(tokens, BF16),
            pltpu.VMEM(tokens, BF16),
            pltpu.VMEM((8, 128, wide), BF16),
            pltpu.VMEM((8, 2, 64, DV), BF16),
            pltpu.VMEM((4, 2, 128, w_up.shape[1]), BF16),
            pltpu.VMEM((LENGTH, LENGTH), F32),
            pltpu.VMEM((4,) + tokens, F32),
            pltpu.VMEM((2, 4) + tokens, BF16),
            pltpu.VMEM((2, 4) + tokens, BF16),
            pltpu.VMEM((2, 3) + tokens, BF16),
            pltpu.VMEM((2,) + tokens, BF16),
            pltpu.VMEM((2, 2) + tokens, BF16),
            dma((8,)),
            dma((4,)),
            dma((4, number)),
            dma((2,)),
            dma((2, len(GATHER))),
            dma((2,)),
            dma((2, 4, 2)),
            dma((2,)),
            dma((2, 2, 6)),
        ],
        compiler_params=pltpu.CompilerParams(
            collective_id=0, has_side_effects=True, vmem_limit_bytes=63 * 1024 * 1024
        ),
    )(
        resid.reshape(tokens), mix_gain[None], cut(w_query), cut(w_key), cut(w_value), cut(w_gate),
        cut(w_output), decay_rate, mlp_gain[None], cut(w_up), cut(w_down),
    )
    return result.reshape(resid.shape)


def solution(mesh):
    placed = (
        P(("fs", "tp"), None),
        P(),
        P("fs", "tp"),
        P("fs", "tp"),
        P("fs", "tp"),
        P("fs", "tp"),
        P("tp", "fs"),
        P("tp"),
        P(),
        P("fs", "tp"),
        P("tp", "fs"),
    )
    return jax.shard_map(
        on_device, mesh=mesh, in_specs=placed, out_specs=P(("fs", "tp"), None), check_vma=False
    )
```

time: 120 us -> 113 us (0.942)
  Pallas kernels: 117 us -> 110 us
    pallas_call x1, Pallas kernels: 117 us -> 110 us  [on_device(): pl.pallas_call(kernel, out_shape=jax.ShapeDtypeStruct(tokens, BF16), in_s...]
where the time goes in v2:
time: 113 us; the launch traced here: 112 us
  Pallas kernels  110 us (97%)
  local copies, waits for them, and re-layouts  1.88 us (2%)
    pallas_call x1, Pallas kernels, on_device(): pl.pallas_call(kernel, out_shape=jax.ShapeDtypeStruct(tokens, BF16), in_s...  110 us

profile of v2, /device:TPU:1, one launch (start us, length us, event | category | flops | bytes accessed | tf_op | source)
XLA Modules:
  0.0 112.2 jit_solution(6637186696256638725)
XLA Ops:
  0.7 109.6 %shard_map.109 = bf16[2,2,32,2048]{3,2,1,0:T(8,128)(2,1)} custom-call(bf16[2,2,32,2048]{3,2,1,0:T(8,128)(2,1)} %bitcast.12, f32[1,2048]{1,0:T(1,128)} %bitcast.20, bf16[2,2,32,128]{3,2,1,0:T(8,128)(2,1)} %bitcast.18, bf16[2,2,32,128]{3,2,1,0:T(8,128)(2,1)} %bitcast.19, bf16[2,2,32,256]{3,2,1,0:T(8,128)(2,1)} %bitcast.15, bf16[2,2,32,256]{3,2,1,0:T(8,128)(2,1)} %bitcast.16, ...), custom_call_target="tpu_custom_call" | custom-call | tf_op jit(solution)/shard_map/pallas_call | solution.py:500
  110.3 1.9 %copy.14 = bf16[128,2048]{1,0:T(8,128)(2,1)} copy(bf16[128,2048]{1,0:T(8,128)(2,1)} %bitcast.11) | data formatting | bytes 1048576

commit v3 on v2

v3 whole, which is shorter than its diff:
```python
import jax
import jax.numpy as jnp
from jax import lax
from jax.experimental import pallas as pl
from jax.experimental.pallas import tpu as pltpu
from jax.sharding import PartitionSpec as P

D = 2048
DK = 128
DV = 256
LENGTH = 512
RING = 4
EPS = 1e-06
MESH = pl.DeviceIdType.MESH
F32 = jnp.float32
BF16 = jnp.bfloat16

STEP = {"y+": (1, 0), "y-": (-1, 0), "z+": (0, 1), "z-": (0, -1)}


def near(d):
    return {0: 0, 1: 1, 2: 2, 3: -1}[d % RING]


def arrived(message):
    dy, dz, part, way = message
    return near(dy - STEP[way][0]), near(dz - STEP[way][1]), part, way


def onward(message):
    dy, dz, part, way = arrived(message)
    half = "0" if way[1] == "+" else "1"
    along = way[0] == "y"
    across = ("z+", "z-") if along else ("y+", "y-")
    first = "A" if along else "B"
    if part == "full":
        return [(dy, dz, "h" + half, way)] + [(dy, dz, first, w) for w in across]
    if part in ("h0", "h1"):
        onto = [(dy, dz, part, way)] if (dy if along else dz) != 2 and part[1] == half else []
        return onto + [(dy, dz, first + part, w) for w in across]
    if part in ("A", "B"):
        return [(dy, dz, part + "h" + half, way)]
    if (dy if way[0] == "y" else dz) != 2 and part[-1] == half:
        return [(dy, dz, part, way)]
    return []


def plan(parts):
    messages = [(0, 0, part, way) for part in parts for way in ("y+", "y-", "z+", "z-")]
    for message in messages:
        messages += onward(message)
    return messages


MESSAGES = [plan(parts) for parts in (("h0", "h1"), ("full",), ("full",), ("h0", "h1"))]
PLACES = (
    (0, 0), (1, 0), (-1, 0), (0, 1), (0, -1), (2, 0), (0, 2), (1, 1),
    (1, -1), (-1, 1), (-1, -1), (2, 1), (2, -1), (1, 2), (-1, 2), (2, 2),
)

GATHER = (
    [(0, h, q, w) for h in (0, 1) for q in (0, 1) for w in ("x+", "x-")]
    + [(0, h, None, "d") for h in (0, 1)]
    + [(dx, h, q, "d") for dx in (-1, 1, 2) for h in (0, 1) for q in (0, 1)]
    + [(-1, h, 0, "x+") for h in (0, 1)]
    + [(1, h, 1, "x-") for h in (0, 1)]
)
TURN = {2: 0, 1: 1, -1: 2, 0: 3}

SCHEDULE = (
    ("s", "w", 0, 0), ("s", "w", 0, 5), ("s", "w", 0, 2), ("s", "w", 0, 7), ("s", "g", 0, 0), ("s", "g", 0, 3), ("s", "g", 0, 8),
    ("s", "g", 0, 9), ("decay",), ("r", "g", 0, 8), ("s", "w", 1, 0), ("s", "w", 1, 1), ("s", "w", 1, 2), ("s", "w", 1, 3),
    ("r", "g", 0, 9), ("s", "g", 0, 2), ("s", "g", 0, 1), ("s", "w", 0, 4), ("s", "w", 0, 1), ("s", "w", 0, 6), ("s", "w", 0, 3),
    ("r", "w", 0, 0), ("r", "w", 0, 5), ("r", "w", 0, 2), ("r", "w", 0, 7), ("r", "g", 0, 0), ("s", "g", 0, 10), ("r", "g", 0, 3),
    ("s", "g", 0, 15), ("s", "w", 0, 8), ("s", "w", 0, 20), ("s", "w", 0, 13), ("s", "w", 0, 25), ("s", "g", 0, 22), ("s", "g", 0, 24),
    ("r", "w", 1, 0), ("r", "w", 1, 1), ("r", "w", 1, 2), ("r", "w", 1, 3), ("r", "g", 0, 10), ("r", "g", 0, 15), ("s", "w", 1, 4),
    ("s", "w", 1, 7), ("s", "w", 1, 10), ("s", "w", 1, 13), ("r", "g", 0, 2), ("s", "g", 0, 11), ("r", "g", 0, 1), ("s", "g", 0, 14),
    ("r", "w", 0, 4), ("r", "w", 0, 1), ("r", "w", 0, 6), ("r", "w", 0, 3), ("s", "w", 0, 14), ("s", "w", 0, 27), ("s", "w", 0, 9),
    ("s", "w", 0, 22), ("s", "g", 0, 4), ("s", "g", 0, 7), ("r", "g", 0, 11), ("s", "w", 1, 11), ("s", "w", 1, 12), ("s", "w", 1, 5),
    ("s", "w", 1, 6), ("r", "g", 0, 14), ("r", "w", 0, 8), ("r", "w", 0, 20), ("r", "w", 0, 13), ("r", "w", 0, 25), ("s", "w", 1, 14),
    ("s", "w", 1, 15), ("s", "w", 1, 8), ("s", "w", 1, 9), ("r", "g", 0, 22), ("s", "g", 0, 18), ("r", "g", 0, 24), ("s", "g", 0, 19),
    ("r", "w", 1, 4), ("r", "w", 1, 7), ("r", "w", 1, 10), ("r", "w", 1, 13), ("s", "w", 0, 16), ("s", "w", 0, 24), ("s", "w", 0, 11),
    ("s", "w", 0, 19), ("s", "g", 0, 6), ("s", "g", 0, 5), ("r", "w", 0, 14), ("r", "w", 0, 27), ("r", "w", 0, 9), ("r", "w", 0, 22),
    ("s", "w", 0, 32), ("s", "w", 0, 42), ("s", "w", 0, 28), ("s", "w", 0, 38), ("r", "g", 0, 18), ("r", "g", 0, 19), ("r", "w", 1, 11),
    ("r", "w", 1, 12), ("r", "w", 1, 5), ("r", "w", 1, 6), ("s", "w", 1, 24), ("s", "w", 1, 29), ("s", "w", 1, 16), ("s", "w", 1, 21),
    ("r", "w", 1, 14), ("r", "w", 1, 15), ("r", "w", 1, 8), ("r", "w", 1, 9), ("s", "w", 0, 26), ("s", "w", 0, 15), ("s", "w", 0, 21),
    ("s", "w", 0, 10), ("r", "g", 0, 4), ("s", "g", 0, 12), ("r", "g", 0, 7), ("s", "g", 0, 17), ("s", "g", 0, 23), ("s", "g", 0, 25),
    ("r", "w", 0, 16), ("r", "w", 0, 24), ("r", "w", 0, 11), ("r", "w", 0, 19), ("s", "w", 0, 23), ("s", "w", 0, 17), ("s", "w", 0, 18),
    ("s", "w", 0, 12), ("r", "g", 0, 12), ("r", "g", 0, 17), ("r", "w", 0, 32), ("r", "w", 0, 42), ("r", "w", 0, 28), ("r", "w", 0, 38),
    ("s", "w", 0, 41), ("s", "w", 0, 33), ("s", "w", 0, 37), ("s", "w", 0, 29), ("r", "w", 1, 24), ("r", "w", 1, 29), ("r", "w", 1, 16),
    ("r", "w", 1, 21), ("r", "g", 0, 6), ("s", "g", 0, 13), ("r", "g", 0, 5), ("s", "g", 0, 16), ("s", "w", 1, 28), ("s", "w", 1, 25),
    ("s", "w", 1, 20), ("s", "w", 1, 17), ("r", "w", 0, 26), ("r", "w", 0, 15), ("r", "w", 0, 21), ("r", "w", 0, 10), ("s", "w", 0, 34),
    ("s", "w", 0, 43), ("s", "w", 0, 30), ("s", "w", 0, 39), ("r", "g", 0, 13), ("r", "w", 0, 23), ("r", "w", 0, 17), ("r", "w", 0, 18),
    ("r", "w", 0, 12), ("s", "w", 1, 26), ("s", "w", 1, 27), ("s", "w", 1, 18), ("s", "w", 1, 19), ("r", "g", 0, 16), ("s", "w", 1, 30),
    ("s", "w", 1, 31), ("s", "w", 1, 22), ("s", "w", 1, 23), ("s", "w", 0, 35), ("s", "w", 0, 40), ("s", "w", 0, 31), ("s", "w", 0, 36),
    ("r", "w", 0, 41), ("r", "w", 0, 33), ("r", "w", 0, 37), ("r", "w", 0, 29), ("r", "g", 0, 23), ("s", "g", 0, 20), ("r", "g", 0, 25),
    ("s", "g", 0, 21), ("r", "w", 1, 28), ("r", "w", 1, 25), ("r", "w", 1, 20), ("r", "w", 1, 17), ("s", "w", 0, 45), ("s", "w", 0, 47),
    ("s", "w", 0, 44), ("s", "w", 0, 46), ("r", "w", 0, 34), ("r", "w", 0, 43), ("r", "w", 0, 30), ("r", "w", 0, 39), ("r", "g", 0, 20),
    ("r", "w", 1, 26), ("r", "w", 1, 27), ("r", "w", 1, 18), ("r", "w", 1, 19), ("s", "w", 1, 34), ("s", "w", 1, 35), ("s", "w", 1, 32),
    ("s", "w", 1, 33), ("r", "g", 0, 21), ("r", "w", 1, 30), ("r", "w", 1, 31), ("r", "w", 1, 22), ("r", "w", 1, 23), ("s", "w", 2, 0),
    ("s", "w", 2, 1), ("s", "w", 2, 2), ("s", "w", 2, 3), ("r", "w", 0, 35), ("r", "w", 0, 40), ("r", "w", 0, 31), ("r", "w", 0, 36),
    ("r", "w", 0, 45), ("r", "w", 0, 47), ("r", "w", 0, 44), ("r", "w", 0, 46), ("project", 1), ("r", "w", 1, 34), ("r", "w", 1, 35),
    ("r", "w", 1, 32), ("r", "w", 1, 33), ("retain", 1), ("s", "w", 3, 0), ("s", "w", 3, 5), ("s", "w", 3, 2), ("s", "w", 3, 7),
    ("part", 0, ((2, 0), (2, 1)), 0), ("project", 0), ("r", "d", 0, 0, 0, 0), ("r", "d", 0, 0, 1, 0), ("far", 0, 0, 0), ("s", "s", 0, 0, 0, 0),
    ("s", "s", 0, 0, 0, 1), ("r", "w", 2, 0), ("r", "w", 2, 1), ("r", "w", 2, 2), ("r", "w", 2, 3), ("far", 0, 1, 0), ("s", "w", 2, 4),
    ("s", "w", 2, 7), ("s", "w", 2, 10), ("s", "w", 2, 13), ("retain", 0), ("part", 0, ((1, 0), (-1, 0)), 0), ("s", "s", 0, 1, 0, 0),
    ("s", "s", 0, 1, 0, 1), ("part", 0, ((1, 1), (-1, 1)), 0), ("s", "w", 2, 11), ("s", "w", 2, 12), ("s", "w", 2, 5), ("s", "w", 2, 6),
    ("part", 0, ((0, 0), (0, 1)), 0), ("r", "w", 3, 0), ("r", "w", 3, 5), ("r", "w", 3, 2), ("r", "w", 3, 7), ("r", "d", 0, 1, 0, 0),
    ("free", 0, 0, 0, 1), ("r", "d", 0, 2, 0, 0), ("free", 0, 0, 0, 2), ("r", "d", 0, 1, 1, 0), ("free", 0, 1, 0, 1), ("r", "s", 0, 0, 0, 0),
    ("r", "s", 0, 0, 0, 1), ("near", 0, 0, 0, 1), ("r", "d", 0, 2, 1, 0), ("near", 0, 0, 0, 2), ("free", 0, 1, 0, 2), ("s", "s", 0, 0, 0, 2),
    ("s", "s", 0, 0, 0, 5), ("r", "d", 0, 3, 0, 0), ("r", "w", 2, 4), ("r", "w", 2, 7), ("r", "w", 2, 10), ("r", "w", 2, 13),
    ("s", "w", 2, 14), ("s", "w", 2, 15), ("s", "w", 2, 8), ("s", "w", 2, 9), ("r", "d", 0, 3, 1, 0), ("r", "s", 0, 1, 0, 0),
    ("r", "s", 0, 1, 0, 1), ("near", 0, 1, 0, 1), ("near", 0, 1, 0, 2), ("s", "s", 0, 0, 0, 3), ("s", "s", 0, 0, 0, 4), ("r", "w", 2, 11),
    ("r", "w", 2, 12), ("r", "w", 2, 5), ("r", "w", 2, 6), ("s", "w", 2, 24), ("s", "w", 2, 29), ("s", "w", 2, 16), ("s", "w", 2, 21),
    ("s", "w", 2, 28), ("s", "w", 2, 25), ("s", "w", 2, 20), ("s", "w", 2, 17), ("r", "s", 0, 0, 0, 2), ("r", "s", 0, 0, 0, 5),
    ("s", "s", 0, 1, 0, 2), ("s", "s", 0, 1, 0, 5), ("r", "w", 2, 14), ("r", "w", 2, 15), ("r", "w", 2, 8), ("r", "w", 2, 9),
    ("s", "w", 2, 26), ("s", "w", 2, 27), ("s", "w", 2, 18), ("s", "w", 2, 19), ("r", "w", 2, 24), ("r", "w", 2, 29), ("r", "w", 2, 16),
    ("r", "w", 2, 21), ("s", "w", 2, 30), ("s", "w", 2, 31), ("s", "w", 2, 22), ("s", "w", 2, 23), ("r", "s", 0, 0, 0, 3),
    ("r", "s", 0, 0, 0, 4), ("s", "s", 0, 1, 0, 3), ("s", "s", 0, 1, 0, 4), ("norm2", 0), ("s", "g", 1, 8), ("r", "w", 2, 28),
    ("r", "w", 2, 25), ("r", "w", 2, 20), ("r", "w", 2, 17), ("s", "w", 2, 34), ("s", "w", 2, 35), ("s", "w", 2, 32), ("s", "w", 2, 33),
    ("r", "w", 2, 26), ("r", "w", 2, 27), ("r", "w", 2, 18), ("r", "w", 2, 19), ("r", "g", 1, 8), ("s", "w", 3, 4), ("s", "w", 3, 1),
    ("s", "w", 3, 6), ("s", "w", 3, 3), ("r", "s", 0, 1, 0, 2), ("r", "s", 0, 1, 0, 5), ("s", "g", 1, 0), ("s", "g", 1, 3), ("r", "w", 2, 30),
    ("r", "w", 2, 31), ("r", "w", 2, 22), ("r", "w", 2, 23), ("r", "w", 2, 34), ("r", "w", 2, 35), ("r", "w", 2, 32), ("r", "w", 2, 33),
    ("s", "w", 3, 8), ("s", "w", 3, 20), ("s", "w", 3, 13), ("s", "w", 3, 25), ("r", "s", 0, 1, 0, 3), ("r", "s", 0, 1, 0, 4),
    ("s", "g", 1, 2), ("s", "g", 1, 1), ("norm2", 1), ("s", "g", 1, 9), ("r", "w", 3, 4), ("r", "w", 3, 1), ("r", "w", 3, 6),
    ("r", "w", 3, 3), ("r", "g", 1, 9), ("s", "w", 3, 14), ("s", "w", 3, 27), ("s", "w", 3, 9), ("s", "w", 3, 22), ("r", "g", 1, 0),
    ("s", "g", 1, 10), ("r", "g", 1, 3), ("s", "g", 1, 15), ("s", "g", 1, 22), ("s", "g", 1, 24), ("s", "w", 3, 16), ("s", "w", 3, 24),
    ("s", "w", 3, 11), ("s", "w", 3, 19), ("r", "g", 1, 10), ("r", "g", 1, 15), ("r", "w", 3, 8), ("r", "w", 3, 20), ("r", "w", 3, 13),
    ("r", "w", 3, 25), ("s", "w", 3, 32), ("s", "w", 3, 42), ("s", "w", 3, 28), ("s", "w", 3, 38), ("r", "g", 1, 2), ("s", "g", 1, 11),
    ("r", "g", 1, 1), ("s", "g", 1, 14), ("s", "g", 1, 4), ("s", "g", 1, 7), ("r", "w", 3, 14), ("r", "w", 3, 27), ("r", "w", 3, 9),
    ("r", "w", 3, 22), ("s", "w", 3, 26), ("s", "w", 3, 15), ("s", "w", 3, 21), ("s", "w", 3, 10), ("r", "g", 1, 11), ("r", "g", 1, 14),
    ("s", "w", 3, 23), ("s", "w", 3, 17), ("s", "w", 3, 18), ("s", "w", 3, 12), ("s", "g", 1, 6), ("s", "g", 1, 5),
    ("lift", ((0, 0), (-1, 0), (1, 0))), ("s", "w", 3, 41), ("s", "w", 3, 33), ("s", "w", 3, 37), ("s", "w", 3, 29), ("r", "w", 3, 16),
    ("r", "w", 3, 24), ("r", "w", 3, 11), ("r", "w", 3, 19), ("r", "g", 1, 22), ("s", "g", 1, 18), ("r", "g", 1, 24), ("s", "g", 1, 19),
    ("r", "w", 3, 32), ("r", "w", 3, 42), ("r", "w", 3, 28), ("r", "w", 3, 38), ("r", "w", 3, 26), ("r", "w", 3, 15), ("r", "w", 3, 21),
    ("r", "w", 3, 10), ("s", "w", 3, 34), ("s", "w", 3, 43), ("s", "w", 3, 30), ("s", "w", 3, 39), ("r", "g", 1, 18), ("r", "g", 1, 4),
    ("s", "g", 1, 12), ("r", "g", 1, 7), ("s", "g", 1, 17), ("r", "g", 1, 19), ("s", "w", 3, 35), ("s", "w", 3, 40), ("s", "w", 3, 31),
    ("s", "w", 3, 36), ("s", "g", 1, 23), ("s", "g", 1, 25), ("lift", ((2, 0),)), ("r", "w", 3, 23), ("r", "w", 3, 17), ("r", "w", 3, 18),
    ("r", "w", 3, 12), ("r", "g", 1, 12), ("part", 1, ((2, 0),), 0), ("r", "g", 1, 17), ("s", "w", 3, 45), ("s", "w", 3, 47),
    ("s", "w", 3, 44), ("s", "w", 3, 46), ("part", 1, ((1, 0), (-1, 0)), 0), ("r", "w", 3, 41), ("r", "w", 3, 33), ("r", "w", 3, 37),
    ("r", "w", 3, 29), ("r", "g", 1, 6), ("s", "g", 1, 13), ("r", "g", 1, 5), ("s", "g", 1, 16), ("r", "d", 1, 0, 0, 0), ("far", 1, 0, 0),
    ("s", "s", 1, 0, 0, 0), ("s", "s", 1, 0, 0, 1), ("r", "w", 3, 34), ("r", "w", 3, 43), ("r", "w", 3, 30), ("r", "w", 3, 39),
    ("r", "d", 1, 1, 0, 0), ("free", 1, 0, 0, 1), ("r", "d", 1, 2, 0, 0), ("free", 1, 0, 0, 2), ("s", "s", 1, 0, 0, 3), ("s", "s", 1, 0, 0, 4),
    ("r", "g", 1, 13), ("r", "w", 3, 35), ("r", "w", 3, 40), ("r", "w", 3, 31), ("r", "w", 3, 36), ("r", "g", 1, 16),
    ("lift", ((0, 1), (-1, 1), (1, 1))), ("r", "g", 1, 23), ("s", "g", 1, 20), ("r", "g", 1, 25), ("s", "g", 1, 21), ("r", "w", 3, 45),
    ("r", "w", 3, 47), ("r", "w", 3, 44), ("r", "w", 3, 46), ("r", "s", 1, 0, 0, 0), ("r", "s", 1, 0, 0, 1), ("near", 1, 0, 0, 1),
    ("s", "s", 1, 0, 0, 2), ("near", 1, 0, 0, 2), ("s", "s", 1, 0, 0, 5), ("part", 1, ((2, 0),), 1), ("part", 1, ((1, 1), (-1, 1)), 0),
    ("r", "s", 1, 0, 0, 3), ("r", "s", 1, 0, 0, 4), ("r", "g", 1, 20), ("part", 1, ((1, 0), (-1, 0)), 1), ("r", "g", 1, 21),
    ("r", "d", 1, 0, 0, 1), ("far", 1, 0, 1), ("s", "s", 1, 0, 1, 0), ("s", "s", 1, 0, 1, 1), ("lift", ((2, 1),)), ("r", "d", 1, 1, 1, 0),
    ("r", "d", 1, 2, 1, 0), ("r", "s", 1, 0, 0, 2), ("r", "s", 1, 0, 0, 5), ("r", "d", 1, 1, 0, 1), ("free", 1, 1, 0, 1), ("s", "s", 1, 1, 0, 3),
    ("free", 1, 1, 0, 2), ("s", "s", 1, 1, 0, 4), ("free", 1, 0, 1, 1), ("part", 1, ((2, 1),), 0), ("r", "d", 1, 2, 0, 1), ("free", 1, 0, 1, 2),
    ("s", "s", 1, 0, 1, 3), ("s", "s", 1, 0, 1, 4), ("part", 1, ((2, 1),), 1), ("part", 1, ((1, 1), (-1, 1)), 1), ("r", "d", 1, 0, 1, 0),
    ("r", "s", 1, 0, 1, 0), ("r", "s", 1, 0, 1, 1), ("far", 1, 1, 0), ("near", 1, 0, 1, 1), ("near", 1, 0, 1, 2), ("s", "s", 1, 1, 0, 0),
    ("s", "s", 1, 1, 0, 1), ("part", 1, ((0, 0), (0, 1)), 0), ("r", "d", 1, 0, 1, 1), ("far", 1, 1, 1), ("s", "s", 1, 1, 1, 0),
    ("s", "s", 1, 1, 1, 1), ("part", 1, ((0, 0), (0, 1)), 1), ("r", "s", 1, 1, 0, 3), ("r", "s", 1, 1, 0, 4), ("r", "d", 1, 1, 1, 1),
    ("r", "d", 1, 2, 1, 1), ("free", 1, 1, 1, 1), ("free", 1, 1, 1, 2), ("r", "d", 1, 3, 0, 0), ("finish", 0, 0), ("r", "d", 1, 3, 1, 0),
    ("r", "s", 1, 0, 1, 3), ("r", "s", 1, 0, 1, 4), ("s", "s", 1, 0, 1, 2), ("s", "s", 1, 0, 1, 5), ("r", "d", 1, 3, 0, 1), ("r", "d", 1, 3, 1, 1),
    ("r", "s", 1, 1, 0, 0), ("near", 1, 1, 0, 1), ("r", "s", 1, 1, 0, 1), ("near", 1, 1, 0, 2), ("s", "s", 1, 1, 0, 2), ("s", "s", 1, 1, 0, 5),
    ("r", "s", 1, 1, 1, 0), ("near", 1, 1, 1, 1), ("r", "s", 1, 1, 1, 1), ("near", 1, 1, 1, 2), ("s", "s", 1, 1, 1, 2), ("s", "s", 1, 1, 1, 5),
    ("r", "s", 1, 0, 1, 2), ("r", "s", 1, 0, 1, 5), ("finish", 0, 1), ("s", "s", 1, 1, 1, 3), ("s", "s", 1, 1, 1, 4), ("r", "s", 1, 1, 0, 2),
    ("r", "s", 1, 1, 0, 5), ("finish", 1, 0), ("r", "s", 1, 1, 1, 2), ("r", "s", 1, 1, 1, 5), ("r", "s", 1, 1, 1, 3), ("r", "s", 1, 1, 1, 4),
    ("finish", 1, 1),
)


def kernel(
    resid, mix_gain, wq, wk, wv, wg, wo, rate, mlp_gain, wu, wd,
    out,
    w_in, w_out, w_up, w_down, xn, rbuf, after, proj, gated, hid, decay, kept,
    dout, din, sout, rin2, rin1,
    local_sem, w_send, w_recv, g_send, g_recv, d_send, d_recv, s_send, s_recv,
):
    fs, tp = lax.axis_index("fs"), lax.axis_index("tp")
    z, y, x, c = fs // RING, fs % RING, tp // 2, tp % 2

    def turn(v, d):
        return (v + d + RING) % RING

    device = {
        "y+": (z * RING + turn(y, 1), tp),
        "y-": (z * RING + turn(y, -1), tp),
        "z+": (turn(z, 1) * RING + y, tp),
        "z-": (turn(z, -1) * RING + y, tp),
        "x+": (fs, turn(x, 1) * 2 + c),
        "x-": (fs, turn(x, -1) * 2 + c),
        "d": (fs, x * 2 + 1 - c),
    }

    def remote(src, dst, send, recv, way):
        return pltpu.make_async_remote_copy(
            src_ref=src, dst_ref=dst, send_sem=send, recv_sem=recv,
            device_id=device[way], device_id_type=MESH,
        )

    def send(*args):
        remote(*args).start()

    weights = (w_in, w_out, w_up, w_down)

    def block(dy, dz):
        return turn(z, dz) * RING + turn(y, dy)

    def piece(t, dy, dz, part):
        ref = weights[t]
        f = block(dy, dz)
        if part == "full":
            return ref.at[f]
        if part in ("A", "B"):
            return ref.at[f, :, "AB".index(part)]
        if part in ("h0", "h1"):
            return ref.at[f, int(part[1])]
        return ref.at[f, int(part[2]), "AB".index(part[0])]

    def w_copy(t, n, place):
        dy, dz, part, way = place
        ref = piece(t, dy, dz, part)
        return (ref, ref, w_send.at[t], w_recv.at[t, n], way)

    def g_copy(g, n, dx, core):
        h, q, way = GATHER[n][1:]
        block = turn(x, dx) * 2 + core
        ref = xn.at[g, block, h] if q is None else xn.at[g, block, h, q]
        return (ref, ref, g_send.at[g], g_recv.at[g, n], way)

    def rows16(count, body):
        def step(i, carry):
            body(pl.ds(pl.multiple_of(i * 16, 16), 16))
            return carry

        lax.fori_loop(0, count // 16, step, 0)

    def of(ref, j, g):
        return ref if g == 0 else ref.at[:, pl.ds(j * 1024, 1024)]

    def d_copy(g, k, h, j):
        columns = slice(None) if g == 0 else pl.ds(j * 1024, 1024)
        return (
            dout.at[g, k, h, :, :, columns], din.at[g, k, h, :, :, columns],
            d_send.at[g], d_recv.at[g, k, h, j], "d",
        )

    def s_copy(g, h, j, n):
        if n < 2:
            src, dst, way = sout.at[g, 0, h, n], rin2.at[g, h, n], ("x+", "x-")[n]
        elif n < 4:
            src, dst, way = sout.at[g, 1, h, n - 2], rin1.at[g, 0, h, n - 2], "x+"
        else:
            src, dst, way = sout.at[g, 2, h, n - 4], rin1.at[g, 1, h, n - 4], "x-"
        return (of(src, j, g), of(dst, j, g), s_send.at[g], s_recv.at[g, h, j, n], way)

    def start(kind, *which):
        if kind == "w":
            t, n = which
            send(*w_copy(t, n, MESSAGES[t][n]))
        elif kind == "g":
            g, n = which
            send(*g_copy(g, n, GATHER[n][0], c))
        else:
            send(*s_copy(*which))

    def receive(kind, *which):
        if kind == "w":
            t, n = which
            copy = w_copy(t, n, arrived(MESSAGES[t][n]))
        elif kind == "g":
            g, n = which
            dx, way = GATHER[n][0], GATHER[n][3]
            if way == "d":
                copy = g_copy(g, n, dx, 1 - c)
            else:
                copy = g_copy(g, n, near(dx - (1 if way == "x+" else -1)), c)
        elif kind == "d":
            copy = d_copy(*which)
        else:
            copy = s_copy(*which)
        remote(*copy).wait_recv()

    def product(g, cases, lhs, w, columns):
        rows = jnp.concatenate([block for case in cases for block in lhs(*case)], axis=0)
        o = jnp.dot(rows, w, preferred_element_type=F32)
        for n, (dx, h) in enumerate(cases):
            mine = o[n * 128 : (n + 1) * 128]
            dout[g, TURN[dx], h, :, :, columns] = mine[:64].astype(BF16).reshape(2, 32, 512)
            kept[TURN[dx], h, :, :, columns] = mine[64:].reshape(2, 32, 512)

    def partial(g, cases, j):
        if g == 0:
            depth = wo.shape[0] * wo.shape[1] * wo.shape[2]

            def step(i, carry):
                w = [w_out[4 * i + n].reshape(depth, 128) for n in range(4)]
                columns = pl.ds(pl.multiple_of(i * 512, 512), 512)
                product(0, cases, gated_rows, jnp.concatenate(w, axis=1), columns)
                return carry

            lax.fori_loop(0, 4, step, 0)
        else:
            depth = wd.shape[0] * wd.shape[1] * wd.shape[2]
            for i in (2 * j, 2 * j + 1):
                w = [w_down[block(*PLACES[4 * i + n])].reshape(depth, 128) for n in range(4)]
                columns = slice(i * 512, (i + 1) * 512)
                product(1, cases, hidden_rows, jnp.concatenate(w, axis=1), columns)
        for dx, h in cases:
            send(*d_copy(g, TURN[dx], h, j))

    def add_quarter(g, k, h, j, q, extra=False):
        columns = slice(None) if g == 0 else slice(j * 1024, (j + 1) * 1024)

        def body(rows):
            total = kept[k, h, q, rows, columns] + din[g, k, h, q, rows, columns].astype(F32)
            if extra:
                total = total + rin2[g, h, q, rows, columns].astype(F32)
            sout[g, k, h, q, rows, columns] = total.astype(BF16)

        rows16(32, body)

    def add_far(g, h, j):
        for q in (0, 1):
            add_quarter(g, 0, h, j, q)

    def add_free(g, h, j, k):
        add_quarter(g, k, h, j, 1 if k == 1 else 0)

    def add_near(g, h, j, k):
        add_quarter(g, k, h, j, 0 if k == 1 else 1, True)

    def sum_rows(h, q, rows):
        total = kept[3, h, q, rows, :] + din[0, 3, h, q, rows, :].astype(F32)
        return total + rin1[0, 0, h, q, rows, :].astype(F32) + rin1[0, 1, h, q, rows, :].astype(F32)

    def normed(values, gain):
        scale = lax.rsqrt(jnp.mean(values * values, axis=-1, keepdims=True) + EPS)
        return (values * scale * gain).astype(BF16)

    loads = []

    def load(src, dst):
        copy = pltpu.make_async_copy(src, dst, local_sem.at[len(loads)])
        copy.start()
        loads.append(copy)

    for src, low, wide in ((wq, 0, 128), (wk, 128, 128), (wv, 256, 256), (wg, 512, 256)):
        load(src, w_in.at[fs, :, :, :, low : low + wide])
    load(resid, rbuf)
    load(wo, w_out.at[fs])
    load(wu, w_up.at[fs])
    load(wd, w_down.at[fs])
    barrier = pltpu.get_barrier_semaphore()
    for way in device:
        pl.semaphore_signal(barrier, inc=1, device_id=device[way], device_id_type=MESH)
    for copy in loads[:5]:
        copy.wait()
    for h in (0, 1):
        for q in (0, 1):
            def first_norm(rows):
                xn[0, tp, h, q, rows, :] = normed(rbuf[h, q, rows, :].astype(F32), mix_gain[...])

            rows16(32, first_norm)
    pl.semaphore_wait(barrier, 7)
    r = rate[0]

    def make_decay():
        def some_rows(i, carry):
            rows = pl.ds(pl.multiple_of(i * 64, 64), 64)
            t = lax.broadcasted_iota(jnp.int32, (64, LENGTH), 0) + i * 64
            s = lax.broadcasted_iota(jnp.int32, (64, LENGTH), 1)
            gap = (t - s).astype(F32)
            value = jnp.exp(-r * jnp.maximum(gap, 0.0)) * DK ** (-0.5)
            decay[rows, :] = jnp.where(gap >= 0.0, value, 0.0)
            return carry

        lax.fori_loop(0, LENGTH // 64, some_rows, 0)

    own = x // 2
    sequence = (own, 1 - own)

    def project(seq):
        def body(j, carry):
            columns = pl.ds(pl.multiple_of(j * 256, 256), 256)
            lhs = xn[0, pl.ds(4 * seq, 4)].reshape(512, D)
            rhs = w_in[:, :, :, :, columns].reshape(D, 256)
            o = jnp.dot(lhs, rhs, preferred_element_type=F32).astype(BF16)
            proj[pl.ds(4 * seq, 4), :, columns] = o.reshape(4, 128, 256)
            return carry

        lax.fori_loop(0, 3, body, 0)

    def retain(seq):
        for i in (0, 1):
            mine = pl.ds(seq * 4 + 2 * i, 2)
            upto = pl.ds(seq * 4, 2 * i + 2)
            wide = 256 * (i + 1)
            q = proj[mine, :, 0:128].reshape(256, DK)
            k = proj[upto, :, 128:256].reshape(wide, DK)
            v = proj[upto, :, 256:512].reshape(wide, DV)
            scores = lax.dot_general(q, k, (((1,), (1,)), ((), ())), preferred_element_type=F32)
            scores = (scores * decay[i * 256 : (i + 1) * 256, 0:wide]).astype(BF16)
            mixed = jnp.dot(scores, v, preferred_element_type=F32)
            mixed = mixed - jnp.mean(mixed, axis=-1, keepdims=True)
            spread = jnp.mean(mixed * mixed, axis=-1, keepdims=True)
            gate = proj[mine, :, 512:768].reshape(256, DV).astype(F32)
            value = gate / (1.0 + jnp.exp(-gate)) * (mixed * lax.rsqrt(spread + EPS))
            gated[mine] = value.astype(BF16).reshape(2, 2, 64, DV)

    def gated_rows(dx, h):
        first = turn(x, dx) * 2
        return gated[first + 1 - c, h], gated[first + c, h]

    def lift(cases):
        def body(j, carry):
            columns = pl.ds(pl.multiple_of(j * 256, 256), 256)
            lhs = jnp.concatenate(
                [
                    xn[1, turn(x, dx) * 2 + core, h].reshape(64, D)
                    for dx, h in cases
                    for core in (1 - c, c)
                ],
                axis=0,
            )
            rhs = w_up[:, :, :, :, columns].reshape(D, 256)
            o = jnp.maximum(jnp.dot(lhs, rhs, preferred_element_type=F32), 0.0)
            o = (o * o).astype(BF16)
            for n, (dx, h) in enumerate(cases):
                hid[TURN[dx], h, :, columns] = o[n * 128 : (n + 1) * 128]
            return carry

        lax.fori_loop(0, w_up.shape[4] // 256, body, 0)

    def hidden_rows(dx, h):
        return (hid[TURN[dx], h],)

    def second_norm(h):
        for q in (0, 1):
            def body(rows):
                value = rbuf[h, q, rows, :].astype(F32) + sum_rows(h, q, rows)
                value = value.astype(BF16)
                after[h, q, rows, :] = value
                xn[1, tp, h, q, rows, :] = normed(value.astype(F32), mlp_gain[...])

            rows16(32, body)

    def finish(h, j):
        for i in range(8 * j, 8 * j + 8):
            here = pl.ds(pl.multiple_of(block(*PLACES[i]) * 128, 128), 128)
            at = slice(i * 128, (i + 1) * 128)
            total = after[h, :, :, here].astype(F32) + kept[3, h, :, :, at]
            total = total + din[1, 3, h, :, :, at].astype(F32)
            total = total + rin1[1, 0, h, :, :, at].astype(F32) + rin1[1, 1, h, :, :, at].astype(F32)
            out[h, :, :, here] = total.astype(BF16)

    actions = {
        "s": start,
        "r": receive,
        "decay": make_decay,
        "project": lambda which: project(sequence[which]),
        "retain": lambda which: retain(sequence[which]),
        "part": partial,
        "far": add_far,
        "free": add_free,
        "near": add_near,
        "norm2": second_norm,
        "lift": lift,
        "finish": finish,
    }
    for copy in loads[5:]:
        copy.wait()
    for name, *which in SCHEDULE:
        actions[name](*which)
    for t in range(4):
        ref = weights[t].at[0:15]
        remote(ref, ref, w_send.at[t], w_recv.at[t, 0], "d").wait_send()
    for g in (0, 1):
        remote(xn.at[g, 0:7], xn.at[g, 0:7], g_send.at[g], g_recv.at[g, 0], "d").wait_send()
        remote(dout.at[g], din.at[g], d_send.at[g], d_recv.at[g, 0, 0, 0], "d").wait_send()
        remote(sout.at[g], sout.at[g], s_send.at[g], s_recv.at[g, 0, 0, 0], "d").wait_send()


def on_device(
    resid, mix_gain, w_query, w_key, w_value, w_gate, w_output, decay_rate, mlp_gain, w_up, w_down
):
    def cut(w):
        return w.reshape(2, 2, w.shape[0] // 4, w.shape[1])

    wide = w_query.shape[1] + w_key.shape[1] + w_value.shape[1] + w_gate.shape[1]
    count = RING * RING

    def held(rows, columns):
        return pltpu.VMEM((count, 2, 2, rows // 4, columns), BF16)

    dma = pltpu.SemaphoreType.DMA
    vmem = pl.BlockSpec(memory_space=pltpu.VMEM)
    hbm = pl.BlockSpec(memory_space=pl.ANY)
    tokens = (2, 2, 32, D)
    number = max(len(messages) for messages in MESSAGES)
    result = pl.pallas_call(
        kernel,
        out_shape=jax.ShapeDtypeStruct(tokens, BF16),
        in_specs=[
            hbm, vmem, hbm, hbm, hbm, hbm, hbm,
            pl.BlockSpec(memory_space=pltpu.SMEM), vmem, hbm, hbm,
        ],
        out_specs=vmem,
        scratch_shapes=[
            held(128, wide),
            held(w_output.shape[0], 128),
            held(128, w_up.shape[1]),
            held(w_down.shape[0], 128),
            pltpu.VMEM((2, 8) + tokens, BF16),
            pltpu.VMEM(tokens, BF16),
            pltpu.VMEM(tokens, BF16),
            pltpu.VMEM((8, 128, wide), BF16),
            pltpu.VMEM((8, 2, 64, DV), BF16),
            pltpu.VMEM((4, 2, 128, w_up.shape[1]), BF16),
            pltpu.VMEM((LENGTH, LENGTH), F32),
            pltpu.VMEM((4,) + tokens, F32),
            pltpu.VMEM((2, 4) + tokens, BF16),
            pltpu.VMEM((2, 4) + tokens, BF16),
            pltpu.VMEM((2, 3) + tokens, BF16),
            pltpu.VMEM((2,) + tokens, BF16),
            pltpu.VMEM((2, 2) + tokens, BF16),
            dma((8,)),
            dma((4,)),
            dma((4, number)),
            dma((2,)),
            dma((2, len(GATHER))),
            dma((2,)),
            dma((2, 4, 2, 2)),
            dma((2,)),
            dma((2, 2, 2, 6)),
        ],
        compiler_params=pltpu.CompilerParams(
            collective_id=0, has_side_effects=True, vmem_limit_bytes=63 * 1024 * 1024
        ),
    )(
        resid.reshape(tokens), mix_gain[None], cut(w_query), cut(w_key), cut(w_value), cut(w_gate),
        cut(w_output), decay_rate, mlp_gain[None], cut(w_up), cut(w_down),
    )
    return result.reshape(resid.shape)


def solution(mesh):
    placed = (
        P(("fs", "tp"), None),
        P(),
        P("fs", "tp"),
        P("fs", "tp"),
        P("fs", "tp"),
        P("fs", "tp"),
        P("tp", "fs"),
        P("tp"),
        P(),
        P("fs", "tp"),
        P("tp", "fs"),
    )
    return jax.shard_map(
        on_device, mesh=mesh, in_specs=placed, out_specs=P(("fs", "tp"), None), check_vma=False
    )
```

time: 113 us -> 102 us (0.903)
  Pallas kernels: 110 us -> 98.9 us
    pallas_call x1, Pallas kernels: 110 us -> 98.9 us  [on_device(): pl.pallas_call(kernel, out_shape=jax.ShapeDtypeStruct(tokens, BF16), in_s...]
where the time goes in v3:
time: 102 us; the launch traced here: 101 us
  Pallas kernels  98.9 us (97%)
  local copies, waits for them, and re-layouts  1.88 us (2%)
    pallas_call x1, Pallas kernels, on_device(): pl.pallas_call(kernel, out_shape=jax.ShapeDtypeStruct(tokens, BF16), in_s...  98.9 us

profile of v3, /device:TPU:1, one launch (start us, length us, event | category | flops | bytes accessed | tf_op | source)
XLA Modules:
  0.0 101.4 jit_solution(13632083874919855944)
XLA Ops:
  0.7 98.9 %shard_map.109 = bf16[2,2,32,2048]{3,2,1,0:T(8,128)(2,1)} custom-call(bf16[2,2,32,2048]{3,2,1,0:T(8,128)(2,1)} %bitcast.12, f32[1,2048]{1,0:T(1,128)} %bitcast.20, bf16[2,2,32,128]{3,2,1,0:T(8,128)(2,1)} %bitcast.18, bf16[2,2,32,128]{3,2,1,0:T(8,128)(2,1)} %bitcast.19, bf16[2,2,32,256]{3,2,1,0:T(8,128)(2,1)} %bitcast.15, bf16[2,2,32,256]{3,2,1,0:T(8,128)(2,1)} %bitcast.16, ...), custom_call_target="tpu_custom_call" | custom-call | tf_op jit(solution)/shard_map/pallas_call | solution.py:495
  99.5 1.9 %copy.14 = bf16[128,2048]{1,0:T(8,128)(2,1)} copy(bf16[128,2048]{1,0:T(8,128)(2,1)} %bitcast.11) | data formatting | bytes 1048576

commit v4 on v3

v4 whole, which is shorter than its diff:
```python
import jax
import jax.numpy as jnp
from jax import lax
from jax.experimental import pallas as pl
from jax.experimental.pallas import tpu as pltpu
from jax.sharding import PartitionSpec as P

D = 2048
DK = 128
DV = 256
LENGTH = 512
RING = 4
EPS = 1e-06
MESH = pl.DeviceIdType.MESH
F32 = jnp.float32
BF16 = jnp.bfloat16

STEP = {"y+": (1, 0), "y-": (-1, 0), "z+": (0, 1), "z-": (0, -1)}


def near(d):
    return {0: 0, 1: 1, 2: 2, 3: -1}[d % RING]


def arrived(message):
    dy, dz, part, way = message
    return near(dy - STEP[way][0]), near(dz - STEP[way][1]), part, way


def onward(message):
    dy, dz, part, way = arrived(message)
    half = "0" if way[1] == "+" else "1"
    along = way[0] == "y"
    across = ("z+", "z-") if along else ("y+", "y-")
    first = "A" if along else "B"
    if part == "full":
        return [(dy, dz, "h" + half, way)] + [(dy, dz, first, w) for w in across]
    if part in ("h0", "h1"):
        onto = [(dy, dz, part, way)] if (dy if along else dz) != 2 and part[1] == half else []
        return onto + [(dy, dz, first + part, w) for w in across]
    if part in ("A", "B"):
        return [(dy, dz, part + "h" + half, way)]
    if (dy if way[0] == "y" else dz) != 2 and part[-1] == half:
        return [(dy, dz, part, way)]
    return []


def plan(parts):
    messages = [(0, 0, part, way) for part in parts for way in ("y+", "y-", "z+", "z-")]
    for message in messages:
        messages += onward(message)
    return messages


MESSAGES = [plan(parts) for parts in (("h0", "h1"), ("full",), ("full",), ("h0", "h1"))]
PLACES = (
    (0, 0), (1, 0), (-1, 0), (0, 1), (0, -1), (2, 0), (0, 2), (1, 1),
    (1, -1), (-1, 1), (-1, -1), (2, 1), (2, -1), (1, 2), (-1, 2), (2, 2),
)

GATHER = (
    [(0, h, q, w) for h in (0, 1) for q in (0, 1) for w in ("x+", "x-")]
    + [(0, h, None, "d") for h in (0, 1)]
    + [(dx, h, q, "d") for dx in (-1, 1, 2) for h in (0, 1) for q in (0, 1)]
    + [(-1, h, 0, "x+") for h in (0, 1)]
    + [(1, h, 1, "x-") for h in (0, 1)]
)
TURN = {2: 0, 1: 1, -1: 2, 0: 3}

S, R, W, G, C, X = range(6)
DECAY, PROJECT, RETAIN, PRODUCT, FAR, FREE, NEAR, NORM, LIFT, FINISH = range(6, 16)
SCHEDULE = (
    (S, W, 0, 0), (S, W, 0, 5), (S, W, 0, 2), (S, W, 0, 7), (S, G, 0, 0), (S, G, 0, 3), (S, G, 0, 8), (S, G, 0, 9),
    (DECAY,), (S, W, 1, 0), (S, W, 1, 1), (S, W, 1, 2), (S, W, 1, 3), (R, G, 0, 8), (S, G, 0, 2), (S, G, 0, 1),
    (R, G, 0, 9), (S, W, 0, 4), (S, W, 0, 1), (S, W, 0, 6), (S, W, 0, 3), (R, W, 0, 0), (R, W, 0, 5), (R, W, 0, 2),
    (R, W, 0, 7), (S, W, 0, 8), (S, W, 0, 20), (S, W, 0, 13), (S, W, 0, 25), (S, G, 0, 4), (S, G, 0, 7), (R, G, 0, 0),
    (S, G, 0, 10), (R, G, 0, 3), (S, G, 0, 15), (R, W, 1, 0), (R, W, 1, 1), (R, W, 1, 2), (R, W, 1, 3), (R, G, 0, 10),
    (S, W, 1, 4), (S, W, 1, 7), (S, W, 1, 10), (S, W, 1, 13), (R, G, 0, 15), (S, W, 0, 14), (S, W, 0, 27),
    (S, W, 0, 9), (S, W, 0, 22), (S, G, 0, 22), (S, G, 0, 24), (R, G, 0, 2), (S, G, 0, 11), (R, G, 0, 1),
    (S, G, 0, 14), (R, W, 0, 4), (R, W, 0, 1), (R, W, 0, 6), (R, W, 0, 3), (S, W, 1, 11), (S, W, 1, 12), (S, W, 1, 5),
    (S, W, 1, 6), (S, W, 1, 14), (S, W, 1, 15), (S, W, 1, 8), (S, W, 1, 9), (R, G, 0, 11), (R, G, 0, 14),
    (S, W, 0, 16), (S, W, 0, 24), (S, W, 0, 11), (S, W, 0, 19), (R, W, 0, 8), (R, W, 0, 20), (R, W, 0, 13),
    (R, W, 0, 25), (S, G, 0, 6), (S, G, 0, 5), (R, G, 0, 4), (S, G, 0, 12), (R, G, 0, 7), (S, G, 0, 17), (R, W, 1, 4),
    (R, W, 1, 7), (R, W, 1, 10), (R, W, 1, 13), (S, W, 0, 32), (S, W, 0, 42), (S, W, 0, 28), (S, W, 0, 38),
    (R, W, 0, 14), (R, W, 0, 27), (R, W, 0, 9), (R, W, 0, 22), (S, W, 1, 24), (S, W, 1, 29), (S, W, 1, 16),
    (S, W, 1, 21), (R, G, 0, 12), (S, W, 0, 26), (S, W, 0, 15), (S, W, 0, 21), (S, W, 0, 10), (R, G, 0, 17),
    (R, W, 1, 11), (R, W, 1, 12), (R, W, 1, 5), (R, W, 1, 6), (S, G, 0, 23), (S, G, 0, 25), (R, W, 1, 14),
    (R, W, 1, 15), (R, W, 1, 8), (R, W, 1, 9), (S, W, 0, 23), (S, W, 0, 17), (S, W, 0, 18), (S, W, 0, 12),
    (R, G, 0, 22), (S, G, 0, 18), (R, G, 0, 24), (S, G, 0, 19), (R, W, 0, 16), (R, W, 0, 24), (R, W, 0, 11),
    (R, W, 0, 19), (S, W, 0, 41), (S, W, 0, 33), (S, W, 0, 37), (S, W, 0, 29), (R, G, 0, 18), (R, G, 0, 19),
    (R, W, 0, 32), (R, W, 0, 42), (R, W, 0, 28), (R, W, 0, 38), (S, W, 1, 28), (S, W, 1, 25), (S, W, 1, 20),
    (S, W, 1, 17), (R, W, 1, 24), (R, W, 1, 29), (R, W, 1, 16), (R, W, 1, 21), (S, W, 0, 34), (S, W, 0, 43),
    (S, W, 0, 30), (S, W, 0, 39), (R, G, 0, 6), (S, G, 0, 13), (R, G, 0, 5), (S, G, 0, 16), (R, W, 0, 26),
    (R, W, 0, 15), (R, W, 0, 21), (R, W, 0, 10), (S, W, 1, 26), (S, W, 1, 27), (S, W, 1, 18), (S, W, 1, 19),
    (S, W, 1, 30), (S, W, 1, 31), (S, W, 1, 22), (S, W, 1, 23), (S, W, 0, 35), (S, W, 0, 40), (S, W, 0, 31),
    (S, W, 0, 36), (R, G, 0, 13), (R, W, 0, 23), (R, W, 0, 17), (R, W, 0, 18), (R, W, 0, 12), (R, G, 0, 16),
    (S, W, 0, 45), (S, W, 0, 47), (S, W, 0, 44), (S, W, 0, 46), (R, W, 0, 41), (R, W, 0, 33), (R, W, 0, 37),
    (R, W, 0, 29), (R, G, 0, 23), (S, G, 0, 20), (R, G, 0, 25), (S, G, 0, 21), (R, W, 1, 28), (R, W, 1, 25),
    (R, W, 1, 20), (R, W, 1, 17), (S, W, 1, 34), (S, W, 1, 35), (S, W, 1, 32), (S, W, 1, 33), (S, W, 2, 0),
    (S, W, 2, 1), (S, W, 2, 2), (S, W, 2, 3), (R, W, 0, 34), (R, W, 0, 43), (R, W, 0, 30), (R, W, 0, 39),
    (R, G, 0, 20), (R, W, 1, 26), (R, W, 1, 27), (R, W, 1, 18), (R, W, 1, 19), (R, G, 0, 21), (R, W, 1, 30),
    (R, W, 1, 31), (R, W, 1, 22), (R, W, 1, 23), (R, W, 0, 35), (R, W, 0, 40), (R, W, 0, 31), (R, W, 0, 36),
    (R, W, 0, 45), (R, W, 0, 47), (R, W, 0, 44), (R, W, 0, 46), (PROJECT, 1, 0), (R, W, 1, 34), (R, W, 1, 35),
    (R, W, 1, 32), (R, W, 1, 33), (PROJECT, 1, 1), (PROJECT, 1, 2), (S, W, 3, 0), (S, W, 3, 5), (S, W, 3, 2),
    (S, W, 3, 7), (RETAIN, 1), (PRODUCT, 0, ((2, 0), (2, 1)), 0), (PROJECT, 0, 0), (PROJECT, 0, 1), (S, W, 3, 4),
    (S, W, 3, 1), (S, W, 3, 6), (S, W, 3, 3), (PROJECT, 0, 2), (R, C, 0, 0, 0, 0), (R, C, 0, 0, 1, 0), (FAR, 0, 0, 0),
    (S, X, 0, 0, 0, 0), (S, X, 0, 0, 0, 1), (R, W, 2, 0), (R, W, 2, 1), (R, W, 2, 2), (R, W, 2, 3), (FAR, 0, 1, 0),
    (RETAIN, 0), (PRODUCT, 0, ((1, 0), (-1, 0)), 0), (S, W, 2, 4), (S, W, 2, 7), (S, W, 2, 10), (S, W, 2, 13),
    (S, X, 0, 1, 0, 0), (S, X, 0, 1, 0, 1), (PRODUCT, 0, ((1, 1), (-1, 1)), 0), (PRODUCT, 0, ((0, 0), (0, 1)), 0),
    (R, W, 3, 0), (R, W, 3, 5), (R, W, 3, 2), (R, W, 3, 7), (R, C, 0, 1, 0, 0), (FREE, 0, 0, 0, 1),
    (R, C, 0, 2, 0, 0), (FREE, 0, 0, 0, 2), (R, C, 0, 1, 1, 0), (FREE, 0, 1, 0, 1), (S, X, 0, 0, 0, 3),
    (S, X, 0, 0, 0, 4), (S, W, 2, 11), (S, W, 2, 12), (S, W, 2, 5), (S, W, 2, 6), (R, C, 0, 2, 1, 0),
    (FREE, 0, 1, 0, 2), (R, X, 0, 0, 0, 0), (R, X, 0, 0, 0, 1), (NEAR, 0, 0, 0, 1), (NEAR, 0, 0, 0, 2),
    (R, C, 0, 3, 0, 0), (R, W, 3, 4), (R, W, 3, 1), (R, W, 3, 6), (R, W, 3, 3), (R, C, 0, 3, 1, 0),
    (S, X, 0, 0, 0, 2), (S, X, 0, 0, 0, 5), (S, W, 2, 14), (S, W, 2, 15), (S, W, 2, 8), (S, W, 2, 9),
    (R, X, 0, 1, 0, 0), (R, X, 0, 1, 0, 1), (NEAR, 0, 1, 0, 1), (NEAR, 0, 1, 0, 2), (R, W, 2, 4), (R, W, 2, 7),
    (R, W, 2, 10), (R, W, 2, 13), (S, X, 0, 1, 0, 2), (S, X, 0, 1, 0, 5), (S, W, 2, 24), (S, W, 2, 29), (S, W, 2, 16),
    (S, W, 2, 21), (R, X, 0, 0, 0, 3), (R, X, 0, 0, 0, 4), (R, W, 2, 11), (R, W, 2, 12), (R, W, 2, 5), (R, W, 2, 6),
    (S, W, 2, 28), (S, W, 2, 25), (S, W, 2, 20), (S, W, 2, 17), (S, X, 0, 1, 0, 3), (S, X, 0, 1, 0, 4), (S, W, 2, 26),
    (S, W, 2, 27), (S, W, 2, 18), (S, W, 2, 19), (R, X, 0, 0, 0, 2), (R, X, 0, 0, 0, 5), (NORM, 0), (S, G, 1, 8),
    (R, W, 2, 14), (R, W, 2, 15), (R, W, 2, 8), (R, W, 2, 9), (S, W, 2, 30), (S, W, 2, 31), (S, W, 2, 22),
    (S, W, 2, 23), (R, W, 2, 24), (R, W, 2, 29), (R, W, 2, 16), (R, W, 2, 21), (S, G, 1, 0), (S, G, 1, 3),
    (R, G, 1, 8), (S, W, 2, 34), (S, W, 2, 35), (S, W, 2, 32), (S, W, 2, 33), (R, X, 0, 1, 0, 2), (R, X, 0, 1, 0, 5),
    (R, W, 2, 28), (R, W, 2, 25), (R, W, 2, 20), (R, W, 2, 17), (S, W, 3, 8), (S, W, 3, 20), (S, W, 3, 13),
    (S, W, 3, 25), (R, W, 2, 26), (R, W, 2, 27), (R, W, 2, 18), (R, W, 2, 19), (S, G, 1, 2), (S, G, 1, 1),
    (R, X, 0, 1, 0, 3), (R, X, 0, 1, 0, 4), (NORM, 1), (S, G, 1, 9), (R, W, 2, 30), (R, W, 2, 31), (R, W, 2, 22),
    (R, W, 2, 23), (S, W, 3, 14), (S, W, 3, 27), (S, W, 3, 9), (S, W, 3, 22), (R, W, 2, 34), (R, W, 2, 35),
    (R, W, 2, 32), (R, W, 2, 33), (S, G, 1, 4), (S, G, 1, 7), (R, G, 1, 9), (S, W, 3, 16), (S, W, 3, 24),
    (S, W, 3, 11), (S, W, 3, 19), (R, G, 1, 0), (S, G, 1, 10), (R, G, 1, 3), (S, G, 1, 15), (S, W, 3, 26),
    (S, W, 3, 15), (S, W, 3, 21), (S, W, 3, 10), (R, G, 1, 10), (R, G, 1, 15), (R, W, 3, 8), (R, W, 3, 20),
    (R, W, 3, 13), (R, W, 3, 25), (S, G, 1, 22), (S, G, 1, 24), (S, W, 3, 32), (S, W, 3, 42), (S, W, 3, 28),
    (S, W, 3, 38), (R, G, 1, 2), (S, G, 1, 11), (R, G, 1, 1), (S, G, 1, 14), (R, W, 3, 14), (R, W, 3, 27),
    (R, W, 3, 9), (R, W, 3, 22), (S, W, 3, 23), (S, W, 3, 17), (S, W, 3, 18), (S, W, 3, 12), (R, G, 1, 11),
    (R, G, 1, 14), (S, W, 3, 41), (S, W, 3, 33), (S, W, 3, 37), (S, W, 3, 29), (S, G, 1, 6), (S, G, 1, 5),
    (LIFT, ((0, 0), (-1, 0), (1, 0)), 0), (R, W, 3, 16), (R, W, 3, 24), (R, W, 3, 11), (R, W, 3, 19), (R, G, 1, 4),
    (S, G, 1, 12), (R, G, 1, 7), (S, G, 1, 17), (S, W, 3, 34), (S, W, 3, 43), (S, W, 3, 30), (S, W, 3, 39),
    (LIFT, ((0, 0), (-1, 0), (1, 0)), 1), (R, W, 3, 26), (R, W, 3, 15), (R, W, 3, 21), (R, W, 3, 10), (R, G, 1, 12),
    (R, W, 3, 32), (R, W, 3, 42), (R, W, 3, 28), (R, W, 3, 38), (R, G, 1, 17), (S, G, 1, 23), (S, G, 1, 25),
    (S, W, 3, 35), (S, W, 3, 40), (S, W, 3, 31), (S, W, 3, 36), (R, G, 1, 22), (S, G, 1, 18), (R, G, 1, 24),
    (S, G, 1, 19), (R, W, 3, 23), (R, W, 3, 17), (R, W, 3, 18), (R, W, 3, 12), (S, W, 3, 45), (S, W, 3, 47),
    (S, W, 3, 44), (S, W, 3, 46), (PRODUCT, 1, ((1, 0), (-1, 0)), 0), (R, G, 1, 18), (R, G, 1, 19),
    (LIFT, ((2, 0),), 0), (R, W, 3, 41), (R, W, 3, 33), (R, W, 3, 37), (R, W, 3, 29), (LIFT, ((2, 0),), 1),
    (R, C, 1, 1, 0, 0), (R, C, 1, 2, 0, 0), (R, G, 1, 6), (S, G, 1, 13), (R, G, 1, 5), (S, G, 1, 16),
    (FREE, 1, 0, 0, 1), (S, X, 1, 0, 0, 3), (FREE, 1, 0, 0, 2), (S, X, 1, 0, 0, 4), (R, W, 3, 34), (R, W, 3, 43),
    (R, W, 3, 30), (R, W, 3, 39), (PRODUCT, 1, ((2, 0),), 0), (R, G, 1, 13), (R, W, 3, 35), (R, W, 3, 40),
    (R, W, 3, 31), (R, W, 3, 36), (R, G, 1, 16), (LIFT, ((0, 1), (-1, 1), (1, 1)), 0), (R, C, 1, 0, 0, 0),
    (R, G, 1, 23), (S, G, 1, 20), (R, G, 1, 25), (S, G, 1, 21), (FAR, 1, 0, 0), (S, X, 1, 0, 0, 0),
    (S, X, 1, 0, 0, 1), (R, W, 3, 45), (R, W, 3, 47), (R, W, 3, 44), (R, W, 3, 46), (PRODUCT, 1, ((2, 0),), 1),
    (PRODUCT, 1, ((1, 0), (-1, 0)), 1), (R, X, 1, 0, 0, 3), (R, X, 1, 0, 0, 4), (R, G, 1, 20),
    (LIFT, ((0, 1), (-1, 1), (1, 1)), 1), (R, G, 1, 21), (R, C, 1, 0, 0, 1), (FAR, 1, 0, 1), (S, X, 1, 0, 1, 0),
    (S, X, 1, 0, 1, 1), (LIFT, ((2, 1),), 0), (R, C, 1, 1, 0, 1), (R, C, 1, 2, 0, 1), (FREE, 1, 0, 1, 1),
    (S, X, 1, 0, 1, 3), (FREE, 1, 0, 1, 2), (S, X, 1, 0, 1, 4), (LIFT, ((2, 1),), 1), (R, X, 1, 0, 0, 0),
    (R, X, 1, 0, 0, 1), (NEAR, 1, 0, 0, 1), (NEAR, 1, 0, 0, 2), (S, X, 1, 0, 0, 2), (S, X, 1, 0, 0, 5),
    (PRODUCT, 1, ((2, 1),), 0), (PRODUCT, 1, ((2, 1),), 1), (PRODUCT, 1, ((1, 1), (-1, 1)), 0), (R, C, 1, 0, 1, 0),
    (FAR, 1, 1, 0), (S, X, 1, 1, 0, 0), (S, X, 1, 1, 0, 1), (PRODUCT, 1, ((1, 1), (-1, 1)), 1), (R, X, 1, 0, 1, 0),
    (R, X, 1, 0, 1, 1), (R, C, 1, 0, 1, 1), (FAR, 1, 1, 1), (S, X, 1, 1, 1, 0), (S, X, 1, 1, 1, 1),
    (NEAR, 1, 0, 1, 1), (NEAR, 1, 0, 1, 2), (PRODUCT, 1, ((0, 0), (0, 1)), 0), (R, C, 1, 1, 1, 0), (R, C, 1, 2, 1, 0),
    (R, X, 1, 0, 1, 3), (R, X, 1, 0, 1, 4), (FREE, 1, 1, 0, 1), (FREE, 1, 1, 0, 2), (S, X, 1, 0, 1, 2),
    (S, X, 1, 0, 1, 5), (PRODUCT, 1, ((0, 0), (0, 1)), 1), (R, C, 1, 1, 1, 1), (R, C, 1, 2, 1, 1), (FREE, 1, 1, 1, 1),
    (FREE, 1, 1, 1, 2), (R, X, 1, 0, 0, 2), (R, X, 1, 0, 0, 5), (R, C, 1, 3, 0, 0), (FINISH, 0, 0),
    (R, C, 1, 3, 1, 0), (S, X, 1, 1, 0, 3), (S, X, 1, 1, 0, 4), (R, C, 1, 3, 0, 1), (R, X, 1, 1, 0, 0),
    (R, X, 1, 1, 0, 1), (NEAR, 1, 1, 0, 1), (NEAR, 1, 1, 0, 2), (R, C, 1, 3, 1, 1), (S, X, 1, 1, 0, 2),
    (S, X, 1, 1, 0, 5), (R, X, 1, 1, 1, 0), (R, X, 1, 1, 1, 1), (NEAR, 1, 1, 1, 1), (NEAR, 1, 1, 1, 2),
    (S, X, 1, 1, 1, 2), (S, X, 1, 1, 1, 5), (R, X, 1, 0, 1, 2), (R, X, 1, 0, 1, 5), (FINISH, 0, 1),
    (S, X, 1, 1, 1, 3), (S, X, 1, 1, 1, 4), (R, X, 1, 1, 0, 3), (R, X, 1, 1, 0, 4), (R, X, 1, 1, 0, 2),
    (R, X, 1, 1, 0, 5), (FINISH, 1, 0), (R, X, 1, 1, 1, 2), (R, X, 1, 1, 1, 5), (R, X, 1, 1, 1, 3),
    (R, X, 1, 1, 1, 4), (FINISH, 1, 1),
)


def way_of(key):
    if key[0] == W:
        return MESSAGES[key[1]][key[2]][3]
    if key[0] == G:
        return GATHER[key[2]][3]
    if key[0] == C:
        return "d"
    return ("x+", "x-", "x+", "x+", "x-", "x-")[key[4]]


def share():
    sent, waited = {}, {}
    for i, (name, *which) in enumerate(SCHEDULE):
        if name == S:
            sent[tuple(which)] = i
        elif name == R:
            waited[tuple(which)] = i
        elif name == PRODUCT:
            g, cases, j = which
            for dx, h in cases:
                sent[(C, g, TURN[dx], h, j)] = i
    back = {"x+": "x-", "x-": "x+", "y+": "y-", "y-": "y+", "z+": "z-", "z-": "z+", "d": "d"}
    last, place = [], {}
    for key in sorted(sent, key=lambda k: (sent[k], k)):
        toward = [k for k in sent if way_of(k) == back[way_of(key)] and waited[k] < sent[key]]
        heard = max([sent[k] for k in toward], default=-1)
        free = [(at, n) for n, at in enumerate(last) if at < heard]
        if free:
            n = max(free)[1]
            last[n] = waited[key]
        else:
            n = len(last)
            last.append(waited[key])
        place[key] = n
    return place, len(last)


SEMAPHORE, SEMAPHORES = share()


def kernel(
    resid, mix_gain, wq, wk, wv, wg, wo, rate, mlp_gain, wu, wd,
    out,
    w_in, w_out, w_up, w_down, xn, rbuf, after, proj, gated, hid, decay, kept,
    dout, din, sout, rin2, rin1,
    local_sem, w_send, g_send, d_send, s_send, recv,
):
    fs, tp = lax.axis_index("fs"), lax.axis_index("tp")
    z, y, x, c = fs // RING, fs % RING, tp // 2, tp % 2

    def turn(v, d):
        return (v + d + RING) % RING

    device = {
        "y+": (z * RING + turn(y, 1), tp),
        "y-": (z * RING + turn(y, -1), tp),
        "z+": (turn(z, 1) * RING + y, tp),
        "z-": (turn(z, -1) * RING + y, tp),
        "x+": (fs, turn(x, 1) * 2 + c),
        "x-": (fs, turn(x, -1) * 2 + c),
        "d": (fs, x * 2 + 1 - c),
    }

    def remote(src, dst, send, recv, way):
        return pltpu.make_async_remote_copy(
            src_ref=src, dst_ref=dst, send_sem=send, recv_sem=recv,
            device_id=device[way], device_id_type=MESH,
        )

    def send(*args):
        remote(*args).start()

    weights = (w_in, w_out, w_up, w_down)

    def block(dy, dz):
        return turn(z, dz) * RING + turn(y, dy)

    def piece(t, dy, dz, part):
        ref = weights[t]
        f = block(dy, dz)
        if part == "full":
            return ref.at[f]
        if part in ("A", "B"):
            return ref.at[f, :, "AB".index(part)]
        if part in ("h0", "h1"):
            return ref.at[f, int(part[1])]
        return ref.at[f, int(part[2]), "AB".index(part[0])]

    def w_copy(t, n, place):
        dy, dz, part, way = place
        ref = piece(t, dy, dz, part)
        return (ref, ref, w_send.at[t], recv.at[SEMAPHORE[W, t, n]], way)

    def g_copy(g, n, dx, core):
        h, q, way = GATHER[n][1:]
        block = turn(x, dx) * 2 + core
        ref = xn.at[g, block, h] if q is None else xn.at[g, block, h, q]
        return (ref, ref, g_send.at[g], recv.at[SEMAPHORE[G, g, n]], way)

    def rows16(count, body):
        def step(i, carry):
            body(pl.ds(pl.multiple_of(i * 16, 16), 16))
            return carry

        lax.fori_loop(0, count // 16, step, 0)

    def of(ref, j, g):
        return ref if g == 0 else ref.at[:, pl.ds(j * 1024, 1024)]

    def d_copy(g, k, h, j):
        columns = slice(None) if g == 0 else pl.ds(j * 1024, 1024)
        return (
            dout.at[g, k, h, :, :, columns], din.at[g, k, h, :, :, columns],
            d_send.at[g], recv.at[SEMAPHORE[C, g, k, h, j]], "d",
        )

    def s_copy(g, h, j, n):
        if n < 2:
            src, dst, way = sout.at[g, 0, h, n], rin2.at[g, h, n], ("x+", "x-")[n]
        elif n < 4:
            src, dst, way = sout.at[g, 1, h, n - 2], rin1.at[g, 0, h, n - 2], "x+"
        else:
            src, dst, way = sout.at[g, 2, h, n - 4], rin1.at[g, 1, h, n - 4], "x-"
        return (of(src, j, g), of(dst, j, g), s_send.at[g], recv.at[SEMAPHORE[X, g, h, j, n]], way)

    def start(kind, *which):
        if kind == W:
            t, n = which
            send(*w_copy(t, n, MESSAGES[t][n]))
        elif kind == G:
            g, n = which
            send(*g_copy(g, n, GATHER[n][0], c))
        else:
            send(*s_copy(*which))

    def receive(kind, *which):
        if kind == W:
            t, n = which
            copy = w_copy(t, n, arrived(MESSAGES[t][n]))
        elif kind == G:
            g, n = which
            dx, way = GATHER[n][0], GATHER[n][3]
            if way == "d":
                copy = g_copy(g, n, dx, 1 - c)
            else:
                copy = g_copy(g, n, near(dx - (1 if way == "x+" else -1)), c)
        elif kind == C:
            copy = d_copy(*which)
        else:
            copy = s_copy(*which)
        remote(*copy).wait_recv()

    def product(g, cases, lhs, w, columns):
        rows = jnp.concatenate([block for case in cases for block in lhs(*case)], axis=0)
        o = jnp.dot(rows, w, preferred_element_type=F32)
        for n, (dx, h) in enumerate(cases):
            mine = o[n * 128 : (n + 1) * 128]
            dout[g, TURN[dx], h, :, :, columns] = mine[:64].astype(BF16).reshape(2, 32, 512)
            kept[TURN[dx], h, :, :, columns] = mine[64:].reshape(2, 32, 512)

    def partial(g, cases, j):
        if g == 0:
            depth = wo.shape[0] * wo.shape[1] * wo.shape[2]

            def step(i, carry):
                w = [w_out[4 * i + n].reshape(depth, 128) for n in range(4)]
                columns = pl.ds(pl.multiple_of(i * 512, 512), 512)
                product(0, cases, gated_rows, jnp.concatenate(w, axis=1), columns)
                return carry

            lax.fori_loop(0, 4, step, 0)
        else:
            depth = wd.shape[0] * wd.shape[1] * wd.shape[2]
            for i in (2 * j, 2 * j + 1):
                w = [w_down[block(*PLACES[4 * i + n])].reshape(depth, 128) for n in range(4)]
                columns = slice(i * 512, (i + 1) * 512)
                product(1, cases, hidden_rows, jnp.concatenate(w, axis=1), columns)
        for dx, h in cases:
            send(*d_copy(g, TURN[dx], h, j))

    def add_quarter(g, k, h, j, q, extra=False):
        columns = slice(None) if g == 0 else slice(j * 1024, (j + 1) * 1024)

        def body(rows):
            total = kept[k, h, q, rows, columns] + din[g, k, h, q, rows, columns].astype(F32)
            if extra:
                total = total + rin2[g, h, q, rows, columns].astype(F32)
            sout[g, k, h, q, rows, columns] = total.astype(BF16)

        rows16(32, body)

    def add_far(g, h, j):
        for q in (0, 1):
            add_quarter(g, 0, h, j, q)

    def add_free(g, h, j, k):
        add_quarter(g, k, h, j, 1 if k == 1 else 0)

    def add_near(g, h, j, k):
        add_quarter(g, k, h, j, 0 if k == 1 else 1, True)

    def sum_rows(h, q, rows):
        total = kept[3, h, q, rows, :] + din[0, 3, h, q, rows, :].astype(F32)
        return total + rin1[0, 0, h, q, rows, :].astype(F32) + rin1[0, 1, h, q, rows, :].astype(F32)

    def normed(values, gain):
        scale = lax.rsqrt(jnp.mean(values * values, axis=-1, keepdims=True) + EPS)
        return (values * scale * gain).astype(BF16)

    loads = []

    def load(src, dst):
        copy = pltpu.make_async_copy(src, dst, local_sem.at[len(loads)])
        copy.start()
        return copy

    for src, low, wide in ((wq, 0, 128), (wk, 128, 128), (wv, 256, 256), (wg, 512, 256)):
        load(src, w_in.at[fs, :, :, :, low : low + wide])
    loads.append(pltpu.make_async_copy(w_in.at[fs], w_in.at[fs], local_sem.at[0]))
    for src, dst in ((resid, rbuf), (wo, w_out.at[fs]), (wu, w_up.at[fs]), (wd, w_down.at[fs])):
        loads.append(load(src, dst))
    barrier = pltpu.get_barrier_semaphore()
    for way in device:
        pl.semaphore_signal(barrier, inc=1, device_id=device[way], device_id_type=MESH)
    for copy in loads[:2]:
        copy.wait()
    for h in (0, 1):
        for q in (0, 1):
            def first_norm(rows):
                xn[0, tp, h, q, rows, :] = normed(rbuf[h, q, rows, :].astype(F32), mix_gain[...])

            rows16(32, first_norm)
    pl.semaphore_wait(barrier, 7)
    r = rate[0]

    def make_decay():
        def some_rows(i, carry):
            rows = pl.ds(pl.multiple_of(i * 64, 64), 64)
            t = lax.broadcasted_iota(jnp.int32, (64, LENGTH), 0) + i * 64
            s = lax.broadcasted_iota(jnp.int32, (64, LENGTH), 1)
            gap = (t - s).astype(F32)
            value = jnp.exp(-r * jnp.maximum(gap, 0.0)) * DK ** (-0.5)
            decay[rows, :] = jnp.where(gap >= 0.0, value, 0.0)
            return carry

        lax.fori_loop(0, LENGTH // 64, some_rows, 0)

    own = x // 2
    sequence = (own, 1 - own)

    def project(seq, j):
        columns = slice(j * 256, (j + 1) * 256)
        lhs = xn[0, pl.ds(4 * seq, 4)].reshape(512, D)
        rhs = w_in[:, :, :, :, columns].reshape(D, 256)
        o = jnp.dot(lhs, rhs, preferred_element_type=F32).astype(BF16)
        proj[pl.ds(4 * seq, 4), :, columns] = o.reshape(4, 128, 256)

    def retain(seq):
        for i in (0, 1):
            mine = pl.ds(seq * 4 + 2 * i, 2)
            upto = pl.ds(seq * 4, 2 * i + 2)
            wide = 256 * (i + 1)
            q = proj[mine, :, 0:128].reshape(256, DK)
            k = proj[upto, :, 128:256].reshape(wide, DK)
            v = proj[upto, :, 256:512].reshape(wide, DV)
            scores = lax.dot_general(q, k, (((1,), (1,)), ((), ())), preferred_element_type=F32)
            scores = (scores * decay[i * 256 : (i + 1) * 256, 0:wide]).astype(BF16)
            mixed = jnp.dot(scores, v, preferred_element_type=F32)
            mixed = mixed - jnp.mean(mixed, axis=-1, keepdims=True)
            spread = jnp.mean(mixed * mixed, axis=-1, keepdims=True)
            gate = proj[mine, :, 512:768].reshape(256, DV).astype(F32)
            value = gate / (1.0 + jnp.exp(-gate)) * (mixed * lax.rsqrt(spread + EPS))
            gated[mine] = value.astype(BF16).reshape(2, 2, 64, DV)

    def gated_rows(dx, h):
        first = turn(x, dx) * 2
        return gated[first + 1 - c, h], gated[first + c, h]

    def lift(cases, half):
        def body(j, carry):
            columns = pl.ds(pl.multiple_of(j * 256, 256), 256)
            lhs = jnp.concatenate(
                [
                    xn[1, turn(x, dx) * 2 + core, h].reshape(64, D)
                    for dx, h in cases
                    for core in (1 - c, c)
                ],
                axis=0,
            )
            rhs = w_up[:, :, :, :, columns].reshape(D, 256)
            o = jnp.maximum(jnp.dot(lhs, rhs, preferred_element_type=F32), 0.0)
            o = (o * o).astype(BF16)
            for n, (dx, h) in enumerate(cases):
                hid[TURN[dx], h, :, columns] = o[n * 128 : (n + 1) * 128]
            return carry

        count = w_up.shape[4] // 512
        lax.fori_loop(half * count, (half + 1) * count, body, 0)

    def hidden_rows(dx, h):
        return (hid[TURN[dx], h],)

    def second_norm(h):
        for q in (0, 1):
            def body(rows):
                value = rbuf[h, q, rows, :].astype(F32) + sum_rows(h, q, rows)
                value = value.astype(BF16)
                after[h, q, rows, :] = value
                xn[1, tp, h, q, rows, :] = normed(value.astype(F32), mlp_gain[...])

            rows16(32, body)

    def finish(h, j):
        for i in range(8 * j, 8 * j + 8):
            here = pl.ds(pl.multiple_of(block(*PLACES[i]) * 128, 128), 128)
            at = slice(i * 128, (i + 1) * 128)
            total = after[h, :, :, here].astype(F32) + kept[3, h, :, :, at]
            total = total + din[1, 3, h, :, :, at].astype(F32)
            total = total + rin1[1, 0, h, :, :, at].astype(F32) + rin1[1, 1, h, :, :, at].astype(F32)
            out[h, :, :, here] = total.astype(BF16)

    actions = {
        S: start,
        R: receive,
        DECAY: make_decay,
        PROJECT: lambda which, j: project(sequence[which], j),
        RETAIN: lambda which: retain(sequence[which]),
        PRODUCT: partial,
        FAR: add_far,
        FREE: add_free,
        NEAR: add_near,
        NORM: second_norm,
        LIFT: lift,
        FINISH: finish,
    }
    for copy in loads[2:]:
        copy.wait()
    for name, *which in SCHEDULE:
        actions[name](*which)
    for t in range(4):
        ref = weights[t].at[0:15]
        remote(ref, ref, w_send.at[t], recv.at[0], "d").wait_send()
    for g in (0, 1):
        remote(xn.at[g, 0:7], xn.at[g, 0:7], g_send.at[g], recv.at[0], "d").wait_send()
        remote(dout.at[g], din.at[g], d_send.at[g], recv.at[0], "d").wait_send()
        remote(sout.at[g], sout.at[g], s_send.at[g], recv.at[0], "d").wait_send()


def on_device(
    resid, mix_gain, w_query, w_key, w_value, w_gate, w_output, decay_rate, mlp_gain, w_up, w_down
):
    def cut(w):
        return w.reshape(2, 2, w.shape[0] // 4, w.shape[1])

    wide = w_query.shape[1] + w_key.shape[1] + w_value.shape[1] + w_gate.shape[1]
    count = RING * RING

    def held(rows, columns):
        return pltpu.VMEM((count, 2, 2, rows // 4, columns), BF16)

    dma = pltpu.SemaphoreType.DMA
    vmem = pl.BlockSpec(memory_space=pltpu.VMEM)
    hbm = pl.BlockSpec(memory_space=pltpu.HBM)
    tokens = (2, 2, 32, D)
    result = pl.pallas_call(
        kernel,
        out_shape=pltpu.VMEM(tokens, BF16),
        in_specs=[
            hbm, vmem, hbm, hbm, hbm, hbm, hbm,
            pl.BlockSpec(memory_space=pltpu.SMEM), vmem, hbm, hbm,
        ],
        out_specs=vmem,
        scratch_shapes=[
            held(128, wide),
            held(w_output.shape[0], 128),
            held(128, w_up.shape[1]),
            held(w_down.shape[0], 128),
            pltpu.VMEM((2, 8) + tokens, BF16),
            pltpu.VMEM(tokens, BF16),
            pltpu.VMEM(tokens, BF16),
            pltpu.VMEM((8, 128, wide), BF16),
            pltpu.VMEM((8, 2, 64, DV), BF16),
            pltpu.VMEM((4, 2, 128, w_up.shape[1]), BF16),
            pltpu.VMEM((LENGTH, LENGTH), F32),
            pltpu.VMEM((4,) + tokens, F32),
            pltpu.VMEM((2, 4) + tokens, BF16),
            pltpu.VMEM((2, 4) + tokens, BF16),
            pltpu.VMEM((2, 3) + tokens, BF16),
            pltpu.VMEM((2,) + tokens, BF16),
            pltpu.VMEM((2, 2) + tokens, BF16),
            dma((5,)),
            dma((4,)),
            dma((2,)),
            dma((2,)),
            dma((2,)),
            dma((SEMAPHORES,)),
        ],
        compiler_params=pltpu.CompilerParams(
            collective_id=0, has_side_effects=True, vmem_limit_bytes=66060288
        ),
    )(
        resid.reshape(tokens), mix_gain[None], cut(w_query), cut(w_key), cut(w_value), cut(w_gate),
        cut(w_output), decay_rate, mlp_gain[None], cut(w_up), cut(w_down),
    )
    return result.reshape(resid.shape)


def solution(mesh):
    placed = (
        P(("fs", "tp"), None),
        P(),
        P("fs", "tp"),
        P("fs", "tp"),
        P("fs", "tp"),
        P("fs", "tp"),
        P("tp", "fs"),
        P("tp"),
        P(),
        P("fs", "tp"),
        P("tp", "fs"),
    )
    return jax.shard_map(
        on_device, mesh=mesh, in_specs=placed, out_specs=P(("fs", "tp"), None), check_vma=False
    )
```

time: 102 us -> 95.7 us (0.938)
  Pallas kernels: 98.9 us -> 94.1 us
  local copies, waits for them, and re-layouts: 1.88 us -> 0.8 us
    pallas_call x1, Pallas kernels: 98.9 us -> 94.1 us  [on_device(): pl.pallas_call(kernel, out_shape=pltpu.VMEM(tokens, BF16), in_specs=[hbm,...]
    unnamed x1, local copies, waits for them, and re-layouts: 1.88 us -> 0.8 us
where the time goes in v4:
time: 95.7 us; the launch traced here: 95.5 us
  Pallas kernels  94.1 us (98%)
    pallas_call x1, Pallas kernels, on_device(): pl.pallas_call(kernel, out_shape=pltpu.VMEM(tokens, BF16), in_specs=[hbm,...  94.1 us

profile of v4, /device:TPU:1, one launch (start us, length us, event | category | flops | bytes accessed | tf_op | source)
XLA Modules:
  0.0 95.5 jit_solution(15238751706060064821)
XLA Ops:
  0.7 94.1 %shard_map.109 = bf16[2,2,32,2048]{3,2,1,0:T(8,128)(2,1)S(1)} custom-call(bf16[2,2,32,2048]{3,2,1,0:T(8,128)(2,1)} %bitcast.12, f32[1,2048]{1,0:T(1,128)} %bitcast.20, bf16[2,2,32,128]{3,2,1,0:T(8,128)(2,1)} %bitcast.18, bf16[2,2,32,128]{3,2,1,0:T(8,128)(2,1)} %bitcast.19, bf16[2,2,32,256]{3,2,1,0:T(8,128)(2,1)} %bitcast.15, ...), custom_call_target="tpu_custom_call" | custom-call | tf_op jit(solution)/shard_map/pallas_call | solution.py:535
  94.7 0.8 copy.13

commit v5 on v4

v5 whole, which is shorter than its diff:
```python
import jax
import jax.numpy as jnp
from jax import lax
from jax.experimental import pallas as pl
from jax.experimental.pallas import tpu as pltpu
from jax.sharding import PartitionSpec as P

D = 2048
DK = 128
DV = 256
LENGTH = 512
RING = 4
EPS = 1e-06
MESH = pl.DeviceIdType.MESH
F32 = jnp.float32
BF16 = jnp.bfloat16

STEP = {"y+": (1, 0), "y-": (-1, 0), "z+": (0, 1), "z-": (0, -1)}


def near(d):
    return {0: 0, 1: 1, 2: 2, 3: -1}[d % RING]


def arrived(message):
    dy, dz, part, way = message
    return near(dy - STEP[way][0]), near(dz - STEP[way][1]), part, way


def onward(message):
    dy, dz, part, way = arrived(message)
    half = "0" if way[1] == "+" else "1"
    along = way[0] == "y"
    across = ("z+", "z-") if along else ("y+", "y-")
    first = "A" if along else "B"
    if part == "full":
        return [(dy, dz, "h" + half, way)] + [(dy, dz, first, w) for w in across]
    if part in ("h0", "h1"):
        onto = [(dy, dz, part, way)] if (dy if along else dz) != 2 and part[1] == half else []
        return onto + [(dy, dz, first + part, w) for w in across]
    if part in ("A", "B"):
        return [(dy, dz, part + "h" + half, way)]
    if (dy if way[0] == "y" else dz) != 2 and part[-1] == half:
        return [(dy, dz, part, way)]
    return []


def plan(parts):
    messages = [(0, 0, part, way) for part in parts for way in ("y+", "y-", "z+", "z-")]
    for message in messages:
        messages += onward(message)
    return messages


MESSAGES = [plan(parts) for parts in (("h0", "h1"), ("full",), ("full",), ("full",))]
PLACES = (
    (0, 0), (1, 0), (-1, 0), (0, 1), (0, -1), (2, 0), (0, 2), (1, 1),
    (1, -1), (-1, 1), (-1, -1), (2, 1), (2, -1), (1, 2), (-1, 2), (2, 2),
)

GATHER = (
    [(0, h, q, w) for h in (0, 1) for q in (0, 1) for w in ("x+", "x-")]
    + [(0, h, None, "d") for h in (0, 1)]
    + [(dx, h, q, "d") for dx in (-1, 1, 2) for h in (0, 1) for q in (0, 1)]
    + [(-1, h, 0, "x+") for h in (0, 1)]
    + [(1, h, 1, "x-") for h in (0, 1)]
)
TURN = {2: 0, 1: 1, -1: 2, 0: 3}

S, R, W, G, C, X = range(6)
DECAY, PROJECT, RETAIN, PRODUCT, FAR, FREE, NEAR, NORM, LIFT, FINISH = range(6, 16)
SCHEDULE = (
    (S, W, 0, 0), (S, W, 1, 1), (S, W, 0, 5), (S, W, 0, 2), (S, W, 1, 3), (S, W, 0, 7), (S, G, 0, 0), (S, G, 0, 3),
    (S, G, 0, 8), (S, G, 0, 9), (DECAY,), (S, W, 1, 0), (S, W, 1, 2), (R, G, 0, 8), (S, W, 0, 4), (S, W, 0, 1),
    (S, W, 0, 6), (S, W, 0, 3), (R, G, 0, 9), (S, G, 0, 2), (S, G, 0, 1), (R, W, 1, 1), (R, W, 1, 3), (S, W, 1, 14),
    (S, W, 1, 7), (S, W, 1, 8), (S, W, 1, 13), (R, W, 0, 0), (R, W, 0, 2), (S, W, 0, 8), (S, W, 1, 15), (S, W, 0, 13),
    (S, W, 1, 9), (R, G, 0, 0), (S, G, 0, 10), (R, G, 0, 3), (S, G, 0, 15), (S, G, 0, 22), (S, G, 0, 24),
    (S, W, 0, 15), (S, W, 0, 10), (R, W, 0, 5), (R, W, 0, 7), (R, W, 1, 0), (R, W, 1, 2), (S, W, 0, 20),
    (S, W, 0, 25), (R, G, 0, 10), (S, W, 1, 4), (S, W, 1, 10), (R, G, 0, 15), (S, W, 1, 11), (S, W, 1, 5),
    (R, W, 0, 4), (R, W, 0, 1), (R, W, 0, 6), (R, W, 0, 3), (R, G, 0, 2), (S, G, 0, 11), (R, G, 0, 1), (S, G, 0, 14),
    (S, G, 0, 4), (S, G, 0, 7), (S, W, 0, 16), (S, W, 0, 11), (S, W, 0, 27), (S, W, 1, 6), (R, W, 1, 14),
    (R, W, 1, 7), (R, W, 1, 8), (R, W, 1, 13), (S, W, 0, 14), (S, W, 0, 9), (S, W, 0, 22), (R, G, 0, 11),
    (R, W, 1, 15), (R, W, 1, 9), (S, W, 1, 12), (R, G, 0, 14), (S, W, 1, 30), (S, W, 0, 24), (S, W, 0, 18),
    (S, W, 1, 21), (R, W, 0, 15), (R, W, 0, 10), (S, W, 0, 26), (S, W, 0, 12), (R, W, 0, 8), (R, W, 0, 13),
    (R, G, 0, 22), (S, G, 0, 18), (R, G, 0, 24), (S, G, 0, 19), (S, G, 0, 6), (S, G, 0, 5), (S, W, 1, 29),
    (S, W, 0, 28), (R, W, 1, 4), (R, W, 1, 10), (S, W, 1, 24), (S, W, 1, 25), (S, W, 0, 19), (S, W, 0, 32),
    (S, W, 0, 33), (R, G, 0, 18), (R, W, 1, 11), (R, W, 1, 5), (S, W, 1, 18), (R, G, 0, 19), (R, W, 0, 20),
    (R, W, 0, 25), (S, W, 1, 16), (S, W, 0, 38), (S, W, 0, 23), (S, W, 0, 42), (S, W, 0, 37), (R, W, 0, 16),
    (R, W, 0, 11), (R, W, 1, 6), (R, G, 0, 4), (S, G, 0, 12), (R, G, 0, 7), (S, G, 0, 17), (R, W, 0, 27),
    (S, G, 0, 23), (S, G, 0, 25), (S, W, 1, 19), (S, W, 0, 35), (S, W, 1, 31), (S, W, 0, 31), (S, W, 1, 23),
    (R, W, 0, 14), (R, W, 0, 9), (R, W, 0, 22), (R, W, 1, 12), (S, W, 1, 27), (S, W, 0, 39), (R, W, 1, 30),
    (R, W, 1, 21), (S, W, 0, 17), (R, G, 0, 12), (S, W, 0, 34), (S, W, 0, 30), (R, G, 0, 17), (R, W, 0, 24),
    (R, W, 0, 18), (S, W, 1, 33), (R, W, 1, 29), (R, W, 0, 26), (R, W, 0, 12), (S, W, 0, 40), (S, W, 0, 29),
    (R, W, 1, 25), (R, W, 1, 24), (S, W, 1, 34), (S, W, 0, 21), (R, W, 0, 28), (R, G, 0, 6), (S, G, 0, 13),
    (R, G, 0, 5), (S, G, 0, 16), (S, W, 1, 28), (R, W, 1, 18), (R, W, 0, 19), (S, W, 0, 41), (S, W, 1, 35),
    (S, W, 0, 36), (R, W, 0, 33), (R, W, 1, 16), (R, W, 0, 32), (S, W, 0, 43), (S, W, 0, 44), (R, G, 0, 13),
    (R, W, 0, 38), (S, W, 0, 45), (S, W, 0, 46), (R, G, 0, 16), (R, W, 0, 42), (R, W, 0, 37), (R, W, 0, 23),
    (R, W, 1, 19), (S, W, 0, 47), (S, W, 1, 32), (R, W, 1, 31), (R, W, 1, 23), (S, W, 1, 22), (R, W, 1, 27),
    (S, W, 1, 26), (S, W, 1, 20), (S, W, 1, 17), (R, W, 0, 31), (R, W, 0, 35), (R, G, 0, 23), (S, G, 0, 20),
    (R, G, 0, 25), (S, G, 0, 21), (S, W, 2, 0), (S, W, 2, 1), (S, W, 2, 2), (S, W, 2, 3), (R, W, 0, 39),
    (R, W, 0, 17), (R, W, 1, 33), (R, W, 0, 30), (R, W, 0, 34), (R, G, 0, 20), (R, W, 1, 34), (R, G, 0, 21),
    (R, W, 0, 40), (R, W, 0, 29), (R, W, 1, 28), (R, W, 1, 35), (R, W, 0, 21), (R, W, 0, 41), (R, W, 0, 36),
    (R, W, 0, 43), (PROJECT, 1, 0), (R, W, 0, 44), (R, W, 1, 32), (R, W, 1, 22), (R, W, 0, 45), (R, W, 0, 46),
    (R, W, 0, 47), (R, W, 1, 20), (R, W, 1, 26), (R, W, 1, 17), (PROJECT, 1, 1), (S, W, 3, 0), (S, W, 3, 1),
    (S, W, 3, 2), (S, W, 3, 3), (RETAIN, 1), (PRODUCT, 0, ((2, 0), (2, 1)), 0), (PRODUCT, 0, ((2, 0), (2, 1)), 1),
    (PROJECT, 0, 0), (R, C, 0, 0, 0, 0), (R, C, 0, 0, 1, 0), (R, C, 0, 0, 0, 1), (R, C, 0, 0, 1, 1), (FAR, 0, 0, 0),
    (S, X, 0, 0, 0, 0), (S, X, 0, 0, 0, 1), (FAR, 0, 1, 0), (FAR, 0, 0, 1), (FAR, 0, 1, 1), (PROJECT, 0, 1),
    (R, W, 2, 1), (R, W, 2, 2), (R, W, 2, 0), (R, W, 2, 3), (S, X, 0, 1, 0, 0), (S, X, 0, 1, 0, 1), (RETAIN, 0),
    (S, W, 2, 4), (S, W, 2, 12), (S, W, 2, 8), (S, W, 2, 13), (PRODUCT, 0, ((1, 0), (-1, 0)), 0), (S, X, 0, 0, 1, 0),
    (S, X, 0, 0, 1, 1), (PRODUCT, 0, ((1, 1), (-1, 1)), 0), (PRODUCT, 0, ((1, 0), (-1, 0)), 1),
    (PRODUCT, 0, ((1, 1), (-1, 1)), 1), (S, X, 0, 1, 1, 0), (S, X, 0, 1, 1, 1), (PRODUCT, 0, ((0, 0), (0, 1)), 0),
    (R, C, 0, 1, 0, 0), (R, X, 0, 0, 0, 0), (R, X, 0, 0, 0, 1), (R, C, 0, 2, 0, 0), (FREE, 0, 0, 0, 1),
    (FREE, 0, 0, 0, 2), (NEAR, 0, 0, 0, 1), (NEAR, 0, 0, 0, 2), (PRODUCT, 0, ((0, 0), (0, 1)), 1), (R, C, 0, 1, 1, 0),
    (R, C, 0, 2, 1, 0), (FREE, 0, 1, 0, 1), (FREE, 0, 1, 0, 2), (R, C, 0, 1, 0, 1), (FREE, 0, 0, 1, 1),
    (R, C, 0, 2, 0, 1), (FREE, 0, 0, 1, 2), (S, W, 2, 14), (S, W, 2, 7), (S, W, 2, 10), (S, W, 2, 6),
    (R, C, 0, 1, 1, 1), (FREE, 0, 1, 1, 1), (R, X, 0, 1, 0, 0), (R, X, 0, 1, 0, 1), (NEAR, 0, 1, 0, 1),
    (S, X, 0, 0, 0, 2), (S, X, 0, 0, 0, 5), (NEAR, 0, 1, 0, 2), (R, C, 0, 2, 1, 1), (FREE, 0, 1, 1, 2),
    (R, C, 0, 3, 0, 0), (R, C, 0, 3, 1, 0), (R, W, 3, 0), (R, W, 3, 1), (R, W, 3, 2), (R, W, 3, 3),
    (R, C, 0, 3, 0, 1), (R, C, 0, 3, 1, 1), (R, X, 0, 0, 1, 0), (R, X, 0, 0, 1, 1), (NEAR, 0, 0, 1, 1),
    (S, X, 0, 0, 1, 2), (S, X, 0, 0, 0, 4), (NEAR, 0, 0, 1, 2), (S, W, 2, 11), (S, W, 2, 15), (S, W, 2, 5),
    (S, W, 2, 9), (R, X, 0, 1, 1, 0), (R, X, 0, 1, 1, 1), (NEAR, 0, 1, 1, 1), (S, X, 0, 0, 0, 3), (S, X, 0, 0, 1, 5),
    (NEAR, 0, 1, 1, 2), (R, W, 2, 4), (R, W, 2, 12), (R, W, 2, 8), (R, W, 2, 13), (R, X, 0, 0, 0, 2),
    (R, X, 0, 0, 0, 5), (S, X, 0, 0, 1, 3), (S, X, 0, 0, 1, 4), (S, W, 2, 28), (S, W, 2, 29), (S, W, 2, 16),
    (S, W, 2, 17), (R, X, 0, 0, 1, 2), (R, X, 0, 0, 0, 4), (S, X, 0, 1, 0, 2), (S, X, 0, 1, 0, 5), (R, W, 2, 14),
    (R, W, 2, 7), (R, W, 2, 10), (R, W, 2, 6), (S, W, 2, 24), (S, W, 2, 25), (S, W, 2, 22), (S, W, 2, 21),
    (R, X, 0, 0, 0, 3), (R, X, 0, 0, 1, 5), (S, X, 0, 1, 1, 2), (S, X, 0, 1, 1, 5), (S, W, 2, 30), (S, W, 2, 27),
    (S, W, 2, 20), (S, W, 2, 19), (R, X, 0, 0, 1, 3), (R, X, 0, 0, 1, 4), (S, X, 0, 1, 0, 3), (S, X, 0, 1, 0, 4),
    (NORM, 0), (S, G, 1, 8), (R, W, 2, 11), (R, W, 2, 15), (R, W, 2, 5), (R, W, 2, 9), (S, W, 2, 26), (S, W, 2, 31),
    (S, W, 2, 18), (S, W, 2, 23), (R, X, 0, 1, 0, 2), (R, X, 0, 1, 0, 5), (S, X, 0, 1, 1, 3), (S, X, 0, 1, 1, 4),
    (R, G, 1, 8), (R, W, 2, 28), (R, W, 2, 29), (R, W, 2, 16), (R, W, 2, 17), (S, W, 3, 4), (S, W, 2, 35),
    (S, W, 2, 32), (S, W, 3, 13), (R, X, 0, 1, 1, 2), (R, X, 0, 1, 1, 5), (S, G, 1, 0), (S, G, 1, 3), (R, W, 2, 24),
    (R, W, 2, 25), (R, W, 2, 22), (R, W, 2, 21), (S, W, 3, 7), (S, W, 3, 10), (R, X, 0, 1, 0, 3), (R, X, 0, 1, 0, 4),
    (R, W, 2, 30), (R, W, 2, 27), (R, W, 2, 20), (R, W, 2, 19), (S, W, 2, 34), (S, W, 2, 33), (R, X, 0, 1, 1, 3),
    (R, X, 0, 1, 1, 4), (S, G, 1, 2), (S, G, 1, 1), (NORM, 1), (S, G, 1, 9), (R, W, 2, 26), (R, W, 2, 31),
    (R, W, 2, 18), (R, W, 2, 23), (S, W, 3, 11), (S, W, 3, 15), (S, W, 3, 8), (S, W, 3, 9), (R, G, 1, 9),
    (R, W, 2, 35), (R, W, 2, 32), (R, G, 1, 0), (S, G, 1, 10), (R, G, 1, 3), (S, G, 1, 15), (S, G, 1, 22),
    (S, G, 1, 24), (R, W, 3, 4), (R, W, 3, 13), (S, W, 3, 14), (S, W, 3, 29), (S, W, 3, 16), (S, W, 3, 6),
    (R, G, 1, 10), (R, G, 1, 15), (R, W, 3, 7), (R, W, 3, 10), (R, W, 2, 34), (R, W, 2, 33), (S, W, 3, 12),
    (S, W, 3, 5), (R, G, 1, 2), (S, G, 1, 11), (R, G, 1, 1), (S, G, 1, 14), (S, G, 1, 4), (S, G, 1, 7), (S, W, 3, 24),
    (S, W, 3, 21), (R, G, 1, 11), (R, G, 1, 14), (S, W, 3, 28), (S, W, 3, 25), (S, W, 3, 20), (S, W, 3, 17),
    (S, G, 1, 6), (S, G, 1, 5), (LIFT, ((0, 0), (-1, 0), (1, 0)), 0), (R, W, 3, 11), (R, W, 3, 15), (R, W, 3, 8),
    (R, W, 3, 9), (R, G, 1, 22), (S, G, 1, 18), (R, G, 1, 24), (S, G, 1, 19), (S, W, 3, 26), (S, W, 3, 31),
    (S, W, 3, 22), (S, W, 3, 23), (LIFT, ((0, 0), (-1, 0), (1, 0)), 1), (R, W, 3, 29), (R, W, 3, 16),
    (PRODUCT, 1, ((1, 0), (-1, 0)), 0), (R, G, 1, 18), (R, G, 1, 19), (S, W, 3, 35), (S, W, 3, 32),
    (LIFT, ((2, 0),), 0), (R, W, 3, 14), (S, W, 3, 30), (R, W, 3, 6), (S, W, 3, 19), (LIFT, ((2, 0),), 1),
    (R, G, 1, 4), (S, G, 1, 23), (S, G, 1, 12), (R, G, 1, 7), (S, G, 1, 25), (S, G, 1, 17), (R, C, 1, 1, 0, 0),
    (FREE, 1, 0, 0, 1), (PRODUCT, 1, ((2, 0),), 0), (R, C, 1, 2, 0, 0), (R, W, 3, 12), (R, W, 3, 5), (R, W, 3, 24),
    (R, W, 3, 21), (S, W, 3, 34), (S, W, 3, 27), (S, W, 3, 18), (S, W, 3, 33), (FREE, 1, 0, 0, 2), (R, G, 1, 12),
    (R, G, 1, 17), (R, W, 3, 28), (R, W, 3, 25), (R, W, 3, 20), (R, W, 3, 17), (R, C, 1, 0, 0, 0), (FAR, 1, 0, 0),
    (R, G, 1, 6), (S, G, 1, 13), (R, G, 1, 5), (S, G, 1, 16), (S, X, 1, 0, 0, 0), (S, X, 1, 0, 0, 1), (R, W, 3, 26),
    (R, W, 3, 31), (R, W, 3, 22), (R, W, 3, 23), (R, G, 1, 13), (R, G, 1, 16), (S, X, 1, 0, 0, 3), (S, X, 1, 0, 0, 4),
    (LIFT, ((0, 1), (-1, 1), (1, 1)), 0), (R, W, 3, 35), (R, W, 3, 32), (R, W, 3, 30), (R, W, 3, 19),
    (LIFT, ((0, 1), (-1, 1), (1, 1)), 1), (R, G, 1, 23), (S, G, 1, 20), (R, G, 1, 25), (S, G, 1, 21), (R, W, 3, 34),
    (R, W, 3, 27), (R, W, 3, 18), (R, W, 3, 33), (PRODUCT, 1, ((2, 0),), 1), (R, X, 1, 0, 0, 0), (R, X, 1, 0, 0, 1),
    (NEAR, 1, 0, 0, 1), (S, X, 1, 0, 0, 2), (NEAR, 1, 0, 0, 2), (S, X, 1, 0, 0, 5),
    (PRODUCT, 1, ((1, 1), (-1, 1)), 0), (PRODUCT, 1, ((1, 0), (-1, 0)), 1), (R, G, 1, 20), (R, G, 1, 21),
    (R, X, 1, 0, 0, 3), (R, X, 1, 0, 0, 4), (R, C, 1, 0, 0, 1), (FAR, 1, 0, 1), (S, X, 1, 0, 1, 0),
    (S, X, 1, 0, 1, 1), (LIFT, ((2, 1),), 0), (R, C, 1, 1, 1, 0), (FREE, 1, 1, 0, 1), (S, X, 1, 1, 0, 3),
    (LIFT, ((2, 1),), 1), (R, C, 1, 2, 1, 0), (R, C, 1, 1, 0, 1), (FREE, 1, 1, 0, 2), (S, X, 1, 1, 0, 4),
    (FREE, 1, 0, 1, 1), (PRODUCT, 1, ((2, 1),), 0), (R, C, 1, 2, 0, 1), (FREE, 1, 0, 1, 2),
    (PRODUCT, 1, ((2, 1),), 1), (R, X, 1, 0, 0, 2), (R, X, 1, 0, 0, 5), (S, X, 1, 0, 1, 3), (S, X, 1, 0, 1, 4),
    (PRODUCT, 1, ((1, 1), (-1, 1)), 1), (PRODUCT, 1, ((0, 0), (0, 1)), 0), (R, C, 1, 0, 1, 0), (R, X, 1, 0, 1, 0),
    (R, X, 1, 0, 1, 1), (R, C, 1, 0, 1, 1), (FAR, 1, 1, 0), (S, X, 1, 1, 0, 0), (S, X, 1, 1, 0, 1), (FAR, 1, 1, 1),
    (NEAR, 1, 0, 1, 1), (NEAR, 1, 0, 1, 2), (PRODUCT, 1, ((0, 0), (0, 1)), 1), (R, C, 1, 1, 1, 1), (R, C, 1, 2, 1, 1),
    (FREE, 1, 1, 1, 1), (FREE, 1, 1, 1, 2), (R, X, 1, 1, 0, 3), (S, X, 1, 1, 1, 0), (R, C, 1, 3, 0, 0),
    (S, X, 1, 1, 1, 1), (FINISH, 0, 0), (R, X, 1, 1, 0, 4), (R, C, 1, 3, 1, 0), (R, C, 1, 3, 0, 1),
    (R, C, 1, 3, 1, 1), (R, X, 1, 0, 1, 3), (S, X, 1, 0, 1, 2), (R, X, 1, 0, 1, 4), (S, X, 1, 0, 1, 5),
    (R, X, 1, 1, 0, 0), (NEAR, 1, 1, 0, 1), (S, X, 1, 1, 0, 2), (R, X, 1, 1, 0, 1), (NEAR, 1, 1, 0, 2),
    (S, X, 1, 1, 0, 5), (R, X, 1, 1, 1, 0), (NEAR, 1, 1, 1, 1), (S, X, 1, 1, 1, 2), (R, X, 1, 1, 1, 1),
    (NEAR, 1, 1, 1, 2), (S, X, 1, 1, 1, 5), (R, X, 1, 0, 1, 2), (S, X, 1, 1, 1, 3), (R, X, 1, 0, 1, 5),
    (S, X, 1, 1, 1, 4), (FINISH, 0, 1), (R, X, 1, 1, 0, 2), (R, X, 1, 1, 0, 5), (FINISH, 1, 0), (R, X, 1, 1, 1, 2),
    (R, X, 1, 1, 1, 5), (R, X, 1, 1, 1, 3), (R, X, 1, 1, 1, 4), (FINISH, 1, 1),
)


def way_of(key):
    if key[0] == W:
        return MESSAGES[key[1]][key[2]][3]
    if key[0] == G:
        return GATHER[key[2]][3]
    if key[0] == C:
        return "d"
    return ("x+", "x-", "x+", "x+", "x-", "x-")[key[4]]


def share():
    sent, waited = {}, {}
    for i, (name, *which) in enumerate(SCHEDULE):
        if name == S:
            sent[tuple(which)] = i
        elif name == R:
            waited[tuple(which)] = i
        elif name == PRODUCT:
            g, cases, j = which
            for dx, h in cases:
                sent[(C, g, TURN[dx], h, j)] = i
    back = {"x+": "x-", "x-": "x+", "y+": "y-", "y-": "y+", "z+": "z-", "z-": "z+", "d": "d"}
    last, place = [], {}
    for key in sorted(sent, key=lambda k: (sent[k], k)):
        toward = [k for k in sent if way_of(k) == back[way_of(key)] and waited[k] < sent[key]]
        heard = max([sent[k] for k in toward], default=-1)
        free = [(at, n) for n, at in enumerate(last) if at < heard]
        if free:
            n = max(free)[1]
            last[n] = waited[key]
        else:
            n = len(last)
            last.append(waited[key])
        place[key] = n
    return place, len(last)


SEMAPHORE, SEMAPHORES = share()


def kernel(
    resid, mix_gain, wq, wk, wv, wg, wo, rate, mlp_gain, wu, wd,
    out,
    w_in, w_out, w_up, w_down, xn, rbuf, after, proj, gated, hid, decay, begun, kept,
    dout, din, sout, rin2, rin1,
    local_sem, w_send, g_send, d_send, s_send, recv,
):
    fs, tp = lax.axis_index("fs"), lax.axis_index("tp")
    z, y, x, c = fs // RING, fs % RING, tp // 2, tp % 2

    def turn(v, d):
        return (v + d + RING) % RING

    device = {
        "y+": (z * RING + turn(y, 1), tp),
        "y-": (z * RING + turn(y, -1), tp),
        "z+": (turn(z, 1) * RING + y, tp),
        "z-": (turn(z, -1) * RING + y, tp),
        "x+": (fs, turn(x, 1) * 2 + c),
        "x-": (fs, turn(x, -1) * 2 + c),
        "d": (fs, x * 2 + 1 - c),
    }

    def remote(src, dst, send, recv, way):
        return pltpu.make_async_remote_copy(
            src_ref=src, dst_ref=dst, send_sem=send, recv_sem=recv,
            device_id=device[way], device_id_type=MESH,
        )

    def send(*args):
        remote(*args).start()

    weights = (w_in, w_out, w_up, w_down)

    def block(dy, dz):
        return turn(z, dz) * RING + turn(y, dy)

    def piece(t, dy, dz, part):
        ref = weights[t]
        f = block(dy, dz)
        if part == "full":
            return ref.at[f]
        if part in ("A", "B"):
            return ref.at[f, :, "AB".index(part)]
        if part in ("h0", "h1"):
            return ref.at[f, int(part[1])]
        return ref.at[f, int(part[2]), "AB".index(part[0])]

    def w_copy(t, n, place):
        dy, dz, part, way = place
        ref = piece(t, dy, dz, part)
        return (ref, ref, w_send.at[t], recv.at[SEMAPHORE[W, t, n]], way)

    def g_copy(g, n, dx, core):
        h, q, way = GATHER[n][1:]
        block = turn(x, dx) * 2 + core
        ref = xn.at[g, block, h] if q is None else xn.at[g, block, h, q]
        return (ref, ref, g_send.at[g], recv.at[SEMAPHORE[G, g, n]], way)

    def rows16(count, body):
        def step(i, carry):
            body(pl.ds(pl.multiple_of(i * 16, 16), 16))
            return carry

        lax.fori_loop(0, count // 16, step, 0)

    def of(ref, j):
        return ref.at[:, pl.ds(j * 1024, 1024)]

    def d_copy(g, k, h, j):
        columns = pl.ds(j * 1024, 1024)
        return (
            dout.at[g, k, h, :, :, columns], din.at[g, k, h, :, :, columns],
            d_send.at[g], recv.at[SEMAPHORE[C, g, k, h, j]], "d",
        )

    def s_copy(g, h, j, n):
        if n < 2:
            src, dst, way = sout.at[g, 0, h, n], rin2.at[g, h, n], ("x+", "x-")[n]
        elif n < 4:
            src, dst, way = sout.at[g, 1, h, n - 2], rin1.at[g, 0, h, n - 2], "x+"
        else:
            src, dst, way = sout.at[g, 2, h, n - 4], rin1.at[g, 1, h, n - 4], "x-"
        return (of(src, j), of(dst, j), s_send.at[g], recv.at[SEMAPHORE[X, g, h, j, n]], way)

    def start(kind, *which):
        if kind == W:
            t, n = which
            send(*w_copy(t, n, MESSAGES[t][n]))
        elif kind == G:
            g, n = which
            send(*g_copy(g, n, GATHER[n][0], c))
        else:
            send(*s_copy(*which))

    def receive(kind, *which):
        if kind == W:
            t, n = which
            copy = w_copy(t, n, arrived(MESSAGES[t][n]))
        elif kind == G:
            g, n = which
            dx, way = GATHER[n][0], GATHER[n][3]
            if way == "d":
                copy = g_copy(g, n, dx, 1 - c)
            else:
                copy = g_copy(g, n, near(dx - (1 if way == "x+" else -1)), c)
        elif kind == C:
            copy = d_copy(*which)
        else:
            copy = s_copy(*which)
        remote(*copy).wait_recv()

    def partial(g, cases, j):
        weight, lhs = ((w_out, gated_rows), (w_down, hidden_rows))[g]
        depth = weight.shape[1] * weight.shape[2] * weight.shape[3]
        for i in (2 * j, 2 * j + 1):
            w = [weight[block(*PLACES[4 * i + n])].reshape(depth, 128) for n in range(4)]
            rows = [some for case in cases for some in lhs(*case)]
            o = jnp.dot(
                jnp.concatenate(rows, axis=0), jnp.concatenate(w, axis=1), preferred_element_type=F32
            )
            columns = slice(i * 512, (i + 1) * 512)
            for n, (dx, h) in enumerate(cases):
                mine = o[n * 128 : (n + 1) * 128]
                dout[g, TURN[dx], h, :, :, columns] = mine[:64].astype(BF16).reshape(2, 32, 512)
                kept[TURN[dx], h, :, :, columns] = mine[64:].reshape(2, 32, 512)
        for dx, h in cases:
            send(*d_copy(g, TURN[dx], h, j))

    def add_quarter(g, k, h, j, q, extra=False):
        columns = slice(j * 1024, (j + 1) * 1024)

        def body(rows):
            total = kept[k, h, q, rows, columns] + din[g, k, h, q, rows, columns].astype(F32)
            if extra:
                total = total + rin2[g, h, q, rows, columns].astype(F32)
            sout[g, k, h, q, rows, columns] = total.astype(BF16)

        rows16(32, body)

    def add_far(g, h, j):
        for q in (0, 1):
            add_quarter(g, 0, h, j, q)

    def add_free(g, h, j, k):
        add_quarter(g, k, h, j, 1 if k == 1 else 0)

    def add_near(g, h, j, k):
        add_quarter(g, k, h, j, 0 if k == 1 else 1, True)

    def add_own(g, h, i, source, target):
        here = pl.ds(pl.multiple_of(block(*PLACES[i]) * 128, 128), 128)
        at = slice(i * 128, (i + 1) * 128)
        total = source[h, :, :, here].astype(F32) + kept[3, h, :, :, at]
        total = total + din[g, 3, h, :, :, at].astype(F32)
        total = total + rin1[g, 0, h, :, :, at].astype(F32) + rin1[g, 1, h, :, :, at].astype(F32)
        target[h, :, :, here] = total.astype(BF16)

    def normed(values, gain):
        scale = lax.rsqrt(jnp.mean(values * values, axis=-1, keepdims=True) + EPS)
        return (values * scale * gain).astype(BF16)

    loads = []

    def load(src, dst):
        copy = pltpu.make_async_copy(src, dst, local_sem.at[len(loads)])
        copy.start()
        return copy

    for src, low, wide in ((wq, 0, 128), (wk, 128, 128), (wv, 256, 256), (wg, 512, 256)):
        load(src, w_in.at[fs, :, :, :, low : low + wide])
    loads.append(pltpu.make_async_copy(w_in.at[fs], w_in.at[fs], local_sem.at[0]))
    for src, dst in ((resid, rbuf), (wo, w_out.at[fs]), (wu, w_up.at[fs]), (wd, w_down.at[fs])):
        loads.append(load(src, dst))
    barrier = pltpu.get_barrier_semaphore()
    for way in device:
        pl.semaphore_signal(barrier, inc=1, device_id=device[way], device_id_type=MESH)
    for copy in loads[:2]:
        copy.wait()
    for h in (0, 1):
        for q in (0, 1):
            def first_norm(rows):
                xn[0, tp, h, q, rows, :] = normed(rbuf[h, q, rows, :].astype(F32), mix_gain[...])

            rows16(32, first_norm)
    pl.semaphore_wait(barrier, 7)
    r = rate[0]

    def make_decay():
        def some_rows(i, carry):
            rows = pl.ds(pl.multiple_of(i * 64, 64), 64)
            t = lax.broadcasted_iota(jnp.int32, (64, LENGTH), 0) + i * 64
            s = lax.broadcasted_iota(jnp.int32, (64, LENGTH), 1)
            gap = (t - s).astype(F32)
            value = jnp.exp(-r * jnp.maximum(gap, 0.0)) * DK ** (-0.5)
            decay[rows, :] = jnp.where(gap >= 0.0, value, 0.0)
            return carry

        lax.fori_loop(0, LENGTH // 64, some_rows, 0)

    own = x // 2
    sequence = (own, 1 - own)

    def project(which, seq, part):
        blocks = [block(*place) for place in (PLACES[:12], PLACES[12:])[part]]

        def body(j, carry):
            columns = pl.ds(pl.multiple_of(j * 256, 256), 256)
            lhs = [
                xn[0, pl.ds(4 * seq, 4), :, :, :, pl.ds(pl.multiple_of(f * 128, 128), 128)].reshape(512, 128)
                for f in blocks
            ]
            rhs = [w_in[f, :, :, :, columns].reshape(128, 256) for f in blocks]
            o = jnp.dot(
                jnp.concatenate(lhs, axis=1), jnp.concatenate(rhs, axis=0), preferred_element_type=F32
            )
            if part == 0:
                begun[which, j] = o
            else:
                o = (begun[which, j] + o).astype(BF16)
                proj[pl.ds(4 * seq, 4), :, columns] = o.reshape(4, 128, 256)
            return carry

        lax.fori_loop(0, 3, body, 0)

    def retain(seq):
        for i in (0, 1):
            mine = pl.ds(seq * 4 + 2 * i, 2)
            upto = pl.ds(seq * 4, 2 * i + 2)
            wide = 256 * (i + 1)
            q = proj[mine, :, 0:128].reshape(256, DK)
            k = proj[upto, :, 128:256].reshape(wide, DK)
            v = proj[upto, :, 256:512].reshape(wide, DV)
            scores = lax.dot_general(q, k, (((1,), (1,)), ((), ())), preferred_element_type=F32)
            scores = (scores * decay[i * 256 : (i + 1) * 256, 0:wide]).astype(BF16)
            mixed = jnp.dot(scores, v, preferred_element_type=F32)
            mixed = mixed - jnp.mean(mixed, axis=-1, keepdims=True)
            spread = jnp.mean(mixed * mixed, axis=-1, keepdims=True)
            gate = proj[mine, :, 512:768].reshape(256, DV).astype(F32)
            value = gate / (1.0 + jnp.exp(-gate)) * (mixed * lax.rsqrt(spread + EPS))
            gated[mine] = value.astype(BF16).reshape(2, 2, 64, DV)

    def gated_rows(dx, h):
        first = turn(x, dx) * 2
        return gated[first + 1 - c, h], gated[first + c, h]

    def lift(cases, part):
        def body(j, carry):
            columns = pl.ds(pl.multiple_of(j * 256, 256), 256)
            lhs = jnp.concatenate(
                [
                    xn[1, turn(x, dx) * 2 + core, h].reshape(64, D)
                    for dx, h in cases
                    for core in (1 - c, c)
                ],
                axis=0,
            )
            rhs = w_up[:, :, :, :, columns].reshape(D, 256)
            o = jnp.maximum(jnp.dot(lhs, rhs, preferred_element_type=F32), 0.0)
            o = (o * o).astype(BF16)
            for n, (dx, h) in enumerate(cases):
                hid[TURN[dx], h, :, columns] = o[n * 128 : (n + 1) * 128]
            return carry

        count = w_up.shape[4] // 512
        lax.fori_loop(part * count, (part + 1) * count, body, 0)

    def hidden_rows(dx, h):
        return (hid[TURN[dx], h],)

    def second_norm(h):
        for i in range(16):
            add_own(0, h, i, rbuf, after)
        for q in (0, 1):
            def body(rows):
                xn[1, tp, h, q, rows, :] = normed(after[h, q, rows, :].astype(F32), mlp_gain[...])

            rows16(32, body)

    def finish(h, j):
        for i in range(8 * j, 8 * j + 8):
            add_own(1, h, i, after, out)

    actions = {
        S: start,
        R: receive,
        DECAY: make_decay,
        PROJECT: lambda which, part: project(which, sequence[which], part),
        RETAIN: lambda which: retain(sequence[which]),
        PRODUCT: partial,
        FAR: add_far,
        FREE: add_free,
        NEAR: add_near,
        NORM: second_norm,
        LIFT: lift,
        FINISH: finish,
    }
    for copy in loads[2:]:
        copy.wait()
    for name, *which in SCHEDULE:
        actions[name](*which)
    for t in range(4):
        ref = weights[t].at[0:15]
        remote(ref, ref, w_send.at[t], recv.at[0], "d").wait_send()
    for g in (0, 1):
        remote(xn.at[g, 0:7], xn.at[g, 0:7], g_send.at[g], recv.at[0], "d").wait_send()
        remote(dout.at[g], din.at[g], d_send.at[g], recv.at[0], "d").wait_send()
        remote(sout.at[g], sout.at[g], s_send.at[g], recv.at[0], "d").wait_send()


def on_device(
    resid, mix_gain, w_query, w_key, w_value, w_gate, w_output, decay_rate, mlp_gain, w_up, w_down
):
    def cut(w):
        return w.reshape(2, 2, w.shape[0] // 4, w.shape[1])

    wide = w_query.shape[1] + w_key.shape[1] + w_value.shape[1] + w_gate.shape[1]
    count = RING * RING

    def held(rows, columns):
        return pltpu.VMEM((count, 2, 2, rows // 4, columns), BF16)

    dma = pltpu.SemaphoreType.DMA
    vmem = pl.BlockSpec(memory_space=pltpu.VMEM)
    hbm = pl.BlockSpec(memory_space=pltpu.HBM)
    tokens = (2, 2, 32, D)
    result = pl.pallas_call(
        kernel,
        out_shape=pltpu.VMEM(tokens, BF16),
        in_specs=[
            hbm, vmem, hbm, hbm, hbm, hbm, hbm,
            pl.BlockSpec(memory_space=pltpu.SMEM), vmem, hbm, hbm,
        ],
        out_specs=vmem,
        scratch_shapes=[
            held(128, wide),
            held(w_output.shape[0], 128),
            held(128, w_up.shape[1]),
            held(w_down.shape[0], 128),
            pltpu.VMEM((2, 8) + tokens, BF16),
            pltpu.VMEM(tokens, BF16),
            pltpu.VMEM(tokens, BF16),
            pltpu.VMEM((8, 128, wide), BF16),
            pltpu.VMEM((8, 2, 64, DV), BF16),
            pltpu.VMEM((4, 2, 128, w_up.shape[1]), BF16),
            pltpu.VMEM((LENGTH, LENGTH), F32),
            pltpu.VMEM((2, wide // 256, LENGTH, 256), F32),
            pltpu.VMEM((4,) + tokens, F32),
            pltpu.VMEM((2, 4) + tokens, BF16),
            pltpu.VMEM((2, 4) + tokens, BF16),
            pltpu.VMEM((2, 3) + tokens, BF16),
            pltpu.VMEM((2,) + tokens, BF16),
            pltpu.VMEM((2, 2) + tokens, BF16),
            dma((5,)),
            dma((4,)),
            dma((2,)),
            dma((2,)),
            dma((2,)),
            dma((SEMAPHORES,)),
        ],
        compiler_params=pltpu.CompilerParams(
            collective_id=0, has_side_effects=True, vmem_limit_bytes=66060288
        ),
    )(
        resid.reshape(tokens), mix_gain[None], cut(w_query), cut(w_key), cut(w_value), cut(w_gate),
        cut(w_output), decay_rate, mlp_gain[None], cut(w_up), cut(w_down),
    )
    return result.reshape(resid.shape)


def solution(mesh):
    placed = (
        P(("fs", "tp"), None),
        P(),
        P("fs", "tp"),
        P("fs", "tp"),
        P("fs", "tp"),
        P("fs", "tp"),
        P("tp", "fs"),
        P("tp"),
        P(),
        P("fs", "tp"),
        P("tp", "fs"),
    )
    return jax.shard_map(
        on_device, mesh=mesh, in_specs=placed, out_specs=P(("fs", "tp"), None), check_vma=False
    )
```

time: 95.7 us -> 94 us (0.982)
  Pallas kernels: 94.1 us -> 92.4 us
    pallas_call x1, Pallas kernels: 94.1 us -> 92.4 us  [on_device(): pl.pallas_call(kernel, out_shape=pltpu.VMEM(tokens, BF16), in_specs=[hbm,...]
where the time goes in v5:
time: 94 us; the launch traced here: 93.9 us
  Pallas kernels  92.4 us (98%)
    pallas_call x1, Pallas kernels, on_device(): pl.pallas_call(kernel, out_shape=pltpu.VMEM(tokens, BF16), in_specs=[hbm,...  92.4 us

profile of v5, /device:TPU:1, one launch (start us, length us, event | category | flops | bytes accessed | tf_op | source)
XLA Modules:
  0.0 93.9 jit_solution(13909582763176185000)
XLA Ops:
  0.7 92.4 %shard_map.109 = bf16[2,2,32,2048]{3,2,1,0:T(8,128)(2,1)S(1)} custom-call(bf16[2,2,32,2048]{3,2,1,0:T(8,128)(2,1)} %bitcast.12, f32[1,2048]{1,0:T(1,128)} %bitcast.20, bf16[2,2,32,128]{3,2,1,0:T(8,128)(2,1)} %bitcast.18, bf16[2,2,32,128]{3,2,1,0:T(8,128)(2,1)} %bitcast.19, bf16[2,2,32,256]{3,2,1,0:T(8,128)(2,1)} %bitcast.15, ...), custom_call_target="tpu_custom_call" | custom-call | tf_op jit(solution)/shard_map/pallas_call | solution.py:542
  93.1 0.8 copy.13

commit v6 on v5

--- a/solution.py
+++ b/solution.py
@@ -52,7 +52,7 @@
     return messages
 
 
-MESSAGES = [plan(parts) for parts in (("h0", "h1"), ("full",), ("full",), ("full",))]
+MESSAGES = [plan(parts) for parts in (("h0", "h1"), ("full",), ("h0", "h1"), ("full",))]
 PLACES = (
     (0, 0), (1, 0), (-1, 0), (0, 1), (0, -1), (2, 0), (0, 2), (1, 1),
     (1, -1), (-1, 1), (-1, -1), (2, 1), (2, -1), (1, 2), (-1, 2), (2, 2),
@@ -70,106 +70,110 @@
 S, R, W, G, C, X = range(6)
 DECAY, PROJECT, RETAIN, PRODUCT, FAR, FREE, NEAR, NORM, LIFT, FINISH = range(6, 16)
 SCHEDULE = (
-    (S, W, 0, 0), (S, W, 1, 1), (S, W, 0, 5), (S, W, 0, 2), (S, W, 1, 3), (S, W, 0, 7), (S, G, 0, 0), (S, G, 0, 3),
-    (S, G, 0, 8), (S, G, 0, 9), (DECAY,), (S, W, 1, 0), (S, W, 1, 2), (R, G, 0, 8), (S, W, 0, 4), (S, W, 0, 1),
-    (S, W, 0, 6), (S, W, 0, 3), (R, G, 0, 9), (S, G, 0, 2), (S, G, 0, 1), (R, W, 1, 1), (R, W, 1, 3), (S, W, 1, 14),
-    (S, W, 1, 7), (S, W, 1, 8), (S, W, 1, 13), (R, W, 0, 0), (R, W, 0, 2), (S, W, 0, 8), (S, W, 1, 15), (S, W, 0, 13),
-    (S, W, 1, 9), (R, G, 0, 0), (S, G, 0, 10), (R, G, 0, 3), (S, G, 0, 15), (S, G, 0, 22), (S, G, 0, 24),
-    (S, W, 0, 15), (S, W, 0, 10), (R, W, 0, 5), (R, W, 0, 7), (R, W, 1, 0), (R, W, 1, 2), (S, W, 0, 20),
-    (S, W, 0, 25), (R, G, 0, 10), (S, W, 1, 4), (S, W, 1, 10), (R, G, 0, 15), (S, W, 1, 11), (S, W, 1, 5),
-    (R, W, 0, 4), (R, W, 0, 1), (R, W, 0, 6), (R, W, 0, 3), (R, G, 0, 2), (S, G, 0, 11), (R, G, 0, 1), (S, G, 0, 14),
-    (S, G, 0, 4), (S, G, 0, 7), (S, W, 0, 16), (S, W, 0, 11), (S, W, 0, 27), (S, W, 1, 6), (R, W, 1, 14),
-    (R, W, 1, 7), (R, W, 1, 8), (R, W, 1, 13), (S, W, 0, 14), (S, W, 0, 9), (S, W, 0, 22), (R, G, 0, 11),
-    (R, W, 1, 15), (R, W, 1, 9), (S, W, 1, 12), (R, G, 0, 14), (S, W, 1, 30), (S, W, 0, 24), (S, W, 0, 18),
-    (S, W, 1, 21), (R, W, 0, 15), (R, W, 0, 10), (S, W, 0, 26), (S, W, 0, 12), (R, W, 0, 8), (R, W, 0, 13),
-    (R, G, 0, 22), (S, G, 0, 18), (R, G, 0, 24), (S, G, 0, 19), (S, G, 0, 6), (S, G, 0, 5), (S, W, 1, 29),
-    (S, W, 0, 28), (R, W, 1, 4), (R, W, 1, 10), (S, W, 1, 24), (S, W, 1, 25), (S, W, 0, 19), (S, W, 0, 32),
-    (S, W, 0, 33), (R, G, 0, 18), (R, W, 1, 11), (R, W, 1, 5), (S, W, 1, 18), (R, G, 0, 19), (R, W, 0, 20),
-    (R, W, 0, 25), (S, W, 1, 16), (S, W, 0, 38), (S, W, 0, 23), (S, W, 0, 42), (S, W, 0, 37), (R, W, 0, 16),
-    (R, W, 0, 11), (R, W, 1, 6), (R, G, 0, 4), (S, G, 0, 12), (R, G, 0, 7), (S, G, 0, 17), (R, W, 0, 27),
-    (S, G, 0, 23), (S, G, 0, 25), (S, W, 1, 19), (S, W, 0, 35), (S, W, 1, 31), (S, W, 0, 31), (S, W, 1, 23),
-    (R, W, 0, 14), (R, W, 0, 9), (R, W, 0, 22), (R, W, 1, 12), (S, W, 1, 27), (S, W, 0, 39), (R, W, 1, 30),
-    (R, W, 1, 21), (S, W, 0, 17), (R, G, 0, 12), (S, W, 0, 34), (S, W, 0, 30), (R, G, 0, 17), (R, W, 0, 24),
-    (R, W, 0, 18), (S, W, 1, 33), (R, W, 1, 29), (R, W, 0, 26), (R, W, 0, 12), (S, W, 0, 40), (S, W, 0, 29),
-    (R, W, 1, 25), (R, W, 1, 24), (S, W, 1, 34), (S, W, 0, 21), (R, W, 0, 28), (R, G, 0, 6), (S, G, 0, 13),
-    (R, G, 0, 5), (S, G, 0, 16), (S, W, 1, 28), (R, W, 1, 18), (R, W, 0, 19), (S, W, 0, 41), (S, W, 1, 35),
-    (S, W, 0, 36), (R, W, 0, 33), (R, W, 1, 16), (R, W, 0, 32), (S, W, 0, 43), (S, W, 0, 44), (R, G, 0, 13),
-    (R, W, 0, 38), (S, W, 0, 45), (S, W, 0, 46), (R, G, 0, 16), (R, W, 0, 42), (R, W, 0, 37), (R, W, 0, 23),
-    (R, W, 1, 19), (S, W, 0, 47), (S, W, 1, 32), (R, W, 1, 31), (R, W, 1, 23), (S, W, 1, 22), (R, W, 1, 27),
-    (S, W, 1, 26), (S, W, 1, 20), (S, W, 1, 17), (R, W, 0, 31), (R, W, 0, 35), (R, G, 0, 23), (S, G, 0, 20),
-    (R, G, 0, 25), (S, G, 0, 21), (S, W, 2, 0), (S, W, 2, 1), (S, W, 2, 2), (S, W, 2, 3), (R, W, 0, 39),
-    (R, W, 0, 17), (R, W, 1, 33), (R, W, 0, 30), (R, W, 0, 34), (R, G, 0, 20), (R, W, 1, 34), (R, G, 0, 21),
-    (R, W, 0, 40), (R, W, 0, 29), (R, W, 1, 28), (R, W, 1, 35), (R, W, 0, 21), (R, W, 0, 41), (R, W, 0, 36),
-    (R, W, 0, 43), (PROJECT, 1, 0), (R, W, 0, 44), (R, W, 1, 32), (R, W, 1, 22), (R, W, 0, 45), (R, W, 0, 46),
-    (R, W, 0, 47), (R, W, 1, 20), (R, W, 1, 26), (R, W, 1, 17), (PROJECT, 1, 1), (S, W, 3, 0), (S, W, 3, 1),
-    (S, W, 3, 2), (S, W, 3, 3), (RETAIN, 1), (PRODUCT, 0, ((2, 0), (2, 1)), 0), (PRODUCT, 0, ((2, 0), (2, 1)), 1),
-    (PROJECT, 0, 0), (R, C, 0, 0, 0, 0), (R, C, 0, 0, 1, 0), (R, C, 0, 0, 0, 1), (R, C, 0, 0, 1, 1), (FAR, 0, 0, 0),
-    (S, X, 0, 0, 0, 0), (S, X, 0, 0, 0, 1), (FAR, 0, 1, 0), (FAR, 0, 0, 1), (FAR, 0, 1, 1), (PROJECT, 0, 1),
-    (R, W, 2, 1), (R, W, 2, 2), (R, W, 2, 0), (R, W, 2, 3), (S, X, 0, 1, 0, 0), (S, X, 0, 1, 0, 1), (RETAIN, 0),
-    (S, W, 2, 4), (S, W, 2, 12), (S, W, 2, 8), (S, W, 2, 13), (PRODUCT, 0, ((1, 0), (-1, 0)), 0), (S, X, 0, 0, 1, 0),
-    (S, X, 0, 0, 1, 1), (PRODUCT, 0, ((1, 1), (-1, 1)), 0), (PRODUCT, 0, ((1, 0), (-1, 0)), 1),
-    (PRODUCT, 0, ((1, 1), (-1, 1)), 1), (S, X, 0, 1, 1, 0), (S, X, 0, 1, 1, 1), (PRODUCT, 0, ((0, 0), (0, 1)), 0),
-    (R, C, 0, 1, 0, 0), (R, X, 0, 0, 0, 0), (R, X, 0, 0, 0, 1), (R, C, 0, 2, 0, 0), (FREE, 0, 0, 0, 1),
-    (FREE, 0, 0, 0, 2), (NEAR, 0, 0, 0, 1), (NEAR, 0, 0, 0, 2), (PRODUCT, 0, ((0, 0), (0, 1)), 1), (R, C, 0, 1, 1, 0),
-    (R, C, 0, 2, 1, 0), (FREE, 0, 1, 0, 1), (FREE, 0, 1, 0, 2), (R, C, 0, 1, 0, 1), (FREE, 0, 0, 1, 1),
-    (R, C, 0, 2, 0, 1), (FREE, 0, 0, 1, 2), (S, W, 2, 14), (S, W, 2, 7), (S, W, 2, 10), (S, W, 2, 6),
-    (R, C, 0, 1, 1, 1), (FREE, 0, 1, 1, 1), (R, X, 0, 1, 0, 0), (R, X, 0, 1, 0, 1), (NEAR, 0, 1, 0, 1),
-    (S, X, 0, 0, 0, 2), (S, X, 0, 0, 0, 5), (NEAR, 0, 1, 0, 2), (R, C, 0, 2, 1, 1), (FREE, 0, 1, 1, 2),
-    (R, C, 0, 3, 0, 0), (R, C, 0, 3, 1, 0), (R, W, 3, 0), (R, W, 3, 1), (R, W, 3, 2), (R, W, 3, 3),
-    (R, C, 0, 3, 0, 1), (R, C, 0, 3, 1, 1), (R, X, 0, 0, 1, 0), (R, X, 0, 0, 1, 1), (NEAR, 0, 0, 1, 1),
-    (S, X, 0, 0, 1, 2), (S, X, 0, 0, 0, 4), (NEAR, 0, 0, 1, 2), (S, W, 2, 11), (S, W, 2, 15), (S, W, 2, 5),
-    (S, W, 2, 9), (R, X, 0, 1, 1, 0), (R, X, 0, 1, 1, 1), (NEAR, 0, 1, 1, 1), (S, X, 0, 0, 0, 3), (S, X, 0, 0, 1, 5),
-    (NEAR, 0, 1, 1, 2), (R, W, 2, 4), (R, W, 2, 12), (R, W, 2, 8), (R, W, 2, 13), (R, X, 0, 0, 0, 2),
-    (R, X, 0, 0, 0, 5), (S, X, 0, 0, 1, 3), (S, X, 0, 0, 1, 4), (S, W, 2, 28), (S, W, 2, 29), (S, W, 2, 16),
-    (S, W, 2, 17), (R, X, 0, 0, 1, 2), (R, X, 0, 0, 0, 4), (S, X, 0, 1, 0, 2), (S, X, 0, 1, 0, 5), (R, W, 2, 14),
-    (R, W, 2, 7), (R, W, 2, 10), (R, W, 2, 6), (S, W, 2, 24), (S, W, 2, 25), (S, W, 2, 22), (S, W, 2, 21),
-    (R, X, 0, 0, 0, 3), (R, X, 0, 0, 1, 5), (S, X, 0, 1, 1, 2), (S, X, 0, 1, 1, 5), (S, W, 2, 30), (S, W, 2, 27),
-    (S, W, 2, 20), (S, W, 2, 19), (R, X, 0, 0, 1, 3), (R, X, 0, 0, 1, 4), (S, X, 0, 1, 0, 3), (S, X, 0, 1, 0, 4),
-    (NORM, 0), (S, G, 1, 8), (R, W, 2, 11), (R, W, 2, 15), (R, W, 2, 5), (R, W, 2, 9), (S, W, 2, 26), (S, W, 2, 31),
-    (S, W, 2, 18), (S, W, 2, 23), (R, X, 0, 1, 0, 2), (R, X, 0, 1, 0, 5), (S, X, 0, 1, 1, 3), (S, X, 0, 1, 1, 4),
-    (R, G, 1, 8), (R, W, 2, 28), (R, W, 2, 29), (R, W, 2, 16), (R, W, 2, 17), (S, W, 3, 4), (S, W, 2, 35),
-    (S, W, 2, 32), (S, W, 3, 13), (R, X, 0, 1, 1, 2), (R, X, 0, 1, 1, 5), (S, G, 1, 0), (S, G, 1, 3), (R, W, 2, 24),
-    (R, W, 2, 25), (R, W, 2, 22), (R, W, 2, 21), (S, W, 3, 7), (S, W, 3, 10), (R, X, 0, 1, 0, 3), (R, X, 0, 1, 0, 4),
-    (R, W, 2, 30), (R, W, 2, 27), (R, W, 2, 20), (R, W, 2, 19), (S, W, 2, 34), (S, W, 2, 33), (R, X, 0, 1, 1, 3),
-    (R, X, 0, 1, 1, 4), (S, G, 1, 2), (S, G, 1, 1), (NORM, 1), (S, G, 1, 9), (R, W, 2, 26), (R, W, 2, 31),
-    (R, W, 2, 18), (R, W, 2, 23), (S, W, 3, 11), (S, W, 3, 15), (S, W, 3, 8), (S, W, 3, 9), (R, G, 1, 9),
-    (R, W, 2, 35), (R, W, 2, 32), (R, G, 1, 0), (S, G, 1, 10), (R, G, 1, 3), (S, G, 1, 15), (S, G, 1, 22),
-    (S, G, 1, 24), (R, W, 3, 4), (R, W, 3, 13), (S, W, 3, 14), (S, W, 3, 29), (S, W, 3, 16), (S, W, 3, 6),
-    (R, G, 1, 10), (R, G, 1, 15), (R, W, 3, 7), (R, W, 3, 10), (R, W, 2, 34), (R, W, 2, 33), (S, W, 3, 12),
-    (S, W, 3, 5), (R, G, 1, 2), (S, G, 1, 11), (R, G, 1, 1), (S, G, 1, 14), (S, G, 1, 4), (S, G, 1, 7), (S, W, 3, 24),
-    (S, W, 3, 21), (R, G, 1, 11), (R, G, 1, 14), (S, W, 3, 28), (S, W, 3, 25), (S, W, 3, 20), (S, W, 3, 17),
-    (S, G, 1, 6), (S, G, 1, 5), (LIFT, ((0, 0), (-1, 0), (1, 0)), 0), (R, W, 3, 11), (R, W, 3, 15), (R, W, 3, 8),
-    (R, W, 3, 9), (R, G, 1, 22), (S, G, 1, 18), (R, G, 1, 24), (S, G, 1, 19), (S, W, 3, 26), (S, W, 3, 31),
-    (S, W, 3, 22), (S, W, 3, 23), (LIFT, ((0, 0), (-1, 0), (1, 0)), 1), (R, W, 3, 29), (R, W, 3, 16),
-    (PRODUCT, 1, ((1, 0), (-1, 0)), 0), (R, G, 1, 18), (R, G, 1, 19), (S, W, 3, 35), (S, W, 3, 32),
-    (LIFT, ((2, 0),), 0), (R, W, 3, 14), (S, W, 3, 30), (R, W, 3, 6), (S, W, 3, 19), (LIFT, ((2, 0),), 1),
-    (R, G, 1, 4), (S, G, 1, 23), (S, G, 1, 12), (R, G, 1, 7), (S, G, 1, 25), (S, G, 1, 17), (R, C, 1, 1, 0, 0),
-    (FREE, 1, 0, 0, 1), (PRODUCT, 1, ((2, 0),), 0), (R, C, 1, 2, 0, 0), (R, W, 3, 12), (R, W, 3, 5), (R, W, 3, 24),
-    (R, W, 3, 21), (S, W, 3, 34), (S, W, 3, 27), (S, W, 3, 18), (S, W, 3, 33), (FREE, 1, 0, 0, 2), (R, G, 1, 12),
-    (R, G, 1, 17), (R, W, 3, 28), (R, W, 3, 25), (R, W, 3, 20), (R, W, 3, 17), (R, C, 1, 0, 0, 0), (FAR, 1, 0, 0),
-    (R, G, 1, 6), (S, G, 1, 13), (R, G, 1, 5), (S, G, 1, 16), (S, X, 1, 0, 0, 0), (S, X, 1, 0, 0, 1), (R, W, 3, 26),
-    (R, W, 3, 31), (R, W, 3, 22), (R, W, 3, 23), (R, G, 1, 13), (R, G, 1, 16), (S, X, 1, 0, 0, 3), (S, X, 1, 0, 0, 4),
-    (LIFT, ((0, 1), (-1, 1), (1, 1)), 0), (R, W, 3, 35), (R, W, 3, 32), (R, W, 3, 30), (R, W, 3, 19),
-    (LIFT, ((0, 1), (-1, 1), (1, 1)), 1), (R, G, 1, 23), (S, G, 1, 20), (R, G, 1, 25), (S, G, 1, 21), (R, W, 3, 34),
-    (R, W, 3, 27), (R, W, 3, 18), (R, W, 3, 33), (PRODUCT, 1, ((2, 0),), 1), (R, X, 1, 0, 0, 0), (R, X, 1, 0, 0, 1),
-    (NEAR, 1, 0, 0, 1), (S, X, 1, 0, 0, 2), (NEAR, 1, 0, 0, 2), (S, X, 1, 0, 0, 5),
-    (PRODUCT, 1, ((1, 1), (-1, 1)), 0), (PRODUCT, 1, ((1, 0), (-1, 0)), 1), (R, G, 1, 20), (R, G, 1, 21),
-    (R, X, 1, 0, 0, 3), (R, X, 1, 0, 0, 4), (R, C, 1, 0, 0, 1), (FAR, 1, 0, 1), (S, X, 1, 0, 1, 0),
-    (S, X, 1, 0, 1, 1), (LIFT, ((2, 1),), 0), (R, C, 1, 1, 1, 0), (FREE, 1, 1, 0, 1), (S, X, 1, 1, 0, 3),
-    (LIFT, ((2, 1),), 1), (R, C, 1, 2, 1, 0), (R, C, 1, 1, 0, 1), (FREE, 1, 1, 0, 2), (S, X, 1, 1, 0, 4),
-    (FREE, 1, 0, 1, 1), (PRODUCT, 1, ((2, 1),), 0), (R, C, 1, 2, 0, 1), (FREE, 1, 0, 1, 2),
-    (PRODUCT, 1, ((2, 1),), 1), (R, X, 1, 0, 0, 2), (R, X, 1, 0, 0, 5), (S, X, 1, 0, 1, 3), (S, X, 1, 0, 1, 4),
-    (PRODUCT, 1, ((1, 1), (-1, 1)), 1), (PRODUCT, 1, ((0, 0), (0, 1)), 0), (R, C, 1, 0, 1, 0), (R, X, 1, 0, 1, 0),
-    (R, X, 1, 0, 1, 1), (R, C, 1, 0, 1, 1), (FAR, 1, 1, 0), (S, X, 1, 1, 0, 0), (S, X, 1, 1, 0, 1), (FAR, 1, 1, 1),
-    (NEAR, 1, 0, 1, 1), (NEAR, 1, 0, 1, 2), (PRODUCT, 1, ((0, 0), (0, 1)), 1), (R, C, 1, 1, 1, 1), (R, C, 1, 2, 1, 1),
-    (FREE, 1, 1, 1, 1), (FREE, 1, 1, 1, 2), (R, X, 1, 1, 0, 3), (S, X, 1, 1, 1, 0), (R, C, 1, 3, 0, 0),
-    (S, X, 1, 1, 1, 1), (FINISH, 0, 0), (R, X, 1, 1, 0, 4), (R, C, 1, 3, 1, 0), (R, C, 1, 3, 0, 1),
-    (R, C, 1, 3, 1, 1), (R, X, 1, 0, 1, 3), (S, X, 1, 0, 1, 2), (R, X, 1, 0, 1, 4), (S, X, 1, 0, 1, 5),
-    (R, X, 1, 1, 0, 0), (NEAR, 1, 1, 0, 1), (S, X, 1, 1, 0, 2), (R, X, 1, 1, 0, 1), (NEAR, 1, 1, 0, 2),
-    (S, X, 1, 1, 0, 5), (R, X, 1, 1, 1, 0), (NEAR, 1, 1, 1, 1), (S, X, 1, 1, 1, 2), (R, X, 1, 1, 1, 1),
-    (NEAR, 1, 1, 1, 2), (S, X, 1, 1, 1, 5), (R, X, 1, 0, 1, 2), (S, X, 1, 1, 1, 3), (R, X, 1, 0, 1, 5),
-    (S, X, 1, 1, 1, 4), (FINISH, 0, 1), (R, X, 1, 1, 0, 2), (R, X, 1, 1, 0, 5), (FINISH, 1, 0), (R, X, 1, 1, 1, 2),
-    (R, X, 1, 1, 1, 5), (R, X, 1, 1, 1, 3), (R, X, 1, 1, 1, 4), (FINISH, 1, 1),
+    (S, W, 0, 0), (S, W, 0, 5), (S, W, 0, 2), (S, W, 0, 7), (S, G, 0, 0), (S, G, 0, 3), (S, G, 0, 8), (S, G, 0, 9),
+    (DECAY,), (S, W, 0, 4), (S, W, 0, 1), (S, W, 0, 6), (S, W, 0, 3), (R, G, 0, 8), (R, G, 0, 9), (S, G, 0, 2),
+    (S, G, 0, 1), (S, W, 1, 0), (S, W, 1, 1), (S, W, 1, 2), (S, W, 1, 3), (R, W, 0, 0), (R, W, 0, 5), (R, W, 0, 2),
+    (R, W, 0, 7), (S, W, 0, 8), (S, W, 0, 20), (S, W, 0, 13), (S, W, 0, 25), (S, G, 0, 4), (S, G, 0, 7), (R, G, 0, 0),
+    (S, G, 0, 10), (R, G, 0, 3), (S, G, 0, 15), (R, G, 0, 10), (R, W, 0, 4), (R, W, 0, 1), (R, W, 0, 6), (R, W, 0, 3),
+    (S, W, 0, 16), (S, W, 0, 24), (S, W, 0, 11), (S, W, 0, 22), (R, G, 0, 15), (S, G, 0, 22), (S, G, 0, 24),
+    (S, W, 0, 14), (S, W, 0, 27), (S, W, 0, 9), (S, W, 0, 19), (R, G, 0, 2), (S, G, 0, 11), (R, G, 0, 1),
+    (S, G, 0, 14), (R, W, 1, 0), (R, W, 1, 1), (R, W, 1, 2), (R, W, 1, 3), (S, W, 0, 26), (S, W, 0, 15),
+    (S, W, 0, 21), (S, W, 0, 12), (R, G, 0, 11), (R, G, 0, 14), (S, W, 0, 23), (S, W, 0, 17), (S, W, 0, 18),
+    (S, W, 0, 10), (R, W, 0, 8), (R, W, 0, 20), (R, W, 0, 13), (R, W, 0, 25), (S, G, 0, 6), (S, G, 0, 5),
+    (R, G, 0, 4), (S, G, 0, 12), (R, G, 0, 7), (S, G, 0, 17), (S, W, 0, 32), (S, W, 0, 42), (S, W, 0, 28),
+    (S, W, 0, 38), (R, W, 0, 16), (R, W, 0, 24), (R, W, 0, 11), (R, W, 0, 22), (S, W, 0, 41), (S, W, 0, 33),
+    (S, W, 0, 31), (S, W, 0, 39), (R, G, 0, 12), (R, W, 0, 14), (R, W, 0, 27), (R, W, 0, 9), (R, W, 0, 19),
+    (R, G, 0, 17), (S, W, 0, 35), (S, W, 0, 40), (S, W, 0, 37), (S, W, 0, 29), (R, W, 0, 26), (R, W, 0, 15),
+    (R, W, 0, 21), (R, W, 0, 12), (S, G, 0, 23), (S, G, 0, 25), (R, G, 0, 22), (S, G, 0, 18), (R, G, 0, 24),
+    (S, G, 0, 19), (S, W, 0, 34), (S, W, 0, 43), (S, W, 0, 30), (S, W, 0, 36), (R, W, 0, 23), (R, W, 0, 17),
+    (R, W, 0, 18), (R, W, 0, 10), (R, G, 0, 18), (S, W, 1, 4), (S, W, 1, 7), (S, W, 1, 10), (S, W, 1, 13),
+    (R, G, 0, 19), (R, W, 0, 32), (R, W, 0, 42), (R, W, 0, 28), (R, W, 0, 38), (S, W, 0, 45), (S, W, 0, 47),
+    (S, W, 0, 44), (S, W, 0, 46), (R, W, 0, 41), (R, W, 0, 33), (R, W, 0, 31), (R, W, 0, 39), (R, G, 0, 6),
+    (S, G, 0, 13), (R, G, 0, 5), (S, G, 0, 16), (S, W, 1, 14), (S, W, 1, 12), (S, W, 1, 8), (S, W, 1, 6),
+    (R, W, 0, 35), (R, W, 0, 40), (R, W, 0, 37), (R, W, 0, 29), (S, W, 1, 11), (S, W, 1, 15), (S, W, 1, 5),
+    (S, W, 1, 9), (R, G, 0, 13), (R, G, 0, 16), (S, W, 2, 0), (S, W, 2, 5), (S, W, 2, 2), (S, W, 2, 7), (R, W, 0, 34),
+    (R, W, 0, 43), (R, W, 0, 30), (R, W, 0, 36), (PROJECT, 1, 0), (R, W, 1, 4), (R, W, 1, 7), (R, W, 1, 10),
+    (R, W, 1, 13), (R, G, 0, 23), (S, G, 0, 20), (R, G, 0, 25), (S, G, 0, 21), (S, W, 1, 24), (S, W, 1, 29),
+    (S, W, 1, 16), (S, W, 1, 21), (PROJECT, 0, 0), (R, W, 0, 45), (R, W, 0, 47), (R, W, 0, 44), (R, W, 0, 46),
+    (R, G, 0, 20), (R, W, 1, 14), (R, W, 1, 12), (R, W, 1, 8), (R, W, 1, 6), (R, G, 0, 21), (S, W, 1, 28),
+    (S, W, 1, 30), (S, W, 2, 4), (S, W, 1, 25), (S, W, 1, 27), (S, W, 2, 1), (S, W, 1, 22), (S, W, 1, 20),
+    (S, W, 2, 6), (S, W, 1, 17), (S, W, 1, 19), (S, W, 2, 3), (PROJECT, 2, 0), (R, W, 1, 11), (R, W, 1, 15),
+    (R, W, 1, 5), (R, W, 1, 9), (PROJECT, 1, 1), (RETAIN, 1), (PRODUCT, 0, ((2, 0), (2, 1)), 0), (S, W, 1, 26),
+    (S, W, 1, 31), (S, W, 1, 18), (S, W, 1, 23), (PROJECT, 0, 1), (R, W, 2, 0), (R, W, 2, 5), (R, W, 2, 2),
+    (R, W, 2, 7), (R, W, 1, 24), (R, W, 1, 29), (R, W, 1, 16), (R, W, 1, 21), (R, W, 1, 28), (R, W, 1, 25),
+    (R, W, 1, 22), (R, W, 1, 17), (S, W, 1, 34), (S, W, 2, 8), (S, W, 1, 35), (S, W, 2, 20), (S, W, 1, 32),
+    (S, W, 2, 13), (S, W, 1, 33), (S, W, 2, 25), (RETAIN, 0), (R, W, 1, 30), (R, W, 1, 27), (R, W, 1, 20),
+    (R, W, 1, 19), (R, C, 0, 0, 0, 0), (R, C, 0, 0, 1, 0), (FAR, 0, 0, 0), (S, X, 0, 0, 0, 0), (S, X, 0, 0, 0, 1),
+    (FAR, 0, 1, 0), (PRODUCT, 0, ((1, 0), (-1, 0)), 0), (PRODUCT, 0, ((1, 1), (-1, 1)), 0), (S, X, 0, 1, 0, 0),
+    (S, X, 0, 1, 0, 1), (PRODUCT, 0, ((0, 0), (0, 1)), 0), (R, C, 0, 1, 0, 0), (FREE, 0, 0, 0, 1), (R, C, 0, 2, 0, 0),
+    (FREE, 0, 0, 0, 2), (R, C, 0, 1, 1, 0), (FREE, 0, 1, 0, 1), (R, W, 2, 4), (R, W, 2, 1), (R, W, 2, 6),
+    (R, W, 2, 3), (S, W, 2, 16), (S, W, 2, 27), (S, W, 3, 2), (S, W, 2, 19), (S, X, 0, 0, 0, 3), (S, X, 0, 0, 0, 4),
+    (R, C, 0, 2, 1, 0), (FREE, 0, 1, 0, 2), (R, W, 1, 26), (R, W, 1, 31), (R, W, 1, 18), (R, W, 1, 23),
+    (R, C, 0, 3, 0, 0), (R, W, 1, 34), (R, W, 1, 35), (R, W, 1, 32), (R, W, 1, 33), (PRODUCT, 0, ((2, 0), (2, 1)), 1),
+    (R, C, 0, 3, 1, 0), (PRODUCT, 0, ((1, 0), (-1, 0)), 1), (S, W, 3, 0), (S, W, 2, 24), (S, W, 2, 22),
+    (S, X, 0, 1, 0, 3), (S, X, 0, 1, 0, 4), (PRODUCT, 0, ((1, 1), (-1, 1)), 1), (PRODUCT, 0, ((0, 0), (0, 1)), 1),
+    (R, X, 0, 0, 0, 0), (R, X, 0, 0, 0, 1), (NEAR, 0, 0, 0, 1), (NEAR, 0, 0, 0, 2), (R, C, 0, 0, 0, 1),
+    (FAR, 0, 0, 1), (R, C, 0, 0, 1, 1), (FAR, 0, 1, 1), (S, W, 3, 1), (S, W, 3, 3), (R, C, 0, 1, 0, 1),
+    (S, X, 0, 0, 1, 0), (S, X, 0, 0, 1, 1), (FREE, 0, 0, 1, 1), (R, C, 0, 2, 0, 1), (FREE, 0, 0, 1, 2),
+    (R, X, 0, 1, 0, 0), (R, X, 0, 1, 0, 1), (NEAR, 0, 1, 0, 1), (NEAR, 0, 1, 0, 2), (R, C, 0, 1, 1, 1),
+    (FREE, 0, 1, 1, 1), (R, W, 2, 8), (R, W, 2, 20), (R, W, 2, 13), (R, W, 2, 25), (R, C, 0, 2, 1, 1),
+    (FREE, 0, 1, 1, 2), (R, C, 0, 3, 0, 1), (R, C, 0, 3, 1, 1), (S, X, 0, 1, 1, 0), (S, X, 0, 1, 1, 1),
+    (R, X, 0, 0, 0, 3), (R, X, 0, 0, 0, 4), (R, W, 2, 16), (R, W, 2, 27), (R, W, 2, 19), (S, W, 2, 9),
+    (S, X, 0, 0, 0, 2), (S, X, 0, 0, 0, 5), (R, X, 0, 1, 0, 3), (R, X, 0, 1, 0, 4), (R, W, 2, 24), (R, W, 2, 22),
+    (S, W, 2, 32), (S, W, 2, 28), (S, X, 0, 0, 1, 3), (S, X, 0, 0, 1, 4), (R, X, 0, 0, 1, 0), (R, X, 0, 0, 1, 1),
+    (NEAR, 0, 0, 1, 1), (NEAR, 0, 0, 1, 2), (S, W, 2, 14), (S, W, 2, 42), (S, W, 2, 11), (S, W, 2, 38),
+    (S, X, 0, 0, 1, 2), (S, X, 0, 0, 1, 5), (R, X, 0, 1, 1, 0), (R, X, 0, 1, 1, 1), (NEAR, 0, 1, 1, 1),
+    (NEAR, 0, 1, 1, 2), (R, W, 3, 2), (S, W, 2, 35), (S, W, 2, 15), (S, W, 2, 21), (S, W, 2, 29), (S, X, 0, 1, 0, 2),
+    (S, X, 0, 1, 0, 5), (R, X, 0, 0, 0, 2), (R, X, 0, 0, 0, 5), (R, W, 3, 0), (R, W, 2, 9), (S, W, 2, 41),
+    (S, W, 2, 43), (S, W, 2, 18), (S, W, 2, 10), (S, X, 0, 1, 1, 2), (S, X, 0, 1, 1, 5), (R, X, 0, 0, 1, 3),
+    (R, X, 0, 0, 1, 4), (R, W, 2, 32), (R, W, 3, 1), (R, W, 3, 3), (R, W, 2, 28), (S, W, 3, 4), (S, W, 3, 7),
+    (S, W, 2, 37), (S, W, 3, 13), (S, X, 0, 1, 1, 3), (S, X, 0, 1, 1, 4), (R, X, 0, 0, 1, 2), (R, X, 0, 0, 1, 5),
+    (NORM, 0), (S, G, 1, 8), (R, W, 2, 14), (R, W, 2, 42), (R, W, 2, 11), (R, W, 2, 38), (S, W, 2, 31), (S, G, 1, 0),
+    (S, G, 1, 3), (R, X, 0, 1, 0, 2), (R, X, 0, 1, 0, 5), (R, W, 2, 35), (R, W, 2, 15), (R, W, 2, 21), (R, W, 2, 29),
+    (R, G, 1, 8), (S, W, 2, 34), (S, W, 2, 47), (S, W, 3, 10), (S, W, 2, 46), (R, X, 0, 1, 1, 2), (R, X, 0, 1, 1, 5),
+    (R, W, 2, 41), (R, W, 2, 43), (R, W, 2, 18), (R, W, 2, 10), (S, W, 2, 45), (S, W, 2, 40), (S, W, 2, 36),
+    (S, G, 1, 2), (S, G, 1, 1), (R, X, 0, 1, 1, 3), (R, X, 0, 1, 1, 4), (NORM, 1), (S, G, 1, 9), (R, W, 2, 37),
+    (S, W, 2, 23), (S, W, 2, 33), (S, W, 2, 30), (S, W, 2, 39), (R, W, 3, 4), (R, W, 2, 31), (R, W, 3, 7),
+    (R, W, 3, 13), (R, G, 1, 9), (S, W, 2, 26), (S, W, 2, 17), (S, W, 2, 44), (S, W, 2, 12), (S, G, 1, 4),
+    (S, G, 1, 7), (R, G, 1, 0), (S, G, 1, 10), (R, G, 1, 3), (S, G, 1, 15), (R, W, 2, 34), (R, W, 2, 47),
+    (R, W, 2, 46), (S, W, 3, 11), (S, W, 3, 15), (S, W, 3, 16), (S, W, 3, 9), (R, G, 1, 10), (R, G, 1, 15),
+    (R, W, 2, 45), (R, W, 3, 10), (R, W, 2, 40), (R, W, 2, 36), (S, W, 3, 5), (S, G, 1, 22), (S, G, 1, 24),
+    (R, G, 1, 2), (S, G, 1, 11), (R, G, 1, 1), (S, G, 1, 14), (R, W, 2, 23), (R, W, 2, 33), (R, W, 2, 30),
+    (R, W, 2, 39), (S, W, 3, 24), (S, W, 3, 29), (S, W, 3, 21), (R, G, 1, 11), (R, G, 1, 14), (R, W, 2, 26),
+    (R, W, 2, 17), (R, W, 2, 44), (R, W, 2, 12), (S, W, 3, 14), (S, W, 3, 12), (S, W, 3, 8), (S, W, 3, 6),
+    (S, G, 1, 6), (S, G, 1, 5), (LIFT, ((0, 0), (-1, 0), (1, 0)), 0), (R, G, 1, 4), (S, G, 1, 12), (R, G, 1, 7),
+    (S, G, 1, 17), (LIFT, ((0, 0), (-1, 0), (1, 0)), 1), (R, W, 3, 16), (R, G, 1, 12), (R, W, 3, 11), (R, W, 3, 15),
+    (R, W, 3, 9), (PRODUCT, 1, ((1, 0), (-1, 0)), 0), (R, G, 1, 17), (S, W, 3, 26), (S, W, 3, 31), (S, W, 3, 32),
+    (S, W, 3, 17), (S, G, 1, 23), (S, G, 1, 25), (R, G, 1, 22), (S, G, 1, 18), (R, G, 1, 24), (S, G, 1, 19),
+    (R, W, 3, 24), (R, W, 3, 5), (R, W, 3, 29), (R, W, 3, 21), (R, C, 1, 1, 0, 0), (FREE, 1, 0, 0, 1), (S, W, 3, 34),
+    (S, W, 3, 25), (S, W, 3, 18), (S, W, 3, 23), (R, C, 1, 2, 0, 0), (FREE, 1, 0, 0, 2), (R, G, 1, 18), (R, G, 1, 19),
+    (LIFT, ((2, 0),), 0), (S, W, 3, 28), (S, W, 3, 35), (S, W, 3, 20), (S, W, 3, 33), (S, X, 1, 0, 0, 3),
+    (S, X, 1, 0, 0, 4), (LIFT, ((2, 0),), 1), (R, G, 1, 6), (S, G, 1, 13), (R, G, 1, 5), (S, G, 1, 16), (R, W, 3, 14),
+    (R, W, 3, 12), (R, W, 3, 8), (R, W, 3, 6), (PRODUCT, 1, ((2, 0),), 0), (S, W, 3, 30), (S, W, 3, 27),
+    (S, W, 3, 22), (S, W, 3, 19), (R, G, 1, 13), (R, W, 3, 26), (R, W, 3, 31), (R, W, 3, 32), (R, W, 3, 17),
+    (R, G, 1, 16), (LIFT, ((0, 1), (-1, 1), (1, 1)), 0), (R, C, 1, 0, 0, 0), (R, G, 1, 23), (S, G, 1, 20),
+    (R, G, 1, 25), (S, G, 1, 21), (R, W, 3, 34), (R, W, 3, 25), (R, W, 3, 18), (R, W, 3, 23), (FAR, 1, 0, 0),
+    (S, X, 1, 0, 0, 0), (S, X, 1, 0, 0, 1), (LIFT, ((0, 1), (-1, 1), (1, 1)), 1), (R, X, 1, 0, 0, 3),
+    (R, X, 1, 0, 0, 4), (PRODUCT, 1, ((1, 1), (-1, 1)), 0), (R, G, 1, 20), (R, W, 3, 28), (R, W, 3, 35),
+    (R, W, 3, 20), (R, W, 3, 33), (R, G, 1, 21), (LIFT, ((2, 1),), 0), (LIFT, ((2, 1),), 1), (R, W, 3, 30),
+    (R, W, 3, 27), (R, W, 3, 22), (R, W, 3, 19), (R, C, 1, 1, 1, 0), (FREE, 1, 1, 0, 1), (S, X, 1, 1, 0, 3),
+    (PRODUCT, 1, ((2, 1),), 0), (R, C, 1, 2, 1, 0), (FREE, 1, 1, 0, 2), (S, X, 1, 1, 0, 4),
+    (PRODUCT, 1, ((2, 0),), 1), (R, X, 1, 0, 0, 0), (R, X, 1, 0, 0, 1), (NEAR, 1, 0, 0, 1), (NEAR, 1, 0, 0, 2),
+    (S, X, 1, 0, 0, 2), (PRODUCT, 1, ((2, 1),), 1), (S, X, 1, 0, 0, 5), (PRODUCT, 1, ((1, 0), (-1, 0)), 1),
+    (R, C, 1, 0, 1, 0), (FAR, 1, 1, 0), (S, X, 1, 1, 0, 0), (PRODUCT, 1, ((1, 1), (-1, 1)), 1), (R, C, 1, 0, 0, 1),
+    (R, C, 1, 0, 1, 1), (S, X, 1, 1, 0, 1), (FAR, 1, 0, 1), (FAR, 1, 1, 1), (PRODUCT, 1, ((0, 0), (0, 1)), 0),
+    (R, C, 1, 1, 0, 1), (R, C, 1, 2, 0, 1), (FREE, 1, 0, 1, 1), (FREE, 1, 0, 1, 2), (S, X, 1, 0, 1, 0),
+    (S, X, 1, 0, 1, 1), (PRODUCT, 1, ((0, 0), (0, 1)), 1), (R, X, 1, 1, 0, 3), (R, C, 1, 1, 1, 1), (R, C, 1, 2, 1, 1),
+    (FREE, 1, 1, 1, 1), (FREE, 1, 1, 1, 2), (R, X, 1, 1, 0, 4), (R, C, 1, 3, 0, 0), (S, X, 1, 1, 1, 0),
+    (R, C, 1, 3, 1, 0), (R, X, 1, 0, 0, 2), (S, X, 1, 1, 1, 1), (R, C, 1, 3, 0, 1), (R, X, 1, 0, 0, 5),
+    (FINISH, 0, 0), (R, C, 1, 3, 1, 1), (S, X, 1, 0, 1, 3), (R, X, 1, 1, 0, 0), (NEAR, 1, 1, 0, 1),
+    (S, X, 1, 0, 1, 4), (R, X, 1, 1, 0, 1), (NEAR, 1, 1, 0, 2), (S, X, 1, 1, 0, 2), (R, X, 1, 0, 1, 0),
+    (NEAR, 1, 0, 1, 1), (S, X, 1, 1, 0, 5), (R, X, 1, 0, 1, 1), (NEAR, 1, 0, 1, 2), (S, X, 1, 0, 1, 2),
+    (R, X, 1, 1, 1, 0), (NEAR, 1, 1, 1, 1), (S, X, 1, 0, 1, 5), (R, X, 1, 1, 1, 1), (NEAR, 1, 1, 1, 2),
+    (S, X, 1, 1, 1, 2), (R, X, 1, 0, 1, 3), (S, X, 1, 1, 1, 5), (R, X, 1, 0, 1, 4), (S, X, 1, 1, 1, 3),
+    (R, X, 1, 1, 0, 2), (S, X, 1, 1, 1, 4), (R, X, 1, 1, 0, 5), (FINISH, 1, 0), (R, X, 1, 0, 1, 2),
+    (R, X, 1, 0, 1, 5), (FINISH, 0, 1), (R, X, 1, 1, 1, 2), (R, X, 1, 1, 1, 5), (R, X, 1, 1, 1, 3),
+    (R, X, 1, 1, 1, 4), (FINISH, 1, 1),
 )
 
 
@@ -214,9 +218,9 @@
 
 
 def kernel(
-    resid, mix_gain, wq, wk, wv, wg, wo, rate, mlp_gain, wu, wd,
+    resid, mix_gain_in, wq, wk, wv, wg, wo, rate, mlp_gain_in, wu, wd,
     out,
-    w_in, w_out, w_up, w_down, xn, rbuf, after, proj, gated, hid, decay, begun, kept,
+    w_in, w_out, w_up, w_down, xn, rbuf, after, proj, gated, hid, decay, begun, kept, mix_gain, mlp_gain,
     dout, din, sout, rin2, rin1,
     local_sem, w_send, g_send, d_send, s_send, recv,
 ):
@@ -375,6 +379,9 @@
         scale = lax.rsqrt(jnp.mean(values * values, axis=-1, keepdims=True) + EPS)
         return (values * scale * gain).astype(BF16)
 
+    barrier = pltpu.get_barrier_semaphore()
+    for way in device:
+        pl.semaphore_signal(barrier, inc=1, device_id=device[way], device_id_type=MESH)
     loads = []
 
     def load(src, dst):
@@ -385,12 +392,12 @@
     for src, low, wide in ((wq, 0, 128), (wk, 128, 128), (wv, 256, 256), (wg, 512, 256)):
         load(src, w_in.at[fs, :, :, :, low : low + wide])
     loads.append(pltpu.make_async_copy(w_in.at[fs], w_in.at[fs], local_sem.at[0]))
-    for src, dst in ((resid, rbuf), (wo, w_out.at[fs]), (wu, w_up.at[fs]), (wd, w_down.at[fs])):
+    loads.append(load(resid, rbuf))
+    loads.append(load(mix_gain_in, mix_gain))
+    loads.append(load(mlp_gain_in, mlp_gain))
+    for src, dst in ((wo, w_out.at[fs]), (wu, w_up.at[fs]), (wd, w_down.at[fs])):
         loads.append(load(src, dst))
-    barrier = pltpu.get_barrier_semaphore()
-    for way in device:
-        pl.semaphore_signal(barrier, inc=1, device_id=device[way], device_id_type=MESH)
-    for copy in loads[:2]:
+    for copy in loads[:4]:
         copy.wait()
     for h in (0, 1):
         for q in (0, 1):
@@ -416,24 +423,28 @@
     own = x // 2
     sequence = (own, 1 - own)
 
-    def project(which, seq, part):
+    chips = ((2 * own, 2), (2 * (1 - own) + 1 - x % 2, 1), (turn(x, 2), 1))
+
+    def project(which, part):
         blocks = [block(*place) for place in (PLACES[:12], PLACES[12:])[part]]
+        first, count = chips[which] if part == 0 else (2 * sequence[which], 2)
 
         def body(j, carry):
             columns = pl.ds(pl.multiple_of(j * 256, 256), 256)
             lhs = [
-                xn[0, pl.ds(4 * seq, 4), :, :, :, pl.ds(pl.multiple_of(f * 128, 128), 128)].reshape(512, 128)
+                xn[0, pl.ds(2 * first, 2 * count), :, :, :, pl.ds(pl.multiple_of(f * 128, 128), 128)]
+                .reshape(256 * count, 128)
                 for f in blocks
             ]
             rhs = [w_in[f, :, :, :, columns].reshape(128, 256) for f in blocks]
             o = jnp.dot(
                 jnp.concatenate(lhs, axis=1), jnp.concatenate(rhs, axis=0), preferred_element_type=F32
-            )
+            ).reshape(count, 256, 256)
             if part == 0:
-                begun[which, j] = o
+                begun[j, pl.ds(first, count)] = o
             else:
-                o = (begun[which, j] + o).astype(BF16)
-                proj[pl.ds(4 * seq, 4), :, columns] = o.reshape(4, 128, 256)
+                o = (begun[j, pl.ds(first, count)] + o).astype(BF16)
+                proj[pl.ds(2 * first, 2 * count), :, columns] = o.reshape(2 * count, 128, 256)
             return carry
 
         lax.fori_loop(0, 3, body, 0)
@@ -500,7 +511,7 @@
         S: start,
         R: receive,
         DECAY: make_decay,
-        PROJECT: lambda which, part: project(which, sequence[which], part),
+        PROJECT: project,
         RETAIN: lambda which: retain(sequence[which]),
         PRODUCT: partial,
         FAR: add_far,
@@ -510,7 +521,7 @@
         LIFT: lift,
         FINISH: finish,
     }
-    for copy in loads[2:]:
+    for copy in loads[4:]:
         copy.wait()
     for name, *which in SCHEDULE:
         actions[name](*which)
@@ -543,8 +554,8 @@
         kernel,
         out_shape=pltpu.VMEM(tokens, BF16),
         in_specs=[
-            hbm, vmem, hbm, hbm, hbm, hbm, hbm,
-            pl.BlockSpec(memory_space=pltpu.SMEM), vmem, hbm, hbm,
+            hbm, hbm, hbm, hbm, hbm, hbm, hbm,
+            pl.BlockSpec(memory_space=pltpu.SMEM), hbm, hbm, hbm,
         ],
         out_specs=vmem,
         scratch_shapes=[
@@ -559,14 +570,16 @@
             pltpu.VMEM((8, 2, 64, DV), BF16),
             pltpu.VMEM((4, 2, 128, w_up.shape[1]), BF16),
             pltpu.VMEM((LENGTH, LENGTH), F32),
-            pltpu.VMEM((2, wide // 256, LENGTH, 256), F32),
+            pltpu.VMEM((wide // 256, 4, 256, 256), F32),
             pltpu.VMEM((4,) + tokens, F32),
+            pltpu.VMEM((1, D), F32),
+            pltpu.VMEM((1, D), F32),
             pltpu.VMEM((2, 4) + tokens, BF16),
             pltpu.VMEM((2, 4) + tokens, BF16),
             pltpu.VMEM((2, 3) + tokens, BF16),
             pltpu.VMEM((2,) + tokens, BF16),
             pltpu.VMEM((2, 2) + tokens, BF16),
-            dma((5,)),
+            dma((8,)),
             dma((4,)),
             dma((2,)),
             dma((2,)),

time: 94 us -> 93.1 us (level)
  no operation moved by 1% of the time
where the time goes in v6:
time: 93.1 us; the launch traced here: 93 us
  Pallas kernels  91.5 us (98%)
    pallas_call x1, Pallas kernels, on_device(): pl.pallas_call(kernel, out_shape=pltpu.VMEM(tokens, BF16), in_specs=[hbm,...  91.5 us

profile of v6, /device:TPU:1, one launch (start us, length us, event | category | flops | bytes accessed | tf_op | source)
XLA Modules:
  0.0 93.0 jit_solution(2801406928504048616)
XLA Ops:
  0.7 91.5 %shard_map.109 = bf16[2,2,32,2048]{3,2,1,0:T(8,128)(2,1)S(1)} custom-call(bf16[2,2,32,2048]{3,2,1,0:T(8,128)(2,1)} %bitcast.12, f32[1,2048]{1,0:T(1,128)} %bitcast.20, bf16[2,2,32,128]{3,2,1,0:T(8,128)(2,1)} %bitcast.18, bf16[2,2,32,128]{3,2,1,0:T(8,128)(2,1)} %bitcast.19, bf16[2,2,32,256]{3,2,1,0:T(8,128)(2,1)} %bitcast.15, ...), custom_call_target="tpu_custom_call" | custom-call | tf_op jit(solution)/shard_map/pallas_call | solution.py:553
  92.2 0.8 copy.13

commit v7 on v6

--- a/solution.py
+++ b/solution.py
@@ -218,9 +218,9 @@
 
 
 def kernel(
-    resid, mix_gain_in, wq, wk, wv, wg, wo, rate, mlp_gain_in, wu, wd,
+    resid, mix_gain_in, wq, wk, wv, wg, wo, rate_in, mlp_gain_in, wu, wd,
     out,
-    w_in, w_out, w_up, w_down, xn, rbuf, after, proj, gated, hid, decay, begun, kept, mix_gain, mlp_gain,
+    w_in, w_out, w_up, w_down, xn, rbuf, after, proj, gated, hid, decay, begun, kept, mix_gain, mlp_gain, rate,
     dout, din, sout, rin2, rin1,
     local_sem, w_send, g_send, d_send, s_send, recv,
 ):
@@ -395,9 +395,10 @@
     loads.append(load(resid, rbuf))
     loads.append(load(mix_gain_in, mix_gain))
     loads.append(load(mlp_gain_in, mlp_gain))
+    loads.append(load(rate_in, rate))
     for src, dst in ((wo, w_out.at[fs]), (wu, w_up.at[fs]), (wd, w_down.at[fs])):
         loads.append(load(src, dst))
-    for copy in loads[:4]:
+    for copy in loads[:5]:
         copy.wait()
     for h in (0, 1):
         for q in (0, 1):
@@ -521,7 +522,7 @@
         LIFT: lift,
         FINISH: finish,
     }
-    for copy in loads[4:]:
+    for copy in loads[5:]:
         copy.wait()
     for name, *which in SCHEDULE:
         actions[name](*which)
@@ -555,7 +556,7 @@
         out_shape=pltpu.VMEM(tokens, BF16),
         in_specs=[
             hbm, hbm, hbm, hbm, hbm, hbm, hbm,
-            pl.BlockSpec(memory_space=pltpu.SMEM), hbm, hbm, hbm,
+            hbm, hbm, hbm, hbm,
         ],
         out_specs=vmem,
         scratch_shapes=[
@@ -574,6 +575,7 @@
             pltpu.VMEM((4,) + tokens, F32),
             pltpu.VMEM((1, D), F32),
             pltpu.VMEM((1, D), F32),
+            pltpu.SMEM((1,), F32),
             pltpu.VMEM((2, 4) + tokens, BF16),
             pltpu.VMEM((2, 4) + tokens, BF16),
             pltpu.VMEM((2, 3) + tokens, BF16),

time: 93.1 us -> 93.1 us (level)
  no operation moved by 1% of the time
where the time goes in v7:
time: 93.1 us; the launch traced here: 93 us
  Pallas kernels  91.6 us (98%)
    pallas_call x1, Pallas kernels, on_device(): pl.pallas_call(kernel, out_shape=pltpu.VMEM(tokens, BF16), in_specs=[hbm,...  91.6 us

profile of v7, /device:TPU:1, one launch (start us, length us, event | category | flops | bytes accessed | tf_op | source)
XLA Modules:
  0.0 93.0 jit_solution(13038769352991475582)
XLA Ops:
  0.7 91.6 %shard_map.109 = bf16[2,2,32,2048]{3,2,1,0:T(8,128)(2,1)S(1)} custom-call(bf16[2,2,32,2048]{3,2,1,0:T(8,128)(2,1)} %bitcast.12, f32[1,2048]{1,0:T(1,128)} %bitcast.20, bf16[2,2,32,128]{3,2,1,0:T(8,128)(2,1)} %bitcast.18, bf16[2,2,32,128]{3,2,1,0:T(8,128)(2,1)} %bitcast.19, bf16[2,2,32,256]{3,2,1,0:T(8,128)(2,1)} %bitcast.15, ...), custom_call_target="tpu_custom_call" | custom-call | tf_op jit(solution)/shard_map/pallas_call | solution.py:554
  92.2 0.8 copy.13
